TPU v7x, 128 devices: a whole 4x4x4 slice. The times are simulated.
128 devices in a mesh: sp: 16 (over z, y), tp: 8 (over x, core).
Axes of the slice: x: 4, y: 4, z: 4, core: 2. Of those that a mesh axis runs over, the one named last changes fastest.
Arguments:
- tokens: bfloat16 [16384, 2048], P('sp'), may hold values from -6 to 6
- norm_gain: bfloat16 [2048], replicated, may hold values from 0.099609375 to 1.8984375
- query_weight: bfloat16 [2048, 2048], P(None, 'tp'), may hold values from -0.125 to 0.125
- key_weight: bfloat16 [2048, 512], P(None, 'tp'), may hold values from -0.125 to 0.125
- value_weight: bfloat16 [2048, 512], P(None, 'tp'), may hold values from -0.125 to 0.125
- query_gain: float32 [64], replicated, may hold values from 1 to 14
- key_gain: float32 [64], replicated, may hold values from 1 to 14
- sink_logit: float32 [32], P('tp'), may hold values from 4 to 10
- gate_weight: bfloat16 [2048, 4096], P(None, 'tp'), may hold values from -0.125 to 0.125
- inner_weight: bfloat16 [2048, 4096], P(None, 'tp'), may hold values from -0.125 to 0.125
- input_map: bfloat16 [2048, 1024], P(None, 'tp'), may hold values from -0.125 to 0.125
- output_map: bfloat16 [2048, 1024], P(None, 'tp'), may hold values from -0.125 to 0.125
- step_weight: bfloat16 [2048, 2, 64], P(None, None, 'tp'), may hold values from -0.125 to 0.125
- conv_inner: bfloat16 [5, 4096], P(None, 'tp'), may hold values from -2.5 to 2.5
- conv_pair: bfloat16 [5, 2, 1024], P(None, None, 'tp'), may hold values from -2.5 to 2.5
- decay_rate: float32 [2, 64], P(None, 'tp'), may hold values from 1.8310547e-06 to 0.05
- decay_jump: float32 [16384, 2, 64], P('sp', None, 'tp'), may hold values from -1.4000854 to 0
- inner_gain: bfloat16 [4096], P('tp'), may hold values from 0.099609375 to 1.8984375
- attn_out_weight: bfloat16 [2048, 2048], P('tp'), may hold values from -0.25 to 0.25
- ssm_out_weight: bfloat16 [4096, 2048], P('tp'), may hold values from -0.09375 to 0.09375
Outputs:
- mixed: bfloat16 [16384, 2048], P(('sp', 'tp'))
All inputs are finite; a program needn't handle non-finite values.
Results may differ from a plain program's by a relative error of at most 0.025.
The roundings to bfloat16 on the way count: a program that leaves them out, or rounds other values in their place, can miss the bound.
Values may be sent and summed in bfloat16 or wider, within the bound.
No kernel may reach another device: no remote copies, remote signals or barrier semaphores. Data moves between devices by JAX's collectives and lax.ppermute only.
A program may use at most 128 MiB of HBM per device.

v0:
```python
import jax
import jax.numpy as jnp
import numpy as np
from jax import lax
from jax.experimental import pallas as pl
from jax.experimental.pallas import tpu as pltpu
from jax.sharding import Mesh
from jax.sharding import PartitionSpec as P

SP = ("z", "y")
SP_TP = ("z", "y", "x", "c")
ROWS = 1024
WIDTH = 2048
SEQ = 16384
HEADS = 8
STATE = 128
INNER = 512
CONV = INNER + 2 * STATE
CHUNK = 128
CHUNKS = ROWS // CHUNK
EDGE = 16
WINDOW = 128
HEAD = 64
HALF = 32
QHEADS = 4
LINE = 4
PACK = 2 * STATE + 16

NORM_EPS = 1e-05
ROPE_BASE = 500000.0
NEG_FILL = -1e30
F32 = jnp.float32
BF16 = jnp.bfloat16


def rope_tables():
    frequency = ROPE_BASE ** (-np.arange(0, HEAD, 2, dtype=np.float64) / HEAD)
    offsets = np.arange(-WINDOW, ROWS + WINDOW, dtype=np.float64)
    near = frequency[:, None] * offsets[None, :]
    far = frequency[None, :] * (ROWS * np.arange(SEQ // ROWS, dtype=np.float64))[:, None]
    near_table = np.concatenate([np.cos(near), np.sin(near)], axis=0).astype(np.float32)
    far_table = np.concatenate([np.cos(far), np.sin(far)], axis=1).astype(np.float32)
    return near_table, far_table[:, :, None]


def head_spread():
    spread = np.repeat(np.eye(HEADS, dtype=np.float32), INNER // HEADS, axis=1)
    return np.concatenate([spread, spread], axis=0)


def dot(a, b):
    return jnp.dot(a, b, preferred_element_type=F32)


def dot_nt(a, b):
    return lax.dot_general(a, b, (((1,), (1,)), ((), ())), preferred_element_type=F32)


def dot_tn(a, b):
    return lax.dot_general(a, b, (((0,), (0,)), ((), ())), preferred_element_type=F32)


def silu(v):
    return v * (1.0 / (1.0 + jnp.exp(-v)))


def normalise(tokens, gain):
    t = tokens.astype(F32)
    mean = jnp.mean(t * t, axis=-1, keepdims=True)
    return (t * lax.rsqrt(mean + NORM_EPS) * gain).astype(BF16)


def widen(rows, spread):
    high = rows.astype(BF16)
    low = (rows - high.astype(F32)).astype(BF16)
    return dot_tn(jnp.concatenate([high, low], axis=0), spread)


def front_kernel(
    ids, tok, gain, low, high, w_inner, w_in, w_out, w_step, taps, rate, jump, spread,
    normed_ref, x_ref, b_ref, c_ref, cum_ref, step_ref, run_ref, enter_ref, back_ref, state_ref,
    rows, raw,
):
    i = pl.program_id(0)
    g = gain[...]

    def project(n):
        return [dot(n, w[...]).astype(BF16).astype(F32) for w in (w_inner, w_in, w_out)]

    n = normalise(tok[...], g)
    normed_ref[...] = n
    a, b, c = project(n)
    start = pl.multiple_of(EDGE + i * 256, 16)
    rows[pl.ds(start, 256), :INNER] = a
    rows[pl.ds(start, 256), INNER : INNER + STATE] = b
    rows[pl.ds(start, 256), INNER + STATE :] = c
    raw[:, pl.ds(pl.multiple_of(i * 256, 128), 256)] = dot_nt(w_step[...], n).astype(BF16).astype(F32)

    @pl.when(i == pl.num_programs(0) - 1)
    def _():
        edge = normalise(jnp.concatenate([low[...], high[...]], axis=0), g)
        ea, eb, ec = project(edge)
        for value, lo, hi in ((ea, 0, INNER), (eb, INNER, INNER + STATE), (ec, INNER + STATE, CONV)):
            rows[0:EDGE, lo:hi] = value[:EDGE]
            rows[EDGE + ROWS :, lo:hi] = value[EDGE:]
        v = raw[...]
        step = jnp.maximum(v, 0.0) + jnp.log1p(jnp.exp(-jnp.abs(v)))
        step_ref[...] = step
        decay = jump[...] - rate[...] * step
        lane = lax.broadcasted_iota(jnp.int32, (HEADS, CHUNK), 1)
        cums = []
        for k in range(CHUNKS):
            f = decay[:HEADS, k * CHUNK : (k + 1) * CHUNK]
            r = decay[HEADS:, k * CHUNK : (k + 1) * CHUNK]
            for shift in (1, 2, 4, 8, 16, 32, 64):
                f = f + jnp.where(lane >= shift, pltpu.roll(f, shift, 1), 0.0)
                r = r + jnp.where(lane < CHUNK - shift, pltpu.roll(r, CHUNK - shift, 1), 0.0)
            cums.append((f, r))
            cum_ref[:HEADS, k * CHUNK : (k + 1) * CHUNK] = f
            cum_ref[HEADS:, k * CHUNK : (k + 1) * CHUNK] = r
        totals = [(f[:, CHUNK - 1 :], r[:, :1]) for f, r in cums]
        zero = jnp.zeros((HEADS, 1), F32)
        ahead = zero
        for k in range(CHUNKS):
            run_ref[:HEADS, k * CHUNK : (k + 1) * CHUNK] = cums[k][0] + ahead
            ahead = ahead + totals[k][0]
        behind = zero
        for k in reversed(range(CHUNKS)):
            run_ref[HEADS:, k * CHUNK : (k + 1) * CHUNK] = cums[k][1] + behind
            behind = behind + totals[k][1]
        sp = spread[...]
        state_f = jnp.zeros((STATE, INNER), F32)
        state_b = jnp.zeros((STATE, INNER), F32)
        passed = zero
        for k in range(CHUNKS):
            base = EDGE + k * CHUNK - 2
            acc = rows[base : base + CHUNK, :] * taps[0:1, :]
            for t in range(1, 5):
                acc = acc + rows[base + t : base + t + CHUNK, :] * taps[t : t + 1, :]
            act = silu(acc)
            here = slice(k * CHUNK, (k + 1) * CHUNK)
            x = act[:, :INNER].astype(BF16)
            bm = act[:, INNER : INNER + STATE].astype(BF16)
            x_ref[here, :] = x
            b_ref[here, :] = bm
            c_ref[here, :] = act[:, INNER + STATE :].astype(BF16)
            f, r = cums[k]
            tf, tr = totals[k]
            wf = jnp.exp(tf - f) * step[:HEADS, here]
            wr = jnp.exp(tr - r) * step[HEADS:, here]
            df = jnp.broadcast_to(jnp.exp(tf), (HEADS, CHUNK))
            dr = jnp.broadcast_to(jnp.exp(passed), (HEADS, CHUNK))
            wide = widen(jnp.concatenate([wf, wr, df, dr], axis=1), sp)
            xf = act[:, :INNER]
            fresh_f = dot_tn(bm, (xf * wide[:CHUNK]).astype(BF16))
            fresh_b = dot_tn(bm, (xf * wide[CHUNK : 2 * CHUNK]).astype(BF16))
            enter_ref[k] = state_f.astype(BF16)
            back_ref[k] = fresh_b.astype(BF16)
            state_f = state_f * wide[2 * CHUNK : 3 * CHUNK] + fresh_f
            state_b = state_b + fresh_b * wide[3 * CHUNK :]
            passed = passed + tr
        state_ref[:STATE, :] = state_f.astype(BF16)
        state_ref[STATE : 2 * STATE, :] = state_b.astype(BF16)
        parts = jnp.zeros((HEADS, CHUNK), F32)
        column = 0
        for total in (ahead, passed):
            rest = total
            for _ in range(3):
                piece = rest.astype(BF16).astype(F32)
                rest = rest - piece
                parts = jnp.where(lane == column, piece, parts)
                column += 1
        state_ref[2 * STATE :, :] = dot_tn(parts.astype(BF16), sp[:HEADS]).astype(BF16)[:16]


def logs_of(ref):
    tail = ref[2 * STATE :, :].astype(F32)
    return tail[0:1] + tail[1:2] + tail[2:3], tail[3:4] + tail[4:5] + tail[5:6]


def line_kernel(ids, own, d1, d2, d3, total_ref, part_ref):
    place = ids[2]
    got = (own, d1, d2, d3)
    logs = [logs_of(r) for r in got]
    state = lambda r, back: r[STATE * back : STATE * (back + 1), :].astype(F32)
    out_logs = []
    for back in (0, 1):
        near = (lambda d: d) if back == 0 else (lambda d: LINE - d)
        count = place if back == 0 else LINE - 1 - place
        far_count = LINE - 1 - count
        prefix = jnp.zeros((STATE, INNER), F32)
        log_prefix = jnp.zeros((1, INNER), F32)
        for d in range(1, LINE):
            r = near(d)
            live = d <= count
            weight = jnp.where(live, jnp.exp(log_prefix), 0.0)
            prefix = prefix + weight * state(got[r], back)
            log_prefix = log_prefix + jnp.where(live, logs[r][back], 0.0)
        total = jnp.zeros((STATE, INNER), F32)
        suffix = jnp.zeros((1, INNER), F32)
        for e in reversed(range(1, LINE)):
            r = near(LINE - e)
            live = e <= far_count
            weight = jnp.where(live, jnp.exp(suffix), 0.0)
            total = total + weight * state(got[r], back)
            suffix = suffix + jnp.where(live, logs[r][back], 0.0)
        total = total + jnp.exp(suffix) * state(own, back)
        suffix = suffix + logs[0][back]
        total = total + jnp.exp(suffix) * prefix
        total_ref[STATE * back : STATE * (back + 1), :] = total.astype(BF16)
        part_ref[STATE * back : STATE * (back + 1), :] = prefix
        part_ref[2 * STATE + back : 2 * STATE + back + 1, :] = log_prefix
        out_logs.append(suffix + log_prefix)
    pieces = []
    for total in out_logs:
        rest = total
        for _ in range(3):
            piece = rest.astype(BF16).astype(F32)
            rest = rest - piece
            pieces.append(piece)
    pieces.append(jnp.zeros((10, INNER), F32))
    total_ref[2 * STATE :, :] = jnp.concatenate(pieces, axis=0).astype(BF16)


def attend_kernel(
    ids, sink, normed, low, high, gain, w_q, w_k, w_v, w_g, q_gain, k_gain, near, far,
    gate_ref, attn_ref, qs, ks, vs,
):
    i = pl.program_id(0)
    n = normed[...]
    far_cos = far[0, :HALF, :]
    far_sin = far[0, HALF:, :]

    def turn(head, at, size):
        co = near[:HALF, pl.ds(at, size)]
        so = near[HALF:, pl.ds(at, size)]
        cos = far_cos * co - far_sin * so
        sin = far_sin * co + far_cos * so
        u, w = head[:HALF], head[HALF:]
        return jnp.concatenate([u * cos - w * sin, w * cos + u * sin], axis=0)

    def head_norm(head, scale):
        mean = jnp.mean(head * head, axis=0, keepdims=True)
        return head * lax.rsqrt(mean + NORM_EPS) * scale

    def keys_values(m, at, size):
        k = dot_nt(w_k[...], m).astype(BF16).astype(F32)
        ks[:, pl.ds(at, size)] = turn(head_norm(k, k_gain[...]), at, size).astype(BF16)
        vs[:, pl.ds(at, size)] = dot_nt(w_v[...], m).astype(BF16)

    at = pl.multiple_of(WINDOW + i * 256, 128)
    gate_ref[...] = dot(n, w_g[...]).astype(BF16)
    keys_values(n, at, 256)
    q = dot(n, w_q[...]).astype(BF16).astype(F32).T
    for h in range(QHEADS):
        head = turn(head_norm(q[h * HEAD : (h + 1) * HEAD], q_gain[...]), at, 256)
        qs[h * HEAD : (h + 1) * HEAD, pl.ds(pl.multiple_of(i * 256, 128), 256)] = (
            head.astype(BF16) * jnp.asarray(HEAD**-0.5, BF16)
        )

    @pl.when(i == pl.num_programs(0) - 1)
    def _():
        g = gain[...]
        keys_values(normalise(low[...], g), 0, WINDOW)
        keys_values(normalise(high[...], g), WINDOW + ROWS, WINDOW)
        reach = 3 * WINDOW
        span = QHEADS * WINDOW
        sinks = jnp.concatenate([jnp.full((1, WINDOW), sink[h], F32) for h in range(QHEADS)], axis=1)
        jj = lax.broadcasted_iota(jnp.int32, (reach, span), 0)
        ii = lax.broadcasted_iota(jnp.int32, (reach, span), 1) % WINDOW
        band = (jj >= ii) & (jj <= ii + 2 * WINDOW)
        first = ids[0] * ROWS - WINDOW

        def block(j, _):
            here = pl.multiple_of(j * WINDOW, 128)
            kb = ks[:, pl.ds(here, reach)]
            vb = vs[:, pl.ds(here, reach)]
            qb = jnp.concatenate(
                [qs[h * HEAD : (h + 1) * HEAD, pl.ds(here, WINDOW)] for h in range(QHEADS)], axis=1
            )
            s = dot_tn(kb, qb)
            position = jj + (first + j * WINDOW)
            s = jnp.where(band & (position >= 0) & (position < SEQ), s, NEG_FILL)
            top = jnp.maximum(jnp.max(s, axis=0, keepdims=True), sinks)
            p = jnp.exp(s - top)
            scale = 1.0 / (jnp.sum(p, axis=0, keepdims=True) + jnp.exp(sinks - top))
            o = dot(vb, (p * scale).astype(BF16))
            o = jnp.concatenate(
                [o[:, h * WINDOW : (h + 1) * WINDOW] for h in range(QHEADS)], axis=0
            )
            attn_ref[pl.ds(here, WINDOW), :] = o.T.astype(BF16)
            return 0

        lax.fori_loop(0, ROWS // WINDOW, block, 0)


def mixer_kernel(x_ref, b_ref, c_ref, cum_ref, step_ref, enter_ref, back_ref, spread, y_ref, state):
    @pl.when(pl.program_id(0) == 0)
    def _():
        state[...] = jnp.zeros_like(state)

    x = x_ref[...]
    c = c_ref[...]
    scores = dot_nt(c, b_ref[...])
    cum = cum_ref[...]
    step = step_ref[...]
    f, r = cum[:HEADS], cum[HEADS:]
    sf, sr = step[:HEADS], step[HEADS:]
    row_f = jnp.log(sf) - f
    row_r = jnp.log(sr) - r
    row_d = jnp.log(sf + sr)
    columns = cum.T
    tt = lax.broadcasted_iota(jnp.int32, (CHUNK, CHUNK), 0)
    ss = lax.broadcasted_iota(jnp.int32, (CHUNK, CHUNK), 1)
    below, same = tt > ss, tt == ss
    left = lax.broadcasted_iota(jnp.int32, (CHUNK, CHUNK), 1) < HEAD

    def weights(h):
        lower = columns[:, h : h + 1] + row_f[h : h + 1]
        upper = columns[:, HEADS + h : HEADS + h + 1] + row_r[h : h + 1]
        power = jnp.where(below, lower, jnp.where(same, row_d[h : h + 1], upper))
        return (jnp.exp(power) * scores).astype(BF16)

    wide = widen(jnp.concatenate([jnp.exp(f), jnp.exp(r)], axis=1), spread[...])
    across = wide[:CHUNK] * dot(c, enter_ref[0])
    across = across + wide[CHUNK:] * dot(c, state[...].astype(BF16))
    nothing = jnp.zeros((CHUNK, CHUNK), BF16)
    for pair in range(HEADS // 2):
        cols = slice(pair * 2 * HEAD, (pair + 1) * 2 * HEAD)
        both = jnp.concatenate([weights(2 * pair), weights(2 * pair + 1)], axis=1)
        xp = x[:, cols]
        stacked = jnp.concatenate([jnp.where(left, xp, nothing), jnp.where(left, nothing, xp)], axis=0)
        y_ref[:, cols] = dot(both, stacked) + across[:, cols]
    state[...] = state[...] * wide[CHUNK : CHUNK + 1] + back_ref[0].astype(F32)


def finish_kernel(
    ids, part, d1, d2, d3, y_ref, c_ref, run_ref, gate_ref, attn_ref, gain, spread,
    mine_ref, theirs_ref, from_low, from_high, rows,
):
    @pl.when(pl.program_id(0) == 0)
    def _():
        got = (None, d1, d2, d3)
        for back, keep in ((0, from_low), (1, from_high)):
            count = ids[1] if back == 0 else LINE - 1 - ids[1]
            prefix = jnp.zeros((STATE, INNER), F32)
            log_prefix = jnp.zeros((1, INNER), F32)
            for d in range(1, LINE):
                r = got[d if back == 0 else LINE - d]
                live = d <= count
                weight = jnp.where(live, jnp.exp(log_prefix), 0.0)
                prefix = prefix + weight * r[STATE * back : STATE * (back + 1), :].astype(F32)
                log_prefix = log_prefix + jnp.where(live, logs_of(r)[back], 0.0)
            own = part[STATE * back : STATE * (back + 1), :]
            reach = jnp.exp(part[2 * STATE + back : 2 * STATE + back + 1, :])
            keep[...] = (own + reach * prefix).astype(BF16)

    c = c_ref[...]
    run = jnp.exp(run_ref[...])
    size = c.shape[0]
    wide = widen(jnp.concatenate([run[:HEADS], run[HEADS:]], axis=1), spread[...])
    y = y_ref[...] + wide[:size] * dot(c, from_low[...]) + wide[size:] * dot(c, from_high[...])
    y = y * silu(gate_ref[...].astype(F32))
    mean = jnp.mean(y * y, axis=-1, keepdims=True)
    out = (y * lax.rsqrt(mean + NORM_EPS) * gain[...]).astype(BF16)
    rows[:, : QHEADS * HEAD] = attn_ref[...]
    rows[:, QHEADS * HEAD :] = out
    mine_ref[0] = rows[pl.ds(pl.multiple_of(ids[4] * 128, 128), 128), :]
    theirs_ref[0] = rows[pl.ds(pl.multiple_of((1 - ids[4]) * 128, 128), 128), :]


def project_kernel(ids, mine, theirs, wa, ws, pa, ps, o0, o1, o2, o3):
    split = QHEADS * HEAD

    def partial(v, a, b):
        return (dot(v[:, :split], a[...]) + dot(v[:, split:], b[...])).astype(BF16).astype(F32)

    value = (partial(mine[0], wa, ws) + partial(theirs[0], pa, ps)).astype(BF16)
    for k, ref in enumerate((o0, o1, o2, o3)):

        @pl.when(pl.program_id(0) == k)
        def _(ref=ref):
            ref[...] = value


def fixed(shape):
    return pl.BlockSpec(shape, lambda i, *_: (0,) * len(shape))


def params():
    return pltpu.CompilerParams(dimension_semantics=("arbitrary",), vmem_limit_bytes=56 << 20)


def cost(flops):
    return pl.CostEstimate(flops=int(flops), transcendentals=0, bytes_accessed=8 << 20)


def shaped(shape, dtype):
    return jax.ShapeDtypeStruct(shape, dtype)


def local(
    tokens, norm_gain, query_weight, key_weight, value_weight, query_gain, key_gain, sink_logit,
    gate_weight, inner_weight, input_map, output_map, step_weight, conv_inner, conv_pair,
    decay_rate, decay_jump, inner_gain, attn_out_weight, ssm_out_weight,
):
    ids = jnp.stack(
        [lax.axis_index(SP), lax.axis_index("z"), lax.axis_index("y"), lax.axis_index("x"),
         lax.axis_index("c")]
    ).astype(jnp.int32)
    up = [(k, k + 1) for k in range(15)]
    down = [(k + 1, k) for k in range(15)]
    swap = [(0, 1), (1, 0)]
    edge_low = lax.ppermute(tokens[ROWS - EDGE :], SP, up)
    edge_high = lax.ppermute(tokens[:EDGE], SP, down)
    halo_low = lax.ppermute(tokens[ROWS - WINDOW :], SP, up)
    halo_high = lax.ppermute(tokens[:WINDOW], SP, down)
    attn_partner = lax.ppermute(attn_out_weight, "c", swap)
    ssm_partner = lax.ppermute(ssm_out_weight, "c", swap)

    gain = norm_gain.astype(F32)[None, :]
    taps = jnp.concatenate([conv_inner, conv_pair.reshape(5, -1)], axis=1).astype(F32)
    spread = jnp.asarray(head_spread(), BF16)
    step_rows = jnp.transpose(step_weight, (1, 2, 0)).reshape(2 * HEADS, WIDTH)
    jump = jnp.transpose(decay_jump, (1, 2, 0)).reshape(2 * HEADS, ROWS)
    rate = decay_rate.reshape(2 * HEADS, 1)
    normed, x, b, c, cum, step, run, enter, back, state = pl.pallas_call(
        front_kernel,
        grid_spec=pltpu.PrefetchScalarGridSpec(
            num_scalar_prefetch=1,
            grid=(4,),
            in_specs=[
                pl.BlockSpec((256, WIDTH), lambda i, _: (i, 0)),
                fixed((1, WIDTH)), fixed((EDGE, WIDTH)), fixed((EDGE, WIDTH)),
                fixed((WIDTH, INNER)), fixed((WIDTH, STATE)), fixed((WIDTH, STATE)),
                fixed((2 * HEADS, WIDTH)), fixed((5, CONV)), fixed((2 * HEADS, 1)),
                fixed((2 * HEADS, ROWS)), fixed((2 * HEADS, INNER)),
            ],
            out_specs=[
                pl.BlockSpec((256, WIDTH), lambda i, _: (i, 0)),
                fixed((ROWS, INNER)), fixed((ROWS, STATE)), fixed((ROWS, STATE)),
                fixed((2 * HEADS, ROWS)), fixed((2 * HEADS, ROWS)), fixed((2 * HEADS, ROWS)),
                fixed((CHUNKS, STATE, INNER)), fixed((CHUNKS, STATE, INNER)), fixed((PACK, INNER)),
            ],
            scratch_shapes=[
                pltpu.VMEM((ROWS + 2 * EDGE, CONV), F32),
                pltpu.VMEM((2 * HEADS, ROWS), F32),
            ],
        ),
        out_shape=[
            shaped((ROWS, WIDTH), BF16), shaped((ROWS, INNER), BF16), shaped((ROWS, STATE), BF16),
            shaped((ROWS, STATE), BF16), shaped((2 * HEADS, ROWS), F32),
            shaped((2 * HEADS, ROWS), F32), shaped((2 * HEADS, ROWS), F32),
            shaped((CHUNKS, STATE, INNER), BF16), shaped((CHUNKS, STATE, INNER), BF16),
            shaped((PACK, INNER), BF16),
        ],
        compiler_params=params(),
        cost_estimate=cost(10e9),
        name="front",
    )(ids, tokens, gain, edge_low, edge_high, inner_weight, input_map, output_map, step_rows, taps,
      rate, jump, spread)

    def along(value, axis):
        return [
            lax.ppermute(value, axis, [(k, (k + d) % LINE) for k in range(LINE)]) for d in (1, 2, 3)
        ]

    got = along(state, "y")

    near, far = (jnp.asarray(t) for t in rope_tables())
    gate, attn = pl.pallas_call(
        attend_kernel,
        grid_spec=pltpu.PrefetchScalarGridSpec(
            num_scalar_prefetch=2,
            grid=(4,),
            in_specs=[
                pl.BlockSpec((256, WIDTH), lambda i, *_: (i, 0)),
                fixed((WINDOW, WIDTH)), fixed((WINDOW, WIDTH)), fixed((1, WIDTH)),
                fixed((WIDTH, QHEADS * HEAD)), fixed((HEAD, WIDTH)), fixed((HEAD, WIDTH)),
                fixed((WIDTH, INNER)), fixed((HEAD, 1)), fixed((HEAD, 1)),
                fixed((HEAD, ROWS + 2 * WINDOW)),
                pl.BlockSpec((1, HEAD, 1), lambda i, ids, _: (ids[0], 0, 0)),
            ],
            out_specs=[
                pl.BlockSpec((256, INNER), lambda i, *_: (i, 0)),
                fixed((ROWS, QHEADS * HEAD)),
            ],
            scratch_shapes=[
                pltpu.VMEM((QHEADS * HEAD, ROWS), BF16),
                pltpu.VMEM((HEAD, ROWS + 2 * WINDOW), BF16),
                pltpu.VMEM((HEAD, ROWS + 2 * WINDOW), BF16),
            ],
        ),
        out_shape=[shaped((ROWS, INNER), BF16), shaped((ROWS, QHEADS * HEAD), BF16)],
        compiler_params=params(),
        cost_estimate=cost(12e9),
        name="attend",
    )(ids, sink_logit, normed, halo_low, halo_high, gain, query_weight, key_weight.T, value_weight.T,
      gate_weight, query_gain[:, None], key_gain[:, None], near, far)

    total, part = pl.pallas_call(
        line_kernel,
        grid_spec=pltpu.PrefetchScalarGridSpec(
            num_scalar_prefetch=1,
            grid=(1,),
            in_specs=[fixed((PACK, INNER))] * 4,
            out_specs=[fixed((PACK, INNER)), fixed((PACK, INNER))],
        ),
        out_shape=[shaped((PACK, INNER), BF16), shaped((PACK, INNER), F32)],
        compiler_params=params(),
        name="line",
    )(ids, state, *got)

    far_got = along(total, "z")

    down_by = lambda i, *_: (CHUNKS - 1 - i, 0)
    lanes_by = lambda i, *_: (0, CHUNKS - 1 - i)
    y = pl.pallas_call(
        mixer_kernel,
        grid_spec=pltpu.PrefetchScalarGridSpec(
            num_scalar_prefetch=0,
            grid=(CHUNKS,),
            in_specs=[
                pl.BlockSpec((CHUNK, INNER), down_by), pl.BlockSpec((CHUNK, STATE), down_by),
                pl.BlockSpec((CHUNK, STATE), down_by), pl.BlockSpec((2 * HEADS, CHUNK), lanes_by),
                pl.BlockSpec((2 * HEADS, CHUNK), lanes_by),
                pl.BlockSpec((1, STATE, INNER), lambda i: (CHUNKS - 1 - i, 0, 0)),
                pl.BlockSpec((1, STATE, INNER), lambda i: (CHUNKS - 1 - i, 0, 0)),
                fixed((2 * HEADS, INNER)),
            ],
            out_specs=pl.BlockSpec((CHUNK, INNER), down_by),
            scratch_shapes=[pltpu.VMEM((STATE, INNER), F32)],
        ),
        out_shape=shaped((ROWS, INNER), F32),
        compiler_params=params(),
        cost_estimate=cost(10e9),
        name="mixer",
    )(x, b, c, cum, step, enter, back, spread)

    depth = QHEADS * HEAD + INNER
    mine, theirs = pl.pallas_call(
        finish_kernel,
        grid_spec=pltpu.PrefetchScalarGridSpec(
            num_scalar_prefetch=1,
            grid=(4,),
            in_specs=[
                fixed((PACK, INNER)), fixed((PACK, INNER)), fixed((PACK, INNER)), fixed((PACK, INNER)),
                pl.BlockSpec((256, INNER), lambda i, _: (i, 0)),
                pl.BlockSpec((256, STATE), lambda i, _: (i, 0)),
                pl.BlockSpec((2 * HEADS, 256), lambda i, _: (0, i)),
                pl.BlockSpec((256, INNER), lambda i, _: (i, 0)),
                pl.BlockSpec((256, QHEADS * HEAD), lambda i, _: (i, 0)),
                fixed((1, INNER)), fixed((2 * HEADS, INNER)),
            ],
            out_specs=[pl.BlockSpec((1, 128, depth), lambda i, _: (i, 0, 0))] * 2,
            scratch_shapes=[
                pltpu.VMEM((STATE, INNER), BF16), pltpu.VMEM((STATE, INNER), BF16),
                pltpu.VMEM((256, depth), BF16),
            ],
        ),
        out_shape=[shaped((4, 128, depth), BF16)] * 2,
        compiler_params=params(),
        cost_estimate=cost(4e9),
        name="finish",
    )(ids, part, *far_got, y, c, run, gate, attn, inner_gain.astype(F32)[None, :], spread)

    theirs = lax.ppermute(theirs, "c", swap)
    block = lambda i, ids: ((ids[3] + (i + 1)) % 4, 0, 0)
    one, two, three, own = pl.pallas_call(
        project_kernel,
        grid_spec=pltpu.PrefetchScalarGridSpec(
            num_scalar_prefetch=1,
            grid=(4,),
            in_specs=[
                pl.BlockSpec((1, 128, depth), block), pl.BlockSpec((1, 128, depth), block),
                fixed((QHEADS * HEAD, WIDTH)), fixed((INNER, WIDTH)),
                fixed((QHEADS * HEAD, WIDTH)), fixed((INNER, WIDTH)),
            ],
            out_specs=[fixed((128, WIDTH))] * 4,
        ),
        out_shape=[shaped((128, WIDTH), BF16)] * 4,
        compiler_params=params(),
        cost_estimate=cost(4e9),
        name="project",
    )(ids, mine, theirs, attn_out_weight, ssm_out_weight, attn_partner, ssm_partner)

    result = own.astype(F32)
    for d, value in ((1, one), (2, two), (3, three)):
        sent = lax.ppermute(value, "x", [(k, (k + d) % 4) for k in range(4)])
        result = result + sent.astype(F32)
    return result.astype(BF16)


def solution(mesh):
    split = Mesh(mesh.devices.reshape(4, 4, 4, 2), SP_TP)
    tp = ("x", "c")
    placed = (
        P(SP, None), P(), P(None, tp), P(None, tp), P(None, tp), P(), P(), P(tp),
        P(None, tp), P(None, tp), P(None, tp), P(None, tp), P(None, None, tp), P(None, tp),
        P(None, None, tp), P(None, tp), P(SP, None, tp), P(tp), P(tp, None), P(tp, None),
    )
    return jax.shard_map(
        local, mesh=split, in_specs=placed, out_specs=P(SP_TP, None), check_vma=False
    )
```

profile of v0, /device:TPU:1, one launch (start us, length us, event | category | flops | bytes accessed | tf_op | source)
XLA Modules:
  0.0 139.2 jit_solution(7863300265713833191)
XLA Ops:
  1.0 4.0 %collective-permute-start = (bf16[16,2048]{1,0:T(8,128)(2,1)S(1)}, bf16[16,2048]{1,0:T(8,128)(2,1)S(1)}, u32[]{:S(2)}, u32[]{:S(2)}) collective-permute-start(bf16[16,2048]{1,0:T(8,128)(2,1)S(1)} %get-tuple-element.48), channel_id=1, source_target_pairs={{0,8},{8,16},{16,24},{24,32},{32,40},{40,48},{48,56},{56,64},{64,7... | collective-permute-start | bytes 196616 | tf_op jit(solution)/shard_map/ppermute | solution.py:414
  5.0 1.3 collective-permute-start.1
  6.3 1.3 fusion
  7.6 4.8 %collective-permute-start.8 = (bf16[128,2048]{1,0:T(8,128)(2,1)S(1)}, bf16[128,2048]{1,0:T(8,128)(2,1)}, u32[]{:S(2)}, u32[]{:S(2)}) collective-permute-start(bf16[128,2048]{1,0:T(8,128)(2,1)S(1)} %get-tuple-element.46), channel_id=1, source_target_pairs={{0,8},{8,16},{16,24},{24,32},{32,40},{40,48},{48,56},{56,64},{64,7... | collective-permute-start | bytes 1572872 | tf_op jit(solution)/shard_map/ppermute | solution.py:416
  12.4 1.3 collective-permute-start.9
  18.8 19.7 %front.1 = (bf16[1024,2048]{1,0:T(8,128)(2,1)}, bf16[1024,512]{1,0:T(8,128)(2,1)}, bf16[1024,128]{1,0:T(8,128)(2,1)}, bf16[1024,128]{1,0:T(8,128)(2,1)}, f32[16,...) custom-call(s32[5]{0:T(128)} %stack.23.ids, ...), custom_call_target="tpu_custom_call" | custom-call | flops 10000000000 | bytes 8388608 | tf_op jit(solution)/shard_map/front/pallas_call | solution.py:427
  38.5 2.2 %collective-permute-start.2 = (bf16[272,512]{1,0:T(8,128)(2,1)}, bf16[272,512]{1,0:T(8,128)(2,1)S(1)}, u32[]{:S(2)}, u32[]{:S(2)}) collective-permute-start(bf16[272,512]{1,0:T(8,128)(2,1)} %get-tuple-element.25.own), channel_id=1, source_target_pairs={{0,8},{8,16},{16,24},{24,0},{1,9},{9,17},{17,25},{25,1},{2,10},{10... | collective-permute-start | bytes 835592 | tf_op jit(solution)/shard_map/ppermute | solution.py:465
  40.7 3.8 %collective-permute-start.3 = (bf16[272,512]{1,0:T(8,128)(2,1)}, bf16[272,512]{1,0:T(8,128)(2,1)S(1)}, u32[]{:S(2)}, u32[]{:S(2)}) collective-permute-start(bf16[272,512]{1,0:T(8,128)(2,1)} %get-tuple-element.25.own), channel_id=1, source_target_pairs={{0,16},{8,24},{16,0},{24,8},{1,17},{9,25},{17,1},{25,9},{2,18},{10... | collective-permute-start | bytes 835592 | tf_op jit(solution)/shard_map/ppermute | solution.py:465
  44.5 9.3 %mixer.1.y_ref = f32[1024,512]{1,0:T(8,128)} custom-call(bf16[1024,512]{1,0:T(8,128)(2,1)} %get-tuple-element.28.x_ref, bf16[1024,128]{1,0:T(8,128)(2,1)} %get-tuple-element.29.b_ref, bf16[1024,128]{1,0:T(8,128)(2,1)} %get-tuple-element.30.c_ref, f32[16,1024]{1,0:T(8,128)} %get-tuple-element.31.cum_ref, f32[16,1024]{1,0:T(8,128)} %get-tuple-element.32.step_ref, ...), custom_call_target="tpu_custom_call" | custom-call | flops 10000000000 | bytes 8388608 | tf_op jit(solution)/shard_map/mixer/pallas_call | solution.py:518
  53.8 2.2 %collective-permute-start.12 = (bf16[512,2048]{1,0:T(8,128)(2,1)S(1)}, bf16[512,2048]{1,0:T(8,128)(2,1)S(1)}, u32[]{:S(2)}, u32[]{:S(2)}) collective-permute-start(bf16[512,2048]{1,0:T(8,128)(2,1)S(1)} %copy-done.10), channel_id=1, source_target_pairs={{0,1},{1,0},{2,3},{3,2},{4,5},{5,4},{6,7},{7,6},{8,9},{9,8},{10,11... | collective-permute-start | bytes 6291464 | tf_op jit(solution)/shard_map/ppermute | solution.py:419
  56.0 2.3 %collective-permute-start.11 = (bf16[256,2048]{1,0:T(8,128)(2,1)S(1)}, bf16[256,2048]{1,0:T(8,128)(2,1)}, u32[]{:S(2)}, u32[]{:S(2)}) collective-permute-start(bf16[256,2048]{1,0:T(8,128)(2,1)S(1)} %copy-done.12), channel_id=1, source_target_pairs={{0,1},{1,0},{2,3},{3,2},{4,5},{5,4},{6,7},{7,6},{8,9},{9,8},{10,11... | collective-permute-start | bytes 3145736 | tf_op jit(solution)/shard_map/ppermute | solution.py:418
  59.0 3.2 %line.1 = (bf16[272,512]{1,0:T(8,128)(2,1)}, f32[272,512]{1,0:T(8,128)}) custom-call(s32[5]{0:T(128)} %stack.23.ids, bf16[272,512]{1,0:T(8,128)(2,1)} %get-tuple-element.25.own, bf16[272,512]{1,0:T(8,128)(2,1)} %copy-done, bf16[272,512]{1,0:T(8,128)(2,1)} %copy-done.1, bf16[272,512]{1,0:T(8,128)(2,1)} %copy-done.2), custom_call_target="tpu_custom_call" | custom-call | tf_op jit(solution)/shard_map/line/pallas_call | solution.py:501
  62.2 3.4 %collective-permute-start.5 = (bf16[272,512]{1,0:T(8,128)(2,1)}, bf16[272,512]{1,0:T(8,128)(2,1)S(1)}, u32[]{:S(2)}, u32[]{:S(2)}) collective-permute-start(bf16[272,512]{1,0:T(8,128)(2,1)} %get-tuple-element.27), channel_id=1, source_target_pairs={{0,32},{32,64},{64,96},{96,0},{1,33},{33,65},{65,97},{97,1},{2,34}... | collective-permute-start | bytes 835592 | tf_op jit(solution)/shard_map/ppermute | solution.py:465
  65.6 3.3 %collective-permute-start.6 = (bf16[272,512]{1,0:T(8,128)(2,1)}, bf16[272,512]{1,0:T(8,128)(2,1)S(1)}, u32[]{:S(2)}, u32[]{:S(2)}) collective-permute-start(bf16[272,512]{1,0:T(8,128)(2,1)} %get-tuple-element.27), channel_id=1, source_target_pairs={{0,64},{32,96},{64,0},{96,32},{1,65},{33,97},{65,1},{97,33},{2,66}... | collective-permute-start | bytes 835592 | tf_op jit(solution)/shard_map/ppermute | solution.py:465
  69.7 18.6 %attend.1 = (bf16[1024,512]{1,0:T(8,128)(2,1)}, bf16[1024,256]{1,0:T(8,128)(2,1)}) custom-call(s32[5]{0:T(128)} %stack.23.ids, f32[4]{0:T(128)} %sink.1, bf16[1024,2048]{1,0:T(8,128)(2,1)} %get-tuple-element.36.normed, bf16[128,2048]{1,0:T(8,128)(2,1)} %collective-permute-done.8.low, bf16[128,2048]{1,0:T(8,128)(2,1)} %collective-permute-done.9.high, ...), custom_call_target="tpu_custom_call" | custom-call | flops 12000000000 | bytes 8388608 | tf_op jit(solution)/shard_map/attend/pallas_call | solution.py:471
  89.1 6.9 %finish.1 = (bf16[4,128,768]{2,1,0:T(8,128)(2,1)}, bf16[4,128,768]{2,1,0:T(8,128)(2,1)}) custom-call(s32[5]{0:T(128)} %stack.23.ids, f32[272,512]{1,0:T(8,128)} %get-tuple-element.26.part, bf16[272,512]{1,0:T(8,128)(2,1)} %copy-done.14, bf16[272,512]{1,0:T(8,128)(2,1)} %copy-done.15, bf16[272,512]{1,0:T(8,128)(2,1)} %copy-done.16, f32[1024,512]{1,0:T(8,128)} %mixer.1.y_ref, ...), custom_call_target="tpu_custom_call" | custom-call | flops 4000000000 | bytes 8388608 | tf_op jit(solution)/shard_map/finish/pallas_call | solution.py:541
  97.0 2.1 %collective-permute-done.10.theirs = bf16[4,128,768]{2,1,0:T(8,128)(2,1)S(1)} collective-permute-done((bf16[4,128,768]{2,1,0:T(8,128)(2,1)}, bf16[4,128,768]{2,1,0:T(8,128)(2,1)S(1)}, u32[]{:S(2)}, u32[]{:S(2)}) %collective-permute-start.10) | collective-permute-done | bytes 786464 | tf_op jit(solution)/shard_map/ppermute | solution.py:567
  100.8 9.5 %project.1 = (bf16[128,2048]{1,0:T(8,128)(2,1)}, bf16[128,2048]{1,0:T(8,128)(2,1)}, bf16[128,2048]{1,0:T(8,128)(2,1)}, bf16[128,2048]{1,0:T(8,128)(2,1)}) custom-call(s32[5]{0:T(128)} %stack.23.ids, bf16[4,128,768]{2,1,0:T(8,128)(2,1)} %get-tuple-element.39.mine, bf16[4,128,768]{2,1,0:T(8,128)(2,1)} %copy-done.13, bf16[256,2048]{1,0:T(8,128)(2,1)} %wa.1, ...), custom_call_target="tpu_custom_call" | custom-call | flops 4000000000 | bytes 8388608 | tf_op jit(solution)/shard_map/project/pallas_call | solution.py:569
  110.2 1.2 collective-permute-start.13
  111.5 2.5 %collective-permute-start.14 = (bf16[128,2048]{1,0:T(8,128)(2,1)}, bf16[128,2048]{1,0:T(8,128)(2,1)S(1)}, u32[]{:S(2)}, u32[]{:S(2)}) collective-permute-start(bf16[128,2048]{1,0:T(8,128)(2,1)} %get-tuple-element.43), channel_id=1, source_target_pairs={{0,4},{2,6},{4,0},{6,2},{1,5},{3,7},{5,1},{7,3},{8,12},{10,14},{12... | collective-permute-start | bytes 1572872 | tf_op jit(solution)/shard_map/ppermute | solution.py:589
  113.9 1.2 collective-permute-start.15
  115.1 9.7 %collective-permute-done.13 = bf16[128,2048]{1,0:T(8,128)(2,1)S(1)} collective-permute-done((bf16[128,2048]{1,0:T(8,128)(2,1)}, bf16[128,2048]{1,0:T(8,128)(2,1)S(1)}, u32[]{:S(2)}, u32[]{:S(2)}) %collective-permute-start.13) | collective-permute-done | bytes 524320 | tf_op jit(solution)/shard_map/ppermute | solution.py:589
  124.8 12.2 %collective-permute-done.14 = bf16[128,2048]{1,0:T(8,128)(2,1)S(1)} collective-permute-done((bf16[128,2048]{1,0:T(8,128)(2,1)}, bf16[128,2048]{1,0:T(8,128)(2,1)S(1)}, u32[]{:S(2)}, u32[]{:S(2)}) %collective-permute-start.14) | collective-permute-done | bytes 524320 | tf_op jit(solution)/shard_map/ppermute | solution.py:589
  137.0 2.2 %add_convert_fusion = bf16[128,2048]{1,0:T(8,128)(2,1)} fusion(bf16[128,2048]{1,0:T(8,128)(2,1)S(1)} %collective-permute-done.15, bf16[128,2048]{1,0:T(8,128)(2,1)S(1)} %collective-permute-done.14, bf16[128,2048]{1,0:T(8,128)(2,1)S(1)} %collective-permute-done.13, bf16[128,2048]{1,0:T(8,128)(2,1)} %get-tuple-element.41), kind=kLoop, calls=%fused_computation | loop fusion | flops 2097152 | bytes 2621440 | tf_op jit(solution)/shard_map/convert_element_type | solution.py:591
  (63 shorter events, 11.0 us)
Async XLA Ops:
  0.0 13.7 %copy-start.4 = (bf16[2048]{0:T(1024)(128)(2,1)S(1)}, bf16[2048]{0:T(1024)(128)(2,1)}, u32[]{:S(2)}) copy-start(bf16[2048]{0:T(1024)(128)(2,1)} %param.24) | copy-start | bytes 12292
  0.0 14.3 %copy-start.5 = (bf16[5,2,128]{2,1,0:T(2,128)(2,1)S(1)}, bf16[5,2,128]{2,1,0:T(2,128)(2,1)}, u32[]{:S(2)}) copy-start(bf16[5,2,128]{2,1,0:T(2,128)(2,1)} %param.37) | copy-start | bytes 7684
  0.0 14.3 %copy-start.6 = (f32[2,8]{1,0:T(2,128)S(1)}, f32[2,8]{1,0:T(2,128)}, u32[]{:S(2)}) copy-start(f32[2,8]{1,0:T(2,128)} %param.38) | copy-start | bytes 196
  0.0 15.0 %copy-start.8 = (f32[64]{0:T(128)S(1)}, f32[64]{0:T(128)}, u32[]{:S(2)}) copy-start(f32[64]{0:T(128)} %param.28) | copy-start | bytes 772
  0.0 15.7 %copy-start.9 = (f32[64]{0:T(128)S(1)}, f32[64]{0:T(128)}, u32[]{:S(2)}) copy-start(f32[64]{0:T(128)} %param.29) | copy-start | bytes 772
  0.0 16.3 %copy-start.7 = (bf16[512]{0:T(512)(128)(2,1)S(1)}, bf16[512]{0:T(512)(128)(2,1)}, u32[]{:S(2)}) copy-start(bf16[512]{0:T(512)(128)(2,1)} %param.40) | copy-start | bytes 3076
  0.0 17.5 %copy-start.3 = (bf16[5,512]{1,0:T(8,128)(2,1)S(1)}, bf16[5,512]{1,0:T(8,128)(2,1)}, u32[]{:S(2)}) copy-start(bf16[5,512]{1,0:T(8,128)(2,1)} %param.36) | copy-start | bytes 15364
  1.0 17.2 %collective-permute-start = (bf16[16,2048]{1,0:T(8,128)(2,1)S(1)}, bf16[16,2048]{1,0:T(8,128)(2,1)S(1)}, u32[]{:S(2)}, u32[]{:S(2)}) collective-permute-start(bf16[16,2048]{1,0:T(8,128)(2,1)S(1)} %get-tuple-element.48), channel_id=1, source_target_pairs={{0,8},{8,16},{16,24},{24,32},{32,40},{40,48},{48,56},{56,64},{64,7... | collective-permute-start | bytes 196616 | tf_op jit(solution)/shard_map/ppermute | solution.py:414
  5.0 13.1 %collective-permute-start.1 = (bf16[16,2048]{1,0:T(8,128)(2,1)S(1)}, bf16[16,2048]{1,0:T(8,128)(2,1)S(1)}, u32[]{:S(2)}, u32[]{:S(2)}) collective-permute-start(bf16[16,2048]{1,0:T(8,128)(2,1)S(1)} %get-tuple-element.47), channel_id=1, source_target_pairs={{8,0},{16,8},{24,16},{32,24},{40,32},{48,40},{56,48},{64,56},{72,6... | collective-permute-start | bytes 196616 | tf_op jit(solution)/shard_map/ppermute | solution.py:415
  7.6 58.0 %collective-permute-start.8 = (bf16[128,2048]{1,0:T(8,128)(2,1)S(1)}, bf16[128,2048]{1,0:T(8,128)(2,1)}, u32[]{:S(2)}, u32[]{:S(2)}) collective-permute-start(bf16[128,2048]{1,0:T(8,128)(2,1)S(1)} %get-tuple-element.46), channel_id=1, source_target_pairs={{0,8},{8,16},{16,24},{24,32},{32,40},{40,48},{48,56},{56,64},{64,7... | collective-permute-start | bytes 1572872 | tf_op jit(solution)/shard_map/ppermute | solution.py:416
  12.4 56.5 %collective-permute-start.9 = (bf16[128,2048]{1,0:T(8,128)(2,1)S(1)}, bf16[128,2048]{1,0:T(8,128)(2,1)}, u32[]{:S(2)}, u32[]{:S(2)}) collective-permute-start(bf16[128,2048]{1,0:T(8,128)(2,1)S(1)} %get-tuple-element.45), channel_id=1, source_target_pairs={{8,0},{16,8},{24,16},{32,24},{40,32},{48,40},{56,48},{64,56},{72,6... | collective-permute-start | bytes 1572872 | tf_op jit(solution)/shard_map/ppermute | solution.py:417
  38.5 15.3 %collective-permute-start.2 = (bf16[272,512]{1,0:T(8,128)(2,1)}, bf16[272,512]{1,0:T(8,128)(2,1)S(1)}, u32[]{:S(2)}, u32[]{:S(2)}) collective-permute-start(bf16[272,512]{1,0:T(8,128)(2,1)} %get-tuple-element.25.own), channel_id=1, source_target_pairs={{0,8},{8,16},{16,24},{24,0},{1,9},{9,17},{17,25},{25,1},{2,10},{10... | collective-permute-start | bytes 835592 | tf_op jit(solution)/shard_map/ppermute | solution.py:465
  40.7 15.3 %collective-permute-start.3 = (bf16[272,512]{1,0:T(8,128)(2,1)}, bf16[272,512]{1,0:T(8,128)(2,1)S(1)}, u32[]{:S(2)}, u32[]{:S(2)}) collective-permute-start(bf16[272,512]{1,0:T(8,128)(2,1)} %get-tuple-element.25.own), channel_id=1, source_target_pairs={{0,16},{8,24},{16,0},{24,8},{1,17},{9,25},{17,1},{25,9},{2,18},{10... | collective-permute-start | bytes 835592 | tf_op jit(solution)/shard_map/ppermute | solution.py:465
  44.5 13.8 %collective-permute-start.4 = (bf16[272,512]{1,0:T(8,128)(2,1)}, bf16[272,512]{1,0:T(8,128)(2,1)S(1)}, u32[]{:S(2)}, u32[]{:S(2)}) collective-permute-start(bf16[272,512]{1,0:T(8,128)(2,1)} %get-tuple-element.25.own), channel_id=1, source_target_pairs={{0,24},{8,0},{16,8},{24,16},{1,25},{9,1},{17,9},{25,17},{2,26},{10... | collective-permute-start | bytes 835592 | tf_op jit(solution)/shard_map/ppermute | solution.py:465
  44.5 11.5 %copy-start.12 = (bf16[256,2048]{1,0:T(8,128)(2,1)S(1)}, bf16[256,2048]{1,0:T(8,128)(2,1)}, u32[]{:S(2)}) copy-start(bf16[256,2048]{1,0:T(8,128)(2,1)} %wa.1) | copy-start | bytes 3145732
  53.8 45.4 %collective-permute-start.12 = (bf16[512,2048]{1,0:T(8,128)(2,1)S(1)}, bf16[512,2048]{1,0:T(8,128)(2,1)S(1)}, u32[]{:S(2)}, u32[]{:S(2)}) collective-permute-start(bf16[512,2048]{1,0:T(8,128)(2,1)S(1)} %copy-done.10), channel_id=1, source_target_pairs={{0,1},{1,0},{2,3},{3,2},{4,5},{5,4},{6,7},{7,6},{8,9},{9,8},{10,11... | collective-permute-start | bytes 6291464 | tf_op jit(solution)/shard_map/ppermute | solution.py:419
  56.0 41.1 %collective-permute-start.11 = (bf16[256,2048]{1,0:T(8,128)(2,1)S(1)}, bf16[256,2048]{1,0:T(8,128)(2,1)}, u32[]{:S(2)}, u32[]{:S(2)}) collective-permute-start(bf16[256,2048]{1,0:T(8,128)(2,1)S(1)} %copy-done.12), channel_id=1, source_target_pairs={{0,1},{1,0},{2,3},{3,2},{4,5},{5,4},{6,7},{7,6},{8,9},{9,8},{10,11... | collective-permute-start | bytes 3145736 | tf_op jit(solution)/shard_map/ppermute | solution.py:418
  62.2 26.0 %collective-permute-start.5 = (bf16[272,512]{1,0:T(8,128)(2,1)}, bf16[272,512]{1,0:T(8,128)(2,1)S(1)}, u32[]{:S(2)}, u32[]{:S(2)}) collective-permute-start(bf16[272,512]{1,0:T(8,128)(2,1)} %get-tuple-element.27), channel_id=1, source_target_pairs={{0,32},{32,64},{64,96},{96,0},{1,33},{33,65},{65,97},{97,1},{2,34}... | collective-permute-start | bytes 835592 | tf_op jit(solution)/shard_map/ppermute | solution.py:465
  65.6 22.6 %collective-permute-start.6 = (bf16[272,512]{1,0:T(8,128)(2,1)}, bf16[272,512]{1,0:T(8,128)(2,1)S(1)}, u32[]{:S(2)}, u32[]{:S(2)}) collective-permute-start(bf16[272,512]{1,0:T(8,128)(2,1)} %get-tuple-element.27), channel_id=1, source_target_pairs={{0,64},{32,96},{64,0},{96,32},{1,65},{33,97},{65,1},{97,33},{2,66}... | collective-permute-start | bytes 835592 | tf_op jit(solution)/shard_map/ppermute | solution.py:465
  68.9 19.3 %collective-permute-start.7 = (bf16[272,512]{1,0:T(8,128)(2,1)}, bf16[272,512]{1,0:T(8,128)(2,1)S(1)}, u32[]{:S(2)}, u32[]{:S(2)}) collective-permute-start(bf16[272,512]{1,0:T(8,128)(2,1)} %get-tuple-element.27), channel_id=1, source_target_pairs={{0,96},{32,0},{64,32},{96,64},{1,97},{33,1},{65,33},{97,65},{2,98}... | collective-permute-start | bytes 835592 | tf_op jit(solution)/shard_map/ppermute | solution.py:465
  96.0 3.1 %collective-permute-start.10 = (bf16[4,128,768]{2,1,0:T(8,128)(2,1)}, bf16[4,128,768]{2,1,0:T(8,128)(2,1)S(1)}, u32[]{:S(2)}, u32[]{:S(2)}) collective-permute-start(bf16[4,128,768]{2,1,0:T(8,128)(2,1)} %get-tuple-element.40), channel_id=1, source_target_pairs={{0,1},{1,0},{2,3},{3,2},{4,5},{5,4},{6,7},{7,6},{8,9},{9,8},{10,11... | collective-permute-start | bytes 2359304 | tf_op jit(solution)/shard_map/ppermute | solution.py:567
  110.2 14.5 %collective-permute-start.13 = (bf16[128,2048]{1,0:T(8,128)(2,1)}, bf16[128,2048]{1,0:T(8,128)(2,1)S(1)}, u32[]{:S(2)}, u32[]{:S(2)}) collective-permute-start(bf16[128,2048]{1,0:T(8,128)(2,1)} %get-tuple-element.42), channel_id=1, source_target_pairs={{0,2},{2,4},{4,6},{6,0},{1,3},{3,5},{5,7},{7,1},{8,10},{10,12},{12... | collective-permute-start | bytes 1572872 | tf_op jit(solution)/shard_map/ppermute | solution.py:589
  111.5 25.5 %collective-permute-start.14 = (bf16[128,2048]{1,0:T(8,128)(2,1)}, bf16[128,2048]{1,0:T(8,128)(2,1)S(1)}, u32[]{:S(2)}, u32[]{:S(2)}) collective-permute-start(bf16[128,2048]{1,0:T(8,128)(2,1)} %get-tuple-element.43), channel_id=1, source_target_pairs={{0,4},{2,6},{4,0},{6,2},{1,5},{3,7},{5,1},{7,3},{8,12},{10,14},{12... | collective-permute-start | bytes 1572872 | tf_op jit(solution)/shard_map/ppermute | solution.py:589
  113.9 23.1 %collective-permute-start.15 = (bf16[128,2048]{1,0:T(8,128)(2,1)}, bf16[128,2048]{1,0:T(8,128)(2,1)S(1)}, u32[]{:S(2)}, u32[]{:S(2)}) collective-permute-start(bf16[128,2048]{1,0:T(8,128)(2,1)} %get-tuple-element.44), channel_id=1, source_target_pairs={{0,6},{2,0},{4,2},{6,4},{1,7},{3,1},{5,3},{7,5},{8,14},{10,8},{12,... | collective-permute-start | bytes 1572872 | tf_op jit(solution)/shard_map/ppermute | solution.py:589
  (11 other events, 22.9 us)
where the time goes:
time: 140 us; the launch traced here: 139 us
  Pallas kernels  67.1 us (48%)
  starting transfers between devices  35 us (25%)
  waiting for transfers between devices  24.1 us (17%)
  local copies, waits for them, and re-layouts  8.72 us (6%)
  other arithmetic  3.97 us (3%)
    ppermute x3, waiting for transfers between devices, local(): sent = lax.ppermute(value, 'x', [(k, (k + d) % 4) for k in range(4)])  21.9 us
    pallas_call x1, Pallas kernels, local(): pl.pallas_call(front_kernel, grid_spec=pltpu.PrefetchScalarGridSpec(num_s...  19.7 us
    pallas_call x1, Pallas kernels, local(): pl.pallas_call(attend_kernel, grid_spec=pltpu.PrefetchScalarGridSpec(num_...  18.6 us
    ppermute x6, starting transfers between devices, along(): lax.ppermute(value, axis, [(k, (k + d) % LINE) for k in range(LINE)])  13.4 us
    pallas_call x1, Pallas kernels, local(): pl.pallas_call(project_kernel, grid_spec=pltpu.PrefetchScalarGridSpec(num...  9.48 us
    pallas_call x1, Pallas kernels, local(): pl.pallas_call(mixer_kernel, grid_spec=pltpu.PrefetchScalarGridSpec(num_s...  9.29 us
    pallas_call x1, Pallas kernels, local(): pl.pallas_call(finish_kernel, grid_spec=pltpu.PrefetchScalarGridSpec(num_...  6.93 us
    ppermute x3, starting transfers between devices, local(): sent = lax.ppermute(value, 'x', [(k, (k + d) % 4) for k in range(4)])  4.82 us
  transfers between devices with their start and end apart: 16, of which 3 were waited for; matrix products, arithmetic and copies ran while one was open for 4% of the time, Pallas kernels for 41%

commit v1 on v0

v1 whole, which is shorter than its diff:
```python
import jax
import jax.numpy as jnp
import numpy as np
from jax import lax
from jax.experimental import pallas as pl
from jax.experimental.pallas import tpu as pltpu
from jax.sharding import Mesh
from jax.sharding import PartitionSpec as P

SP = ("z", "y")
SP_TP = ("z", "y", "x", "c")
ROWS = 1024
WIDTH = 2048
SEQ = 16384
HEADS = 8
STATE = 128
INNER = 512
CONV = INNER + 2 * STATE
CHUNK = 128
CHUNKS = ROWS // CHUNK
EDGE = 16
WINDOW = 128
HEAD = 64
HALF = 32
QHEADS = 4
LINE = 4
PACK = 2 * STATE + 16

NORM_EPS = 1e-05
ROPE_BASE = 500000.0
NEG_FILL = -1e30
F32 = jnp.float32
BF16 = jnp.bfloat16


def rope_tables():
    frequency = ROPE_BASE ** (-np.arange(0, HEAD, 2, dtype=np.float64) / HEAD)
    offsets = np.arange(-WINDOW, ROWS + WINDOW, dtype=np.float64)
    near = frequency[:, None] * offsets[None, :]
    far = frequency[None, :] * (ROWS * np.arange(SEQ // ROWS, dtype=np.float64))[:, None]
    near_table = np.concatenate([np.cos(near), np.sin(near)], axis=0).astype(np.float32)
    far_table = np.concatenate([np.cos(far), np.sin(far)], axis=1).astype(np.float32)
    return near_table, far_table[:, None, :]


def head_spread():
    spread = np.repeat(np.eye(HEADS, dtype=np.float32), INNER // HEADS, axis=1)
    return np.concatenate([spread, spread], axis=0)


def dot(a, b):
    return jnp.dot(a, b, preferred_element_type=F32)


def dot_nt(a, b):
    return lax.dot_general(a, b, (((1,), (1,)), ((), ())), preferred_element_type=F32)


def dot_tn(a, b):
    return lax.dot_general(a, b, (((0,), (0,)), ((), ())), preferred_element_type=F32)


def silu(v):
    return v * (1.0 / (1.0 + jnp.exp(-v)))


def normalise(tokens, gain):
    t = tokens.astype(F32)
    mean = jnp.mean(t * t, axis=-1, keepdims=True)
    return (t * lax.rsqrt(mean + NORM_EPS) * gain).astype(BF16)


def lane_row(ref):
    value = ref[...].astype(F32)
    return jnp.concatenate([value[k : k + 1] for k in range(value.shape[0])], axis=1)


def column(row):
    size = row.shape[1]
    a = lax.broadcasted_iota(jnp.int32, (size, size), 0)
    b = lax.broadcasted_iota(jnp.int32, (size, size), 1)
    return jnp.sum(jnp.where(a == b, row, 0.0), axis=1, keepdims=True)


def fetch(pairs, sems):
    copies = [pltpu.make_async_copy(a, b, sems.at[k]) for k, (a, b) in enumerate(pairs)]
    for copy in copies:
        copy.start()
    return copies


def widen(rows, spread):
    high = rows.astype(BF16)
    low = (rows - high.astype(F32)).astype(BF16)
    return dot_tn(jnp.concatenate([high, low], axis=0), spread)


def edge_kernel(tok, low, high, sems):
    pairs = [(tok.at[pl.ds(ROWS - WINDOW, WINDOW)], low), (tok.at[pl.ds(0, WINDOW)], high)]
    for copy in fetch(pairs, sems):
        copy.wait()


BLOCK = 256


def front_kernel(
    gain, tok, h_inner, h_in, h_out, h_gate, h_step, h_q, h_k, h_v, h_attn, h_ssm,
    normed, rows, raw, gate, w_inner, w_in, w_out, w_q, w_kv, w_attn, w_ssm,
    w_gate, w_step, sems,
):
    blocks = [pl.ds(k * BLOCK, BLOCK) for k in range(ROWS // BLOCK)]
    copies = fetch(
        [(tok.at[blocks[0]], normed.at[blocks[0]]), (h_inner, w_inner), (h_in, w_in), (h_out, w_out)]
        + [(tok.at[b], normed.at[b]) for b in blocks[1:]]
        + [
            (h_gate, w_gate), (h_step, w_step), (h_q, w_q), (h_k, w_kv.at[pl.ds(0, HEAD)]),
            (h_v, w_kv.at[pl.ds(HEAD, HEAD)]), (h_attn, w_attn), (h_ssm, w_ssm),
        ],
        sems,
    )
    g = lane_row(gain)
    for i, block in enumerate(blocks):
        copies[0 if i == 0 else 3 + i].wait()
        n = normalise(normed[block, :], g)
        normed[block, :] = n
        if i == 0:
            for k in (1, 2, 3):
                copies[k].wait()
        for k in range(0, INNER, 2 * STATE):
            value = dot(n, w_inner[:, k : k + 2 * STATE]).astype(BF16).astype(F32)
            rows[k // STATE, block, :] = value[:, :STATE]
            rows[k // STATE + 1, block, :] = value[:, STATE:]
        pair = jnp.concatenate([w_in[...], w_out[...]], axis=1)
        value = dot(n, pair).astype(BF16).astype(F32)
        rows[INNER // STATE, block, :] = value[:, :STATE]
        rows[INNER // STATE + 1, block, :] = value[:, STATE:]
        if i == 0:
            copies[7].wait()
            copies[8].wait()
        gate[block, :] = dot(n, w_gate[...]).astype(BF16)
        raw[:, block] = dot_nt(w_step[...], n).astype(BF16).astype(F32)
    for copy in copies[9:]:
        copy.wait()


def state_kernel(
    rate, rows, raw, low, high, gain, w_inner, w_in, w_out, h_inner_taps, h_pair_taps, h_jump, h_spread,
    x_ref, b_ref, c_ref, cum_ref, step_ref, run_ref, enter_ref, back_ref, state_ref, spread,
    first, last, jump, inner_taps, pair_taps, sems,
):
    copies = fetch(
        [(h_jump, jump), (h_spread, spread), (h_inner_taps, inner_taps), (h_pair_taps, pair_taps)], sems
    )
    g = lane_row(gain)
    edge = normalise(jnp.concatenate([low[WINDOW - EDGE :, :], high[:EDGE, :]], axis=0), g)
    for k in range(CONV // STATE):
        if k < INNER // STATE:
            w = w_inner[:, k * STATE : (k + 1) * STATE]
        else:
            w = (w_in if k == INNER // STATE else w_out)[...]
        value = dot(edge, w).astype(BF16).astype(F32)
        first[k, :EDGE, :] = value[:EDGE]
        first[k, EDGE:, :] = rows[k, : CHUNK + EDGE, :]
        last[k, : CHUNK + EDGE, :] = rows[k, ROWS - CHUNK - EDGE :, :]
        last[k, CHUNK + EDGE :, :] = value[EDGE:]
    for copy in copies:
        copy.wait()
    taps = jnp.concatenate(
        [inner_taps[...].astype(F32)] + [pair_taps[:, k, :].astype(F32) for k in (0, 1)], axis=1
    )
    rates = [
        jnp.concatenate([jnp.full((1, CHUNK), rate[d, h], F32) for h in range(HEADS)], axis=0)
        for d in (0, 1)
    ]
    v = raw[...]
    step = jnp.maximum(v, 0.0) + jnp.log1p(jnp.exp(-jnp.abs(v)))
    step_ref[...] = step
    lane = lax.broadcasted_iota(jnp.int32, (HEADS, CHUNK), 1)
    cums = []
    for k in range(CHUNKS):
        at = slice(k * CHUNK, (k + 1) * CHUNK)
        f = jump[:HEADS, at] - rates[0] * step[:HEADS, at]
        r = jump[HEADS:, at] - rates[1] * step[HEADS:, at]
        for shift in (1, 2, 4, 8, 16, 32, 64):
            f = f + jnp.where(lane >= shift, pltpu.roll(f, shift, 1), 0.0)
            r = r + jnp.where(lane < CHUNK - shift, pltpu.roll(r, CHUNK - shift, 1), 0.0)
        cums.append((f, r))
        cum_ref[:HEADS, k * CHUNK : (k + 1) * CHUNK] = f
        cum_ref[HEADS:, k * CHUNK : (k + 1) * CHUNK] = r
    totals = [(f[:, CHUNK - 1 :], r[:, :1]) for f, r in cums]
    zero = jnp.zeros((HEADS, 1), F32)
    ahead = zero
    for k in range(CHUNKS):
        run_ref[:HEADS, k * CHUNK : (k + 1) * CHUNK] = cums[k][0] + ahead
        ahead = ahead + totals[k][0]
    behind = zero
    for k in reversed(range(CHUNKS)):
        run_ref[HEADS:, k * CHUNK : (k + 1) * CHUNK] = cums[k][1] + behind
        behind = behind + totals[k][1]
    sp = spread[...]
    state_f = jnp.zeros((STATE, INNER), F32)
    state_b = jnp.zeros((STATE, INNER), F32)
    passed = zero
    for k in range(CHUNKS):
        if k == 0:
            source, base = first, EDGE - 2
        elif k == CHUNKS - 1:
            source, base = last, EDGE - 2
        else:
            source, base = rows, k * CHUNK - 2
        here = slice(k * CHUNK, (k + 1) * CHUNK)
        act = []
        for lanes in range(CONV // STATE):
            cols = slice(lanes * STATE, (lanes + 1) * STATE)
            acc = source[lanes, base : base + CHUNK, :] * taps[0:1, cols]
            for t in range(1, 5):
                acc = acc + source[lanes, base + t : base + t + CHUNK, :] * taps[t : t + 1, cols]
            act.append(silu(acc))
        bm = act[-2].astype(BF16)
        b_ref[here, :] = bm
        c_ref[here, :] = act[-1].astype(BF16)
        xf = jnp.concatenate(act[:-2], axis=1)
        x_ref[here, :] = xf.astype(BF16)
        f, r = cums[k]
        tf, tr = totals[k]
        wf = jnp.exp(tf - f) * step[:HEADS, here]
        wr = jnp.exp(tr - r) * step[HEADS:, here]
        df = jnp.broadcast_to(jnp.exp(tf), (HEADS, CHUNK))
        dr = jnp.broadcast_to(jnp.exp(passed), (HEADS, CHUNK))
        wide = widen(jnp.concatenate([wf, wr, df, dr], axis=1), sp)
        fresh_f = dot_tn(bm, (xf * wide[:CHUNK]).astype(BF16))
        fresh_b = dot_tn(bm, (xf * wide[CHUNK : 2 * CHUNK]).astype(BF16))
        enter_ref[k] = state_f.astype(BF16)
        back_ref[k] = fresh_b.astype(BF16)
        state_f = state_f * wide[2 * CHUNK : 3 * CHUNK] + fresh_f
        state_b = state_b + fresh_b * wide[3 * CHUNK :]
        passed = passed + tr
    state_ref[:STATE, :] = state_f.astype(BF16)
    state_ref[STATE : 2 * STATE, :] = state_b.astype(BF16)
    parts = jnp.zeros((HEADS, CHUNK), F32)
    column = 0
    for total in (ahead, passed):
        rest = total
        for _ in range(3):
            piece = rest.astype(BF16).astype(F32)
            rest = rest - piece
            parts = jnp.where(lane == column, piece, parts)
            column += 1
    state_ref[2 * STATE :, :] = dot_tn(parts.astype(BF16), sp[:HEADS]).astype(BF16)[:16]


def logs_of(ref):
    tail = ref[2 * STATE :, :].astype(F32)
    return tail[0:1] + tail[1:2] + tail[2:3], tail[3:4] + tail[4:5] + tail[5:6]


def line_kernel(own, d1, d2, d3, m1, m2, m3, part_ref):
    place, level = lax.axis_index("y"), lax.axis_index("z")
    got = (own, d1, d2, d3)
    logs = [logs_of(r) for r in got]
    state = lambda r, back: r[STATE * back : STATE * (back + 1), :].astype(F32)
    totals = []
    for back in (0, 1):
        near = (lambda d: d) if back == 0 else (lambda d: LINE - d)
        count = place if back == 0 else LINE - 1 - place
        far_count = LINE - 1 - count
        prefix = jnp.zeros((STATE, INNER), F32)
        log_prefix = jnp.zeros((1, INNER), F32)
        for d in range(1, LINE):
            r = near(d)
            live = d <= count
            weight = jnp.where(live, jnp.exp(log_prefix), 0.0)
            prefix = prefix + weight * state(got[r], back)
            log_prefix = log_prefix + jnp.where(live, logs[r][back], 0.0)
        total = jnp.zeros((STATE, INNER), F32)
        suffix = jnp.zeros((1, INNER), F32)
        for e in reversed(range(1, LINE)):
            r = near(LINE - e)
            live = e <= far_count
            weight = jnp.where(live, jnp.exp(suffix), 0.0)
            total = total + weight * state(got[r], back)
            suffix = suffix + jnp.where(live, logs[r][back], 0.0)
        total = total + jnp.exp(suffix) * state(own, back)
        suffix = suffix + logs[0][back]
        total = total + jnp.exp(suffix) * prefix
        part_ref[STATE * back : STATE * (back + 1), :] = prefix
        part_ref[2 * STATE + back : 2 * STATE + back + 1, :] = log_prefix
        rest = suffix + log_prefix
        pieces = []
        for _ in range(3):
            piece = rest.astype(BF16).astype(F32)
            rest = rest - piece
            pieces.append(piece)
        pieces.append(jnp.zeros((13, INNER), F32))
        totals.append((total.astype(BF16), jnp.concatenate(pieces, axis=0).astype(BF16)))
    for d, ref in ((1, m1), (2, m2), (3, m3)):
        for back in (0, 1):

            @pl.when(level + d < LINE if back == 0 else level + d >= LINE)
            def _(ref=ref, back=back):
                ref[:STATE, :] = totals[back][0]
                ref[STATE:, :] = totals[back][1]


def heads_kernel(
    normed, low, high, gain, w_q, w_kv, q_row, k_row, h_near, h_far, qs, ks, vs, near, far, sems
):
    copies = fetch([(h_near, near), (h_far.at[lax.axis_index(SP)], far)], sems)
    q_gain, k_gain = column(q_row[...]), column(k_row[...])
    for copy in copies:
        copy.wait()
    turns = column(far[...])
    far_cos = turns[:HALF, :]
    far_sin = turns[HALF:, :]
    scale = jnp.asarray(HEAD**-0.5, BF16)

    def turn(head, at, size):
        co = near[:HALF, at : at + size]
        so = near[HALF:, at : at + size]
        cos = far_cos * co - far_sin * so
        sin = far_sin * co + far_cos * so
        u, w = head[:HALF], head[HALF:]
        return jnp.concatenate([u * cos - w * sin, w * cos + u * sin], axis=0)

    def head_norm(head, scale):
        mean = jnp.mean(head * head, axis=0, keepdims=True)
        return head * lax.rsqrt(mean + NORM_EPS) * scale

    def keys_values(m, at, size):
        kv = dot_nt(w_kv[...], m).astype(BF16)
        k = head_norm(kv[:HEAD].astype(F32), k_gain)
        ks[:, at : at + size] = turn(k, at, size).astype(BF16)
        vs[:, at : at + size] = kv[HEAD:]

    for i in range(4):
        at = WINDOW + i * 256
        n = normed[i * 256 : (i + 1) * 256, :]
        keys_values(n, at, 256)
        q = dot(n, w_q[...]).astype(BF16).astype(F32).T
        for h in range(QHEADS):
            head = turn(head_norm(q[h * HEAD : (h + 1) * HEAD], q_gain), at, 256)
            qs[h * HEAD : (h + 1) * HEAD, i * 256 : (i + 1) * 256] = head.astype(BF16) * scale
    g = lane_row(gain)
    keys_values(normalise(low[...], g), 0, WINDOW)
    keys_values(normalise(high[...], g), WINDOW + ROWS, WINDOW)


def attend_kernel(sink, qs, ks, vs, attn_ref):
    reach = 3 * WINDOW
    span = QHEADS * WINDOW
    sinks = jnp.concatenate([jnp.full((1, WINDOW), sink[h], F32) for h in range(QHEADS)], axis=1)
    jj = lax.broadcasted_iota(jnp.int32, (reach, span), 0)
    ii = lax.broadcasted_iota(jnp.int32, (reach, span), 1) % WINDOW
    band = (jj >= ii) & (jj <= ii + 2 * WINDOW)
    first = lax.axis_index(SP) * ROWS - WINDOW

    def block(j, _):
        here = pl.multiple_of(j * WINDOW, 128)
        kb = ks[:, pl.ds(here, reach)]
        vb = vs[:, pl.ds(here, reach)]
        qb = jnp.concatenate(
            [qs[h * HEAD : (h + 1) * HEAD, pl.ds(here, WINDOW)] for h in range(QHEADS)], axis=1
        )
        s = dot_tn(kb, qb)
        position = jj + (first + j * WINDOW)
        s = jnp.where(band & (position >= 0) & (position < SEQ), s, NEG_FILL)
        top = jnp.maximum(jnp.max(s, axis=0, keepdims=True), sinks)
        p = jnp.exp(s - top)
        scale = 1.0 / (jnp.sum(p, axis=0, keepdims=True) + jnp.exp(sinks - top))
        o = dot(vb, (p * scale).astype(BF16))
        o = jnp.concatenate([o[:, h * WINDOW : (h + 1) * WINDOW] for h in range(QHEADS)], axis=0)
        attn_ref[pl.ds(here, WINDOW), :] = o.T.astype(BF16)
        return 0

    lax.fori_loop(0, ROWS // WINDOW, block, 0)


def mixer_kernel(x_ref, b_ref, c_ref, cum_ref, step_ref, enter_ref, back_ref, spread, y_ref, state):
    @pl.when(pl.program_id(0) == 0)
    def _():
        state[...] = jnp.zeros_like(state)

    x = x_ref[...]
    c = c_ref[...]
    scores = dot_nt(c, b_ref[...])
    cum = cum_ref[...]
    step = step_ref[...]
    f, r = cum[:HEADS], cum[HEADS:]
    sf, sr = step[:HEADS], step[HEADS:]
    row_f = jnp.log(sf) - f
    row_r = jnp.log(sr) - r
    row_d = jnp.log(sf + sr)
    columns = cum.T
    tt = lax.broadcasted_iota(jnp.int32, (CHUNK, CHUNK), 0)
    ss = lax.broadcasted_iota(jnp.int32, (CHUNK, CHUNK), 1)
    below, same = tt > ss, tt == ss
    left = lax.broadcasted_iota(jnp.int32, (CHUNK, CHUNK), 1) < HEAD

    def weights(h):
        lower = columns[:, h : h + 1] + row_f[h : h + 1]
        upper = columns[:, HEADS + h : HEADS + h + 1] + row_r[h : h + 1]
        power = jnp.where(below, lower, jnp.where(same, row_d[h : h + 1], upper))
        return (jnp.exp(power) * scores).astype(BF16)

    wide = widen(jnp.concatenate([jnp.exp(f), jnp.exp(r)], axis=1), spread[...])
    across = wide[:CHUNK] * dot(c, enter_ref[0])
    across = across + wide[CHUNK:] * dot(c, state[...].astype(BF16))
    nothing = jnp.zeros((CHUNK, CHUNK), BF16)
    for pair in range(HEADS // 2):
        cols = slice(pair * 2 * HEAD, (pair + 1) * 2 * HEAD)
        both = jnp.concatenate([weights(2 * pair), weights(2 * pair + 1)], axis=1)
        xp = x[:, cols]
        stacked = jnp.concatenate([jnp.where(left, xp, nothing), jnp.where(left, nothing, xp)], axis=0)
        y_ref[:, cols] = dot(both, stacked) + across[:, cols]
    state[...] = state[...] * wide[CHUNK : CHUNK + 1] + back_ref[0].astype(F32)


def finish_kernel(
    part, d1, d2, d3, y_ref, c_ref, run_ref, gate_ref, attn_ref, gain, spread,
    mine_ref, theirs_ref, from_low, from_high, rows,
):
    @pl.when(pl.program_id(0) == 0)
    def _():
        got = (None, d1, d2, d3)
        for back, keep in ((0, from_low), (1, from_high)):
            level = lax.axis_index("z")
            count = level if back == 0 else LINE - 1 - level
            prefix = jnp.zeros((STATE, INNER), F32)
            log_prefix = jnp.zeros((1, INNER), F32)
            for d in range(1, LINE):
                r = got[d if back == 0 else LINE - d]
                live = d <= count
                weight = jnp.where(live, jnp.exp(log_prefix), 0.0)
                prefix = prefix + weight * r[:STATE, :].astype(F32)
                tail = r[STATE:, :].astype(F32)
                log = tail[0:1] + tail[1:2] + tail[2:3]
                log_prefix = log_prefix + jnp.where(live, log, 0.0)
            own = part[STATE * back : STATE * (back + 1), :]
            reach = jnp.exp(part[2 * STATE + back : 2 * STATE + back + 1, :])
            keep[...] = (own + reach * prefix).astype(BF16)

    c = c_ref[...]
    run = jnp.exp(run_ref[...])
    size = c.shape[0]
    wide = widen(jnp.concatenate([run[:HEADS], run[HEADS:]], axis=1), spread[...])
    y = y_ref[...] + wide[:size] * dot(c, from_low[...]) + wide[size:] * dot(c, from_high[...])
    y = y * silu(gate_ref[...].astype(F32))
    mean = jnp.mean(y * y, axis=-1, keepdims=True)
    out = (y * lax.rsqrt(mean + NORM_EPS) * lane_row(gain)).astype(BF16)
    rows[:, : QHEADS * HEAD] = attn_ref[...]
    rows[:, QHEADS * HEAD :] = out
    core = lax.axis_index("c")
    mine_ref[0] = rows[pl.ds(pl.multiple_of(core * 128, 128), 128), :]
    theirs_ref[0] = rows[pl.ds(pl.multiple_of((1 - core) * 128, 128), 128), :]


def chunk_partial(order, mine, theirs, wa, ws, pa, ps):
    split = QHEADS * HEAD

    def partial(v, a, b):
        return (dot(v[:, :split], a[...]) + dot(v[:, split:], b[...])).astype(BF16).astype(F32)

    join = lambda ref: jnp.concatenate([ref[index] for index in order], axis=0)
    return partial(join(mine), wa, ws) + partial(join(theirs), pa, ps)


HALVES = 64


def opposite_kernel(mine, theirs, wa, ws, pa, ps, right, left):
    index = (lax.axis_index("x") + 2) % LINE
    value = chunk_partial([index], mine, theirs, wa, ws, pa, ps).astype(BF16)
    right[...] = value[:HALVES]
    left[...] = value[HALVES:]


def beside_kernel(mine, theirs, wa, ws, pa, ps, right, left, keep_right, keep_left, own):
    x = lax.axis_index("x")
    order = [(x + 1) % LINE, (x + 3) % LINE, x]
    value = chunk_partial(order, mine, theirs, wa, ws, pa, ps)
    keep_right[...] = value[:HALVES]
    right[...] = value[HALVES : 2 * HALVES].astype(BF16)
    left[...] = value[2 * HALVES : 3 * HALVES].astype(BF16)
    keep_left[...] = value[3 * HALVES : 4 * HALVES]
    own[...] = value[4 * HALVES :]


HBM = pl.BlockSpec(memory_space=pltpu.HBM)


def whole(count):
    return [pl.BlockSpec(memory_space=pltpu.VMEM)] * count


SCALARS = pl.BlockSpec(memory_space=pltpu.SMEM)


def plain(kernel, name, inputs, outs, scalars=0, remote=0, scratch=(), size=8, flops=1e9):
    return pl.pallas_call(
        kernel,
        in_specs=[SCALARS] * scalars + whole(inputs) + [HBM] * remote,
        out_specs=whole(len(outs)),
        out_shape=outs,
        scratch_shapes=list(scratch),
        compiler_params=pltpu.CompilerParams(vmem_limit_bytes=size << 20),
        cost_estimate=cost(flops),
        name=name,
    )


def fixed(shape):
    return pl.BlockSpec(memory_space=pltpu.VMEM)


def params(size):
    return pltpu.CompilerParams(dimension_semantics=("arbitrary",), vmem_limit_bytes=size << 20)


def cost(flops):
    return pl.CostEstimate(flops=int(flops), transcendentals=0, bytes_accessed=8 << 20)


def shaped(shape, dtype):
    return jax.ShapeDtypeStruct(shape, dtype)


def local(
    tokens, norm_gain, query_weight, key_weight, value_weight, query_gain, key_gain, sink_logit,
    gate_weight, inner_weight, input_map, output_map, step_weight, conv_inner, conv_pair,
    decay_rate, decay_jump, inner_gain, attn_out_weight, ssm_out_weight,
):
    up = [(k, k + 1) for k in range(15)]
    down = [(k + 1, k) for k in range(15)]
    swap = [(0, 1), (1, 0)]
    pin = lambda v: pltpu.with_memory_space_constraint(v, pltpu.HBM)
    edge_low, edge_high = plain(
        edge_kernel, "edge", 0, [shaped((WINDOW, WIDTH), BF16)] * 2, remote=1,
        scratch=[pltpu.SemaphoreType.DMA((2,))], size=2, flops=1e6,
    )(pin(tokens))
    halo_low = lax.ppermute(edge_low, SP, up)
    halo_high = lax.ppermute(edge_high, SP, down)
    attn_partner = lax.ppermute(attn_out_weight, "c", swap)
    ssm_partner = lax.ppermute(ssm_out_weight, "c", swap)

    gain = norm_gain.reshape(WIDTH // 128, 128)
    spread = jnp.asarray(head_spread(), BF16)
    step_rows = jnp.transpose(step_weight, (1, 2, 0)).reshape(2 * HEADS, WIDTH)
    jump = jnp.transpose(decay_jump, (1, 2, 0)).reshape(2 * HEADS, ROWS)
    normed, rows, raw, gate, w_inner, w_in, w_out, w_q, w_kv, w_attn, w_ssm = plain(
        front_kernel, "front", 1,
        [
            shaped((ROWS, WIDTH), BF16), shaped((CONV // STATE, ROWS, STATE), F32),
            shaped((2 * HEADS, ROWS), F32), shaped((ROWS, INNER), BF16),
            shaped((WIDTH, INNER), BF16), shaped((WIDTH, STATE), BF16), shaped((WIDTH, STATE), BF16),
            shaped((WIDTH, QHEADS * HEAD), BF16), shaped((2 * HEAD, WIDTH), BF16),
            shaped((QHEADS * HEAD, WIDTH), BF16), shaped((INNER, WIDTH), BF16),
        ],
        remote=11,
        scratch=[
            pltpu.VMEM((WIDTH, INNER), BF16), pltpu.VMEM((2 * HEADS, WIDTH), BF16),
            pltpu.SemaphoreType.DMA((14,)),
        ],
        size=8, flops=10e9,
    )(gain, *map(pin, (tokens, inner_weight, input_map, output_map, gate_weight, step_rows, query_weight,
      key_weight.T, value_weight.T, attn_out_weight, ssm_out_weight)))

    x, b, c, cum, step, run, enter, back, state, spread = plain(
        state_kernel, "state", 8,
        [
            shaped((ROWS, INNER), BF16), shaped((ROWS, STATE), BF16),
            shaped((ROWS, STATE), BF16), shaped((2 * HEADS, ROWS), F32),
            shaped((2 * HEADS, ROWS), F32), shaped((2 * HEADS, ROWS), F32),
            shaped((CHUNKS, STATE, INNER), BF16), shaped((CHUNKS, STATE, INNER), BF16),
            shaped((PACK, INNER), BF16), shaped((2 * HEADS, INNER), BF16),
        ],
        scalars=1, remote=4,
        scratch=[pltpu.VMEM((CONV // STATE, CHUNK + 2 * EDGE, STATE), F32)] * 2
        + [
            pltpu.VMEM((2 * HEADS, ROWS), F32), pltpu.VMEM((5, INNER), BF16),
            pltpu.VMEM((5, 2, STATE), BF16), pltpu.SemaphoreType.DMA((4,)),
        ],
        size=8, flops=6e9,
    )(decay_rate, rows, raw, halo_low, halo_high, gain, w_inner, w_in, w_out, conv_inner, conv_pair,
      jump, spread)

    def along(values, axis):
        return [
            lax.ppermute(value, axis, [(k, (k + d) % LINE) for k in range(LINE)])
            for d, value in zip((1, 2, 3), values)
        ]

    got = along([state] * 3, "y")

    near, far = rope_tables()
    qs, ks, vs = plain(
        heads_kernel, "heads", 8,
        [
            shaped((QHEADS * HEAD, ROWS), BF16), shaped((HEAD, ROWS + 2 * WINDOW), BF16),
            shaped((HEAD, ROWS + 2 * WINDOW), BF16),
        ],
        remote=2,
        scratch=[
            pltpu.VMEM((HEAD, ROWS + 2 * WINDOW), F32), pltpu.VMEM((1, HEAD), F32),
            pltpu.SemaphoreType.DMA((2,)),
        ],
        size=6, flops=5e9,
    )(normed, halo_low, halo_high, gain, w_q, w_kv, query_gain[None, :], key_gain[None, :],
      jnp.asarray(near), jnp.asarray(far))

    *messages, part = plain(
        line_kernel, "line", 4,
        [shaped((STATE + 16, INNER), BF16)] * 3 + [shaped((PACK, INNER), F32)],
        size=4, flops=1e9,
    )(state, *got)

    far_got = along(messages, "z")

    attn = plain(
        attend_kernel, "attend", 3, [shaped((ROWS, QHEADS * HEAD), BF16)], scalars=1, size=8,
        flops=7e9,
    )(sink_logit, qs, ks, vs)[0]

    down_by = lambda i, *_: (CHUNKS - 1 - i, 0)
    lanes_by = lambda i, *_: (0, CHUNKS - 1 - i)
    y = pl.pallas_call(
        mixer_kernel,
        grid_spec=pltpu.PrefetchScalarGridSpec(
            num_scalar_prefetch=0,
            grid=(CHUNKS,),
            in_specs=[
                pl.BlockSpec((CHUNK, INNER), down_by), pl.BlockSpec((CHUNK, STATE), down_by),
                pl.BlockSpec((CHUNK, STATE), down_by), pl.BlockSpec((2 * HEADS, CHUNK), lanes_by),
                pl.BlockSpec((2 * HEADS, CHUNK), lanes_by),
                pl.BlockSpec((1, STATE, INNER), lambda i: (CHUNKS - 1 - i, 0, 0)),
                pl.BlockSpec((1, STATE, INNER), lambda i: (CHUNKS - 1 - i, 0, 0)),
                fixed((2 * HEADS, INNER)),
            ],
            out_specs=pl.BlockSpec((CHUNK, INNER), down_by),
            scratch_shapes=[pltpu.VMEM((STATE, INNER), F32)],
        ),
        out_shape=shaped((ROWS, INNER), F32),
        compiler_params=params(6),
        cost_estimate=cost(10e9),
        name="mixer",
    )(x, b, c, cum, step, enter, back, spread)

    depth = QHEADS * HEAD + INNER
    mine, theirs = pl.pallas_call(
        finish_kernel,
        grid=(4,),
        in_specs=whole(4) + [
            pl.BlockSpec((256, INNER), lambda i: (i, 0)),
            pl.BlockSpec((256, STATE), lambda i: (i, 0)),
            pl.BlockSpec((2 * HEADS, 256), lambda i: (0, i)),
            pl.BlockSpec((256, INNER), lambda i: (i, 0)),
            pl.BlockSpec((256, QHEADS * HEAD), lambda i: (i, 0)),
        ] + whole(2),
        out_specs=[pl.BlockSpec((1, 128, depth), lambda i: (i, 0, 0))] * 2,
        scratch_shapes=[
            pltpu.VMEM((STATE, INNER), BF16), pltpu.VMEM((STATE, INNER), BF16),
            pltpu.VMEM((256, depth), BF16),
        ],
        out_shape=[shaped((4, 128, depth), BF16)] * 2,
        compiler_params=params(8),
        cost_estimate=cost(4e9),
        name="finish",
    )(part, *far_got, y, c, run, gate, attn, inner_gain.reshape(INNER // 128, 128), spread)

    theirs = lax.ppermute(theirs, "c", swap)
    operands = (
        mine, theirs, w_attn, w_ssm, attn_partner, ssm_partner
    )
    sent = shaped((HALVES, WIDTH), BF16)
    kept = shaped((HALVES, WIDTH), F32)
    right = [(k, (k + 1) % LINE) for k in range(LINE)]
    left = [((k + 1) % LINE, k) for k in range(LINE)]
    shift_right = lambda value: lax.ppermute(value, "x", right)
    shift_left = lambda value: lax.ppermute(value, "x", left)
    relay_right, relay_left = plain(
        opposite_kernel, "opposite", 6, [sent, sent], flops=1e9
    )(*operands)
    relay_right = shift_right(relay_right)
    relay_left = shift_left(relay_left)
    direct_right, direct_left, keep_right, keep_left, own = plain(
        beside_kernel, "beside", 6, [sent, sent, kept, kept, shaped((2 * HALVES, WIDTH), F32)],
        flops=3e9,
    )(*operands)
    direct_right = shift_right(direct_right)
    direct_left = shift_left(direct_left)
    last_right = shift_right((keep_right + relay_right.astype(F32)).astype(BF16))
    last_left = shift_left((keep_left + relay_left.astype(F32)).astype(BF16))
    upper = own[:HALVES] + direct_left.astype(F32) + last_right.astype(F32)
    lower = own[HALVES:] + direct_right.astype(F32) + last_left.astype(F32)
    return jnp.concatenate([upper, lower], axis=0).astype(BF16)


def solution(mesh):
    split = Mesh(mesh.devices.reshape(4, 4, 4, 2), SP_TP)
    tp = ("x", "c")
    placed = (
        P(SP, None), P(), P(None, tp), P(None, tp), P(None, tp), P(), P(), P(tp),
        P(None, tp), P(None, tp), P(None, tp), P(None, tp), P(None, None, tp), P(None, tp),
        P(None, None, tp), P(None, tp), P(SP, None, tp), P(tp), P(tp, None), P(tp, None),
    )
    return jax.shard_map(
        local, mesh=split, in_specs=placed, out_specs=P(SP_TP, None), check_vma=False
    )
```

time: 140 us -> 90.2 us (0.64)
  Pallas kernels: 67.1 us -> 43.3 us
  waiting for transfers between devices: 24.1 us -> 14.7 us
  local copies, waits for them, and re-layouts: 8.72 us -> 0.06 us
  starting transfers between devices: 35 us -> 30.1 us
  other arithmetic: 3.97 us -> 1.14 us
    pallas_call x5 -> x9, Pallas kernels: 57.9 us -> 37.3 us  [the longest x1 11.4 us: local(): plain(front_kernel, 'front', 1, [shaped((ROWS, WIDTH), BF16), shaped((CON...]
    ppermute x7 -> x8, waiting for transfers between devices: 21.9 us -> 10.8 us  [the longest x3 5.88 us: local(): shift_right = lambda value: lax.ppermute(value, 'x', right)]
    unnamed x39 -> x28, local copies, waits for them, and re-layouts: 3.88 us -> 0.06 us
    pallas_call x1, Pallas kernels: 9.29 us -> 5.98 us  [local(): pl.pallas_call(mixer_kernel, grid_spec=pltpu.PrefetchScalarGridSpec(num_s...]
    convert_element_type x2, other arithmetic: 2.77 us -> 0.12 us  [the longest x1 0.06 us: local(): last_left = shift_left((keep_left + relay_left.astype(F32)).astype(BF16))]
    slice x2 -> x0, local copies, waits for them, and re-layouts: 2.21 us -> none  [the longest x1 1.27 us: local(): halo_high = lax.ppermute(tokens[:WINDOW], SP, down)]
    ppermute x1, starting transfers between devices: 2.31 us -> 0.1 us  [local(): attn_partner = lax.ppermute(attn_out_weight, 'c', swap)]
    ppermute x7 -> x8, starting transfers between devices: 16.2 us -> 14 us  [the longest x3 8.61 us: local(): shift_left = lambda value: lax.ppermute(value, 'x', left)]
  transfers between devices with their start and end apart: 16 -> 17, of which waited for: 3 -> 8; matrix products, arithmetic and copies ran while one was open for 4% -> 0% of each run, Pallas kernels for 41% -> 46%
where the time goes in v1:
time: 90.2 us; the launch traced here: 89.6 us
  Pallas kernels  43.3 us (48%)
  starting transfers between devices  30.1 us (33%)
  waiting for transfers between devices  14.7 us (16%)
  other arithmetic  1.14 us (1%)
    ppermute x6, starting transfers between devices, along(): lax.ppermute(value, axis, [(k, (k + d) % LINE) for k in range(LINE)])  12.5 us
    pallas_call x1, Pallas kernels, local(): plain(front_kernel, 'front', 1, [shaped((ROWS, WIDTH), BF16), shaped((CON...  11.4 us
    ppermute x3, starting transfers between devices, local(): shift_left = lambda value: lax.ppermute(value, 'x', left)  8.61 us
    pallas_call x1, Pallas kernels, local(): plain(attend_kernel, 'attend', 3, [shaped((ROWS, QHEADS * HEAD), BF16)],...  6.93 us
    pallas_call x1, Pallas kernels, local(): plain(state_kernel, 'state', 8, [shaped((ROWS, INNER), BF16), shaped((ROW...  6.81 us
    pallas_call x1, Pallas kernels, local(): pl.pallas_call(mixer_kernel, grid_spec=pltpu.PrefetchScalarGridSpec(num_s...  5.98 us
    ppermute x3, waiting for transfers between devices, local(): shift_right = lambda value: lax.ppermute(value, 'x', right)  5.88 us
    ppermute x3, waiting for transfers between devices, local(): shift_left = lambda value: lax.ppermute(value, 'x', left)  4.41 us
  transfers between devices with their start and end apart: 17, of which 8 were waited for; matrix products, arithmetic and copies ran while one was open for 0% of the time, Pallas kernels for 46%

profile of v1, /device:TPU:1, one launch (start us, length us, event | category | flops | bytes accessed | tf_op | source)
XLA Modules:
  0.0 89.6 jit_solution(6945558470684778340)
XLA Ops:
  0.0 1.4 %edge.1 = (bf16[128,2048]{1,0:T(8,128)(2,1)S(1)}, bf16[128,2048]{1,0:T(8,128)(2,1)S(1)}) custom-call(bf16[1024,2048]{1,0:T(8,128)(2,1)} %tok.3), custom_call_target="tpu_custom_call" | custom-call | flops 1000000 | bytes 8388608 | tf_op jit(solution)/shard_map/edge/pallas_call | solution.py:537
  1.4 4.1 %collective-permute-start = (bf16[128,2048]{1,0:T(8,128)(2,1)S(1)}, bf16[128,2048]{1,0:T(8,128)(2,1)S(1)}, u32[]{:S(2)}, u32[]{:S(2)}) collective-permute-start(bf16[128,2048]{1,0:T(8,128)(2,1)S(1)} %get-tuple-element.46), channel_id=1, source_target_pairs={{0,8},{8,16},{16,24},{24,32},{32,40},{40,48},{48,56},{56,64},{64,7... | collective-permute-start | bytes 1572872 | tf_op jit(solution)/shard_map/ppermute | solution.py:541
  5.4 1.3 %collective-permute-start.1 = (bf16[128,2048]{1,0:T(8,128)(2,1)S(1)}, bf16[128,2048]{1,0:T(8,128)(2,1)S(1)}, u32[]{:S(2)}, u32[]{:S(2)}) collective-permute-start(bf16[128,2048]{1,0:T(8,128)(2,1)S(1)} %get-tuple-element.47), channel_id=1, source_target_pairs={{8,0},{16,8},{24,16},{32,24},{40,32},{48,40},{56,48},{64,56},{72,6... | collective-permute-start | bytes 1572872 | tf_op jit(solution)/shard_map/ppermute | solution.py:542
  7.9 11.4 %front.1 = (bf16[1024,2048]{1,0:T(8,128)(2,1)S(1)}, f32[6,1024,128]{2,1,0:T(8,128)S(1)}, f32[16,1024]{1,0:T(8,128)S(1)}, bf16[1024,512]{1,0:T(8,128)(2,1)S(1)}, ...) custom-call(bf16[16,128]{1,0:T(8,128)(2,1)S(1)} %bitcast.13, ...), custom_call_target="tpu_custom_call" | custom-call | flops 10000000000 | bytes 8388608 | tf_op jit(solution)/shard_map/front/pallas_call | solution.py:550
  19.9 6.8 %state.1 = (bf16[1024,512]{1,0:T(8,128)(2,1)S(1)}, bf16[1024,128]{1,0:T(8,128)(2,1)S(1)}, bf16[1024,128]{1,0:T(8,128)(2,1)S(1)}, f32[16,1024]{1,0:T(8,128)S(1)},...) custom-call(f32[2,8]{1,0:T(2,128)S(1)} %copy-done.4, ...), custom_call_target="tpu_custom_call" | custom-call | flops 6000000000 | bytes 8388608 | tf_op jit(solution)/shard_map/state/pallas_call | solution.py:568
  26.7 2.2 %collective-permute-start.2 = (bf16[272,512]{1,0:T(8,128)(2,1)S(1)}, bf16[272,512]{1,0:T(8,128)(2,1)S(1)}, u32[]{:S(2)}, u32[]{:S(2)}) collective-permute-start(bf16[272,512]{1,0:T(8,128)(2,1)S(1)} %get-tuple-element.51.own), channel_id=1, source_target_pairs={{0,8},{8,16},{16,24},{24,0},{1,9},{9,17},{17,25},{25,1},{2,10},{10... | collective-permute-start | bytes 835592 | tf_op jit(solution)/shard_map/ppermute | solution.py:589
  28.9 4.1 %collective-permute-start.3 = (bf16[272,512]{1,0:T(8,128)(2,1)S(1)}, bf16[272,512]{1,0:T(8,128)(2,1)S(1)}, u32[]{:S(2)}, u32[]{:S(2)}) collective-permute-start(bf16[272,512]{1,0:T(8,128)(2,1)S(1)} %get-tuple-element.51.own), channel_id=1, source_target_pairs={{0,16},{8,24},{16,0},{24,8},{1,17},{9,25},{17,1},{25,9},{2,18},{10... | collective-permute-start | bytes 835592 | tf_op jit(solution)/shard_map/ppermute | solution.py:589
  33.0 6.0 %mixer.1.y_ref = f32[1024,512]{1,0:T(8,128)S(1)} custom-call(bf16[1024,512]{1,0:T(8,128)(2,1)S(1)} %get-tuple-element.56.x_ref, bf16[1024,128]{1,0:T(8,128)(2,1)S(1)} %get-tuple-element.57.b_ref, bf16[1024,128]{1,0:T(8,128)(2,1)S(1)} %get-tuple-element.58.c_ref, f32[16,1024]{1,0:T(8,128)S(1)} %get-tuple-element.59.cum_ref, ...), custom_call_target="tpu_custom_call" | custom-call | flops 10000000000 | bytes 8388608 | tf_op jit(solution)/shard_map/mixer/pallas_call | solution.py:626
  39.0 3.5 %heads.1 = (bf16[256,1024]{1,0:T(8,128)(2,1)S(1)}, bf16[64,1280]{1,0:T(8,128)(2,1)S(1)}, bf16[64,1280]{1,0:T(8,128)(2,1)S(1)}) custom-call(bf16[1024,2048]{1,0:T(8,128)(2,1)S(1)} %get-tuple-element.66.normed, bf16[128,2048]{1,0:T(8,128)(2,1)S(1)} %collective-permute-done.low, bf16[128,2048]{1,0:T(8,128)(2,1)S(1)} %collective-permute-done.1.high, ...), custom_call_target="tpu_custom_call" | custom-call | flops 5000000000 | bytes 8388608 | tf_op jit(solution)/shard_map/heads/pallas_call | solution.py:596
  42.5 1.4 %collective-permute-done.3.d2 = bf16[272,512]{1,0:T(8,128)(2,1)S(1)} collective-permute-done((bf16[272,512]{1,0:T(8,128)(2,1)S(1)}, bf16[272,512]{1,0:T(8,128)(2,1)S(1)}, u32[]{:S(2)}, u32[]{:S(2)}) %collective-permute-start.3) | collective-permute-done | bytes 278560 | tf_op jit(solution)/shard_map/ppermute | solution.py:589
  45.0 2.2 %collective-permute-start.5 = (bf16[144,512]{1,0:T(8,128)(2,1)S(1)}, bf16[144,512]{1,0:T(8,128)(2,1)S(1)}, u32[]{:S(2)}, u32[]{:S(2)}) collective-permute-start(bf16[144,512]{1,0:T(8,128)(2,1)S(1)} %get-tuple-element.53), channel_id=1, source_target_pairs={{0,32},{32,64},{64,96},{96,0},{1,33},{33,65},{65,97},{97,1},{2,34}... | collective-permute-start | bytes 442376 | tf_op jit(solution)/shard_map/ppermute | solution.py:589
  47.1 3.4 %collective-permute-start.6 = (bf16[144,512]{1,0:T(8,128)(2,1)S(1)}, bf16[144,512]{1,0:T(8,128)(2,1)S(1)}, u32[]{:S(2)}, u32[]{:S(2)}) collective-permute-start(bf16[144,512]{1,0:T(8,128)(2,1)S(1)} %get-tuple-element.54), channel_id=1, source_target_pairs={{0,64},{32,96},{64,0},{96,32},{1,65},{33,97},{65,1},{97,33},{2,66}... | collective-permute-start | bytes 442376 | tf_op jit(solution)/shard_map/ppermute | solution.py:589
  51.2 6.9 %attend.1.attn_ref = bf16[1024,256]{1,0:T(8,128)(2,1)S(1)} custom-call(f32[4]{0:T(128)S(1)} %copy-done.8, bf16[256,1024]{1,0:T(8,128)(2,1)S(1)} %get-tuple-element.69.qs, bf16[64,1280]{1,0:T(8,128)(2,1)S(1)} %get-tuple-element.70.ks, bf16[64,1280]{1,0:T(8,128)(2,1)S(1)} %get-tuple-element.71.vs), custom_call_target="tpu_custom_call" | custom-call | flops 7000000000 | bytes 8388608 | tf_op jit(solution)/shard_map/attend/pallas_call | solution.py:619
  58.1 3.2 %finish.1 = (bf16[4,128,768]{2,1,0:T(8,128)(2,1)S(1)}, bf16[4,128,768]{2,1,0:T(8,128)(2,1)S(1)}) custom-call(f32[272,512]{1,0:T(8,128)S(1)} %get-tuple-element.52.part, bf16[144,512]{1,0:T(8,128)(2,1)S(1)} %collective-permute-done.5.d1, bf16[144,512]{1,0:T(8,128)(2,1)S(1)} %collective-permute-done.6.d2, bf16[144,512]{1,0:T(8,128)(2,1)S(1)} %collective-permute-done.7.d3, ...), custom_call_target="tpu_custom_call" | custom-call | flops 4000000000 | bytes 8388608 | tf_op jit(solution)/shard_map/finish/pallas_call | solution.py:649
  61.4 2.5 %collective-permute-start.8 = (bf16[4,128,768]{2,1,0:T(8,128)(2,1)S(1)}, bf16[4,128,768]{2,1,0:T(8,128)(2,1)S(1)}, u32[]{:S(2)}, u32[]{:S(2)}) collective-permute-start(bf16[4,128,768]{2,1,0:T(8,128)(2,1)S(1)} %get-tuple-element.73), channel_id=1, source_target_pairs={{0,1},{1,0},{2,3},{3,2},{4,5},{5,4},{6,7},{7,6},{8,9},{9,8},{10,11... | collective-permute-start | bytes 2359304 | tf_op jit(solution)/shard_map/ppermute | solution.py:670
  63.8 1.9 %collective-permute-done.8.theirs = bf16[4,128,768]{2,1,0:T(8,128)(2,1)S(1)} collective-permute-done((bf16[4,128,768]{2,1,0:T(8,128)(2,1)S(1)}, bf16[4,128,768]{2,1,0:T(8,128)(2,1)S(1)}, u32[]{:S(2)}, u32[]{:S(2)}) %collective-permute-start.8) | collective-permute-done | bytes 786464 | tf_op jit(solution)/shard_map/ppermute | solution.py:670
  66.7 2.5 %collective-permute-start.15 = (bf16[64,2048]{1,0:T(8,128)(2,1)S(1)}, bf16[64,2048]{1,0:T(8,128)(2,1)S(1)}, u32[]{:S(2)}, u32[]{:S(2)}) collective-permute-start(bf16[64,2048]{1,0:T(8,128)(2,1)S(1)} %get-tuple-element.82), channel_id=1, source_target_pairs={{2,0},{4,2},{6,4},{0,6},{3,1},{5,3},{7,5},{1,7},{10,8},{12,10},{14... | collective-permute-start | bytes 786440 | tf_op jit(solution)/shard_map/ppermute | solution.py:679
  69.3 2.7 %beside.1 = (bf16[64,2048]{1,0:T(8,128)(2,1)S(1)}, bf16[64,2048]{1,0:T(8,128)(2,1)S(1)}, f32[64,2048]{1,0:T(8,128)S(1)}, f32[64,2048]{1,0:T(8,128)S(1)}, f32[128,2048]{1,0:T(8,128)S(1)}) custom-call(bf16[4,128,768]{2,1,0:T(8,128)(2,1)S(1)} %get-tuple-element.72.mine, bf16[4,128,768]{2,1,0:T(8,128)(2,1)S(1)} %collective-permute-done.8.theirs, ...), custom_call_target="tpu_custom_call" | custom-call | flops 3000000000 | bytes 8388608 | tf_op jit(solution)/shard_map/beside/pallas_call | solution.py:685
  72.0 2.7 %collective-permute-start.11 = (bf16[64,2048]{1,0:T(8,128)(2,1)S(1)}, bf16[64,2048]{1,0:T(8,128)(2,1)S(1)}, u32[]{:S(2)}, u32[]{:S(2)}) collective-permute-start(bf16[64,2048]{1,0:T(8,128)(2,1)S(1)} %get-tuple-element.77), channel_id=1, source_target_pairs={{2,0},{4,2},{6,4},{0,6},{3,1},{5,3},{7,5},{1,7},{10,8},{12,10},{14... | collective-permute-start | bytes 786440 | tf_op jit(solution)/shard_map/ppermute | solution.py:679
  74.8 3.3 %collective-permute-start.16 = (bf16[64,2048]{1,0:T(8,128)(2,1)S(1)}, bf16[64,2048]{1,0:T(8,128)(2,1)S(1)}, u32[]{:S(2)}, u32[]{:S(2)}) collective-permute-start(bf16[64,2048]{1,0:T(8,128)(2,1)S(1)} %add_convert_fusion.1), channel_id=1, source_target_pairs={{2,0},{4,2},{6,4},{0,6},{3,1},{5,3},{7,5},{1,7},{10,8},{12,10},{14... | collective-permute-start | bytes 786440 | tf_op jit(solution)/shard_map/ppermute | solution.py:679
  78.3 1.7 %collective-permute-done.11 = bf16[64,2048]{1,0:T(8,128)(2,1)S(1)} collective-permute-done((bf16[64,2048]{1,0:T(8,128)(2,1)S(1)}, bf16[64,2048]{1,0:T(8,128)(2,1)S(1)}, u32[]{:S(2)}, u32[]{:S(2)}) %collective-permute-start.11) | collective-permute-done | bytes 262176 | tf_op jit(solution)/shard_map/ppermute | solution.py:679
  80.0 2.9 %collective-permute-done.14 = bf16[64,2048]{1,0:T(8,128)(2,1)S(1)} collective-permute-done((bf16[64,2048]{1,0:T(8,128)(2,1)S(1)}, bf16[64,2048]{1,0:T(8,128)(2,1)S(1)}, u32[]{:S(2)}, u32[]{:S(2)}) %collective-permute-start.14) | collective-permute-done | bytes 262176 | tf_op jit(solution)/shard_map/ppermute | solution.py:678
  82.9 2.7 %collective-permute-done.16 = bf16[64,2048]{1,0:T(8,128)(2,1)S(1)} collective-permute-done((bf16[64,2048]{1,0:T(8,128)(2,1)S(1)}, bf16[64,2048]{1,0:T(8,128)(2,1)S(1)}, u32[]{:S(2)}, u32[]{:S(2)}) %collective-permute-start.16) | collective-permute-done | bytes 262176 | tf_op jit(solution)/shard_map/ppermute | solution.py:679
  85.6 2.9 %collective-permute-done.13 = bf16[64,2048]{1,0:T(8,128)(2,1)S(1)} collective-permute-done((bf16[64,2048]{1,0:T(8,128)(2,1)S(1)}, bf16[64,2048]{1,0:T(8,128)(2,1)S(1)}, u32[]{:S(2)}, u32[]{:S(2)}) %collective-permute-start.13) | collective-permute-done | bytes 262176 | tf_op jit(solution)/shard_map/ppermute | solution.py:678
  (52 shorter events, 5.7 us)
Async XLA Ops:
  0.0 7.9 %copy-start.2 = (bf16[2048]{0:T(1024)(128)(2,1)S(1)}, bf16[2048]{0:T(1024)(128)(2,1)}, u32[]{:S(2)}) copy-start(bf16[2048]{0:T(1024)(128)(2,1)} %param.24) | copy-start | bytes 12292
  1.4 18.0 %collective-permute-start = (bf16[128,2048]{1,0:T(8,128)(2,1)S(1)}, bf16[128,2048]{1,0:T(8,128)(2,1)S(1)}, u32[]{:S(2)}, u32[]{:S(2)}) collective-permute-start(bf16[128,2048]{1,0:T(8,128)(2,1)S(1)} %get-tuple-element.46), channel_id=1, source_target_pairs={{0,8},{8,16},{16,24},{24,32},{32,40},{40,48},{48,56},{56,64},{64,7... | collective-permute-start | bytes 1572872 | tf_op jit(solution)/shard_map/ppermute | solution.py:541
  5.4 14.4 %collective-permute-start.1 = (bf16[128,2048]{1,0:T(8,128)(2,1)S(1)}, bf16[128,2048]{1,0:T(8,128)(2,1)S(1)}, u32[]{:S(2)}, u32[]{:S(2)}) collective-permute-start(bf16[128,2048]{1,0:T(8,128)(2,1)S(1)} %get-tuple-element.47), channel_id=1, source_target_pairs={{8,0},{16,8},{24,16},{32,24},{40,32},{48,40},{56,48},{64,56},{72,6... | collective-permute-start | bytes 1572872 | tf_op jit(solution)/shard_map/ppermute | solution.py:542
  6.8 59.0 %collective-permute-start.10 = (bf16[512,2048]{1,0:T(8,128)(2,1)S(1)}, bf16[512,2048]{1,0:T(8,128)(2,1)S(1)}, u32[]{:S(2)}, u32[]{:S(2)}) collective-permute-start(bf16[512,2048]{1,0:T(8,128)(2,1)S(1)} %copy-done.12), channel_id=1, source_target_pairs={{0,1},{1,0},{2,3},{3,2},{4,5},{5,4},{6,7},{7,6},{8,9},{9,8},{10,11... | collective-permute-start | bytes 6291464 | tf_op jit(solution)/shard_map/ppermute | solution.py:544
  7.8 56.0 %collective-permute-start.9 = (bf16[256,2048]{1,0:T(8,128)(2,1)S(1)}, bf16[256,2048]{1,0:T(8,128)(2,1)S(1)}, u32[]{:S(2)}, u32[]{:S(2)}) collective-permute-start(bf16[256,2048]{1,0:T(8,128)(2,1)S(1)} %copy-done.13), channel_id=1, source_target_pairs={{0,1},{1,0},{2,3},{3,2},{4,5},{5,4},{6,7},{7,6},{8,9},{9,8},{10,11... | collective-permute-start | bytes 3145736 | tf_op jit(solution)/shard_map/ppermute | solution.py:543
  7.9 12.0 %copy-start = (f32[1024,2,8]{0,2,1:T(8,128)S(1)}, f32[1024,2,8]{0,2,1:T(8,128)}, u32[]{:S(2)}) copy-start(f32[1024,2,8]{0,2,1:T(8,128)} %param.39) | copy-start | bytes 196612
  7.9 12.0 %copy-start.1 = (bf16[5,512]{1,0:T(8,128)(2,1)S(1)}, bf16[5,512]{1,0:T(8,128)(2,1)}, u32[]{:S(2)}) copy-start(bf16[5,512]{1,0:T(8,128)(2,1)} %h_inner_taps.1) | copy-start | bytes 15364
  7.9 12.0 %copy-start.3 = (bf16[5,2,128]{2,1,0:T(2,128)(2,1)S(1)}, bf16[5,2,128]{2,1,0:T(2,128)(2,1)}, u32[]{:S(2)}) copy-start(bf16[5,2,128]{2,1,0:T(2,128)(2,1)} %h_pair_taps.1) | copy-start | bytes 7684
  7.9 12.0 %copy-start.4 = (f32[2,8]{1,0:T(2,128)S(1)}, f32[2,8]{1,0:T(2,128)}, u32[]{:S(2)}) copy-start(f32[2,8]{1,0:T(2,128)} %rate.1) | copy-start | bytes 196
  7.9 12.0 %copy-start.10 = (bf16[16,512]{1,0:T(8,128)(2,1)S(1)}, bf16[16,512]{1,0:T(8,128)(2,1)}, u32[]{:S(2)}) copy-start(bf16[16,512]{1,0:T(8,128)(2,1)} %constant.6.clone.h_spread) | copy-start | bytes 49156
  26.7 15.8 %collective-permute-start.2 = (bf16[272,512]{1,0:T(8,128)(2,1)S(1)}, bf16[272,512]{1,0:T(8,128)(2,1)S(1)}, u32[]{:S(2)}, u32[]{:S(2)}) collective-permute-start(bf16[272,512]{1,0:T(8,128)(2,1)S(1)} %get-tuple-element.51.own), channel_id=1, source_target_pairs={{0,8},{8,16},{16,24},{24,0},{1,9},{9,17},{17,25},{25,1},{2,10},{10... | collective-permute-start | bytes 835592 | tf_op jit(solution)/shard_map/ppermute | solution.py:589
  28.9 15.0 %collective-permute-start.3 = (bf16[272,512]{1,0:T(8,128)(2,1)S(1)}, bf16[272,512]{1,0:T(8,128)(2,1)S(1)}, u32[]{:S(2)}, u32[]{:S(2)}) collective-permute-start(bf16[272,512]{1,0:T(8,128)(2,1)S(1)} %get-tuple-element.51.own), channel_id=1, source_target_pairs={{0,16},{8,24},{16,0},{24,8},{1,17},{9,25},{17,1},{25,9},{2,18},{10... | collective-permute-start | bytes 835592 | tf_op jit(solution)/shard_map/ppermute | solution.py:589
  33.0 11.6 %collective-permute-start.4 = (bf16[272,512]{1,0:T(8,128)(2,1)S(1)}, bf16[272,512]{1,0:T(8,128)(2,1)S(1)}, u32[]{:S(2)}, u32[]{:S(2)}) collective-permute-start(bf16[272,512]{1,0:T(8,128)(2,1)S(1)} %get-tuple-element.51.own), channel_id=1, source_target_pairs={{0,24},{8,0},{16,8},{24,16},{1,25},{9,1},{17,9},{25,17},{2,26},{10... | collective-permute-start | bytes 835592 | tf_op jit(solution)/shard_map/ppermute | solution.py:589
  42.5 8.7 %copy-start.8 = (f32[4]{0:T(128)S(1)}, f32[4]{0:T(128)}, u32[]{:S(2)}) copy-start(f32[4]{0:T(128)} %sink.1) | copy-start | bytes 52
  45.0 13.1 %collective-permute-start.5 = (bf16[144,512]{1,0:T(8,128)(2,1)S(1)}, bf16[144,512]{1,0:T(8,128)(2,1)S(1)}, u32[]{:S(2)}, u32[]{:S(2)}) collective-permute-start(bf16[144,512]{1,0:T(8,128)(2,1)S(1)} %get-tuple-element.53), channel_id=1, source_target_pairs={{0,32},{32,64},{64,96},{96,0},{1,33},{33,65},{65,97},{97,1},{2,34}... | collective-permute-start | bytes 442376 | tf_op jit(solution)/shard_map/ppermute | solution.py:589
  47.1 11.0 %collective-permute-start.6 = (bf16[144,512]{1,0:T(8,128)(2,1)S(1)}, bf16[144,512]{1,0:T(8,128)(2,1)S(1)}, u32[]{:S(2)}, u32[]{:S(2)}) collective-permute-start(bf16[144,512]{1,0:T(8,128)(2,1)S(1)} %get-tuple-element.54), channel_id=1, source_target_pairs={{0,64},{32,96},{64,0},{96,32},{1,65},{33,97},{65,1},{97,33},{2,66}... | collective-permute-start | bytes 442376 | tf_op jit(solution)/shard_map/ppermute | solution.py:589
  50.5 7.7 %collective-permute-start.7 = (bf16[144,512]{1,0:T(8,128)(2,1)S(1)}, bf16[144,512]{1,0:T(8,128)(2,1)S(1)}, u32[]{:S(2)}, u32[]{:S(2)}) collective-permute-start(bf16[144,512]{1,0:T(8,128)(2,1)S(1)} %get-tuple-element.55), channel_id=1, source_target_pairs={{0,96},{32,0},{64,32},{96,64},{1,97},{33,1},{65,33},{97,65},{2,98}... | collective-permute-start | bytes 442376 | tf_op jit(solution)/shard_map/ppermute | solution.py:589
  61.4 4.4 %collective-permute-start.8 = (bf16[4,128,768]{2,1,0:T(8,128)(2,1)S(1)}, bf16[4,128,768]{2,1,0:T(8,128)(2,1)S(1)}, u32[]{:S(2)}, u32[]{:S(2)}) collective-permute-start(bf16[4,128,768]{2,1,0:T(8,128)(2,1)S(1)} %get-tuple-element.73), channel_id=1, source_target_pairs={{0,1},{1,0},{2,3},{3,2},{4,5},{5,4},{6,7},{7,6},{8,9},{9,8},{10,11... | collective-permute-start | bytes 2359304 | tf_op jit(solution)/shard_map/ppermute | solution.py:670
  66.7 8.0 %collective-permute-start.15 = (bf16[64,2048]{1,0:T(8,128)(2,1)S(1)}, bf16[64,2048]{1,0:T(8,128)(2,1)S(1)}, u32[]{:S(2)}, u32[]{:S(2)}) collective-permute-start(bf16[64,2048]{1,0:T(8,128)(2,1)S(1)} %get-tuple-element.82), channel_id=1, source_target_pairs={{2,0},{4,2},{6,4},{0,6},{3,1},{5,3},{7,5},{1,7},{10,8},{12,10},{14... | collective-permute-start | bytes 786440 | tf_op jit(solution)/shard_map/ppermute | solution.py:679
  69.3 8.8 %collective-permute-start.12 = (bf16[64,2048]{1,0:T(8,128)(2,1)S(1)}, bf16[64,2048]{1,0:T(8,128)(2,1)S(1)}, u32[]{:S(2)}, u32[]{:S(2)}) collective-permute-start(bf16[64,2048]{1,0:T(8,128)(2,1)S(1)} %get-tuple-element.79), channel_id=1, source_target_pairs={{0,2},{2,4},{4,6},{6,0},{1,3},{3,5},{5,7},{7,1},{8,10},{10,12},{12... | collective-permute-start | bytes 786440 | tf_op jit(solution)/shard_map/ppermute | solution.py:678
  72.0 8.0 %collective-permute-start.11 = (bf16[64,2048]{1,0:T(8,128)(2,1)S(1)}, bf16[64,2048]{1,0:T(8,128)(2,1)S(1)}, u32[]{:S(2)}, u32[]{:S(2)}) collective-permute-start(bf16[64,2048]{1,0:T(8,128)(2,1)S(1)} %get-tuple-element.77), channel_id=1, source_target_pairs={{2,0},{4,2},{6,4},{0,6},{3,1},{5,3},{7,5},{1,7},{10,8},{12,10},{14... | collective-permute-start | bytes 786440 | tf_op jit(solution)/shard_map/ppermute | solution.py:679
  74.7 8.2 %collective-permute-start.14 = (bf16[64,2048]{1,0:T(8,128)(2,1)S(1)}, bf16[64,2048]{1,0:T(8,128)(2,1)S(1)}, u32[]{:S(2)}, u32[]{:S(2)}) collective-permute-start(bf16[64,2048]{1,0:T(8,128)(2,1)S(1)} %get-tuple-element.80), channel_id=1, source_target_pairs={{0,2},{2,4},{4,6},{6,0},{1,3},{3,5},{5,7},{7,1},{8,10},{10,12},{12... | collective-permute-start | bytes 786440 | tf_op jit(solution)/shard_map/ppermute | solution.py:678
  74.8 10.8 %collective-permute-start.16 = (bf16[64,2048]{1,0:T(8,128)(2,1)S(1)}, bf16[64,2048]{1,0:T(8,128)(2,1)S(1)}, u32[]{:S(2)}, u32[]{:S(2)}) collective-permute-start(bf16[64,2048]{1,0:T(8,128)(2,1)S(1)} %add_convert_fusion.1), channel_id=1, source_target_pairs={{2,0},{4,2},{6,4},{0,6},{3,1},{5,3},{7,5},{1,7},{10,8},{12,10},{14... | collective-permute-start | bytes 786440 | tf_op jit(solution)/shard_map/ppermute | solution.py:679
  78.2 10.4 %collective-permute-start.13 = (bf16[64,2048]{1,0:T(8,128)(2,1)S(1)}, bf16[64,2048]{1,0:T(8,128)(2,1)S(1)}, u32[]{:S(2)}, u32[]{:S(2)}) collective-permute-start(bf16[64,2048]{1,0:T(8,128)(2,1)S(1)} %add_convert_fusion.3), channel_id=1, source_target_pairs={{0,2},{2,4},{4,6},{6,0},{1,3},{3,5},{5,7},{7,1},{8,10},{10,12},{12... | collective-permute-start | bytes 786440 | tf_op jit(solution)/shard_map/ppermute | solution.py:678
  (7 other events, 45.6 us)

commit v2 on v1

v2 whole, which is shorter than its diff:
```python
import jax
import jax.numpy as jnp
import numpy as np
from jax import lax
from jax.experimental import pallas as pl
from jax.experimental.pallas import tpu as pltpu
from jax.sharding import Mesh
from jax.sharding import PartitionSpec as P

SP = ("z", "y")
SP_TP = ("z", "y", "x", "c")
ROWS = 1024
WIDTH = 2048
SEQ = 16384
HEADS = 8
STATE = 128
INNER = 512
CONV = INNER + 2 * STATE
CHUNK = 128
CHUNKS = ROWS // CHUNK
EDGE = 16
WINDOW = 128
HEAD = 64
HALF = 32
QHEADS = 4
LINE = 4
PACK = 2 * STATE + 16

NORM_EPS = 1e-05
ROPE_BASE = 500000.0
NEG_FILL = -1e30
F32 = jnp.float32
BF16 = jnp.bfloat16


def rope_tables():
    frequency = ROPE_BASE ** (-np.arange(0, HEAD, 2, dtype=np.float64) / HEAD)
    offsets = np.arange(-WINDOW, ROWS + WINDOW, dtype=np.float64)
    near = frequency[:, None] * offsets[None, :]
    far = frequency[None, :] * (ROWS * np.arange(SEQ // ROWS, dtype=np.float64))[:, None]
    near_table = np.concatenate([np.cos(near), np.sin(near)], axis=0).astype(np.float32)
    far_table = np.concatenate([np.cos(far), np.sin(far)], axis=1).astype(np.float32)
    return near_table, far_table[:, None, :]


def head_spread():
    spread = np.repeat(np.eye(HEADS, dtype=np.float32), INNER // HEADS, axis=1)
    return np.concatenate([spread, spread], axis=0)


def dot(a, b):
    return jnp.dot(a, b, preferred_element_type=F32)


def dot_nt(a, b):
    return lax.dot_general(a, b, (((1,), (1,)), ((), ())), preferred_element_type=F32)


def dot_tn(a, b):
    return lax.dot_general(a, b, (((0,), (0,)), ((), ())), preferred_element_type=F32)


def silu(v):
    half = 0.5 * v
    return half + half * jnp.tanh(half)


def normalise(tokens, gain):
    t = tokens.astype(F32)
    mean = jnp.mean(t * t, axis=-1, keepdims=True)
    return (t * lax.rsqrt(mean + NORM_EPS) * gain).astype(BF16)


def lane_row(ref):
    value = ref[...].astype(F32)
    return jnp.concatenate([value[k : k + 1] for k in range(value.shape[0])], axis=1)


def column(row):
    size = row.shape[1]
    a = lax.broadcasted_iota(jnp.int32, (size, size), 0)
    b = lax.broadcasted_iota(jnp.int32, (size, size), 1)
    return jnp.sum(jnp.where(a == b, row, 0.0), axis=1, keepdims=True)


def fetch(pairs, sems):
    copies = [pltpu.make_async_copy(a, b, sems.at[k]) for k, (a, b) in enumerate(pairs)]
    for copy in copies:
        copy.start()
    return copies


def widen(rows, spread):
    high = rows.astype(BF16)
    low = (rows - high.astype(F32)).astype(BF16)
    return dot_tn(jnp.concatenate([high, low], axis=0), spread)


def edge_kernel(h_gain, tok, h_k, h_v, low, high, edge, w_kv, gain, sems):
    copies = fetch(
        [
            (tok.at[pl.ds(ROWS - WINDOW, WINDOW)], edge.at[pl.ds(0, WINDOW)]),
            (tok.at[pl.ds(0, WINDOW)], edge.at[pl.ds(WINDOW, WINDOW)]),
            (h_k, w_kv.at[pl.ds(0, HEAD)]), (h_v, w_kv.at[pl.ds(HEAD, HEAD)]), (h_gain, gain),
        ],
        sems,
    )
    for copy in copies:
        copy.wait()
    g = lane_row(gain)
    kv = dot_nt(w_kv[...], normalise(edge[...], g)).astype(BF16)
    for ref, at, rows in ((low, 0, WINDOW - EDGE), (high, WINDOW, WINDOW)):
        ref[:EDGE, :] = edge[rows : rows + EDGE, :]
        for k in range(WIDTH // 128):
            ref[EDGE:, k * 128 : (k + 1) * 128] = kv[k * 8 : (k + 1) * 8, at : at + WINDOW]


BLOCK = 256


def front_kernel(
    gain, w_inner, w_in, w_out, tok, h_step, h_gate, h_q, h_k, h_v,
    normed, rows, raw, w_gate, w_q, w_kv, w_step, sems,
):
    blocks = [pl.ds(k * BLOCK, BLOCK) for k in range(ROWS // BLOCK)]
    waits = fetch(
        [(h_step, w_step)], sems
    )
    late = [
        pltpu.make_async_copy(a, b, sems.at[5 + k])
        for k, (a, b) in enumerate(
            [
                (h_gate, w_gate), (h_q, w_q), (h_k, w_kv.at[pl.ds(0, HEAD)]),
                (h_v, w_kv.at[pl.ds(HEAD, HEAD)]),
            ]
        )
    ]
    g = lane_row(gain)

    def prepare(i):
        normed[blocks[i], :] = normalise(tok[blocks[i], :], g)

    prepare(0)
    waits[0].wait()
    pair = jnp.concatenate([w_in[...], w_out[...]], axis=1)
    for i, block in enumerate(blocks):
        if i + 1 < len(blocks):
            prepare(i + 1)
        if i == 1:
            for copy in late:
                copy.start()
        n = normed[block, :]
        for k in range(0, INNER, 2 * STATE):
            value = dot(n, w_inner[:, k : k + 2 * STATE]).astype(BF16).astype(F32)
            rows[k // STATE, block, :] = value[:, :STATE]
            rows[k // STATE + 1, block, :] = value[:, STATE:]
        value = dot(n, pair).astype(BF16).astype(F32)
        rows[INNER // STATE, block, :] = value[:, :STATE]
        rows[INNER // STATE + 1, block, :] = value[:, STATE:]
        raw[:, block] = dot_nt(w_step[...], n).astype(BF16).astype(F32)
    for copy in late:
        copy.wait()


def state_kernel(
    rate, rows, raw, low, high, gain, w_inner, w_in, w_out, h_inner_taps, h_pair_taps, h_jump, h_spread,
    x_ref, b_ref, c_ref, cum_ref, step_ref, run_ref, enter_ref, back_ref, state_ref, spread,
    first, last, state_f, state_b, jump, inner_taps, pair_taps, sems,
):
    copies = fetch(
        [(h_jump, jump), (h_spread, spread), (h_inner_taps, inner_taps), (h_pair_taps, pair_taps)], sems
    )
    g = lane_row(gain)
    edge = normalise(jnp.concatenate([low[:EDGE, :], high[:EDGE, :]], axis=0), g)
    for k in range(CONV // STATE):
        if k < INNER // STATE:
            w = w_inner[:, k * STATE : (k + 1) * STATE]
        else:
            w = (w_in if k == INNER // STATE else w_out)[...]
        value = dot(edge, w).astype(BF16).astype(F32)
        first[k, :EDGE, :] = value[:EDGE]
        first[k, EDGE:, :] = rows[k, : CHUNK + EDGE, :]
        last[k, : CHUNK + EDGE, :] = rows[k, ROWS - CHUNK - EDGE :, :]
        last[k, CHUNK + EDGE :, :] = value[EDGE:]
    for copy in copies:
        copy.wait()
    taps = jnp.concatenate(
        [inner_taps[...].astype(F32)] + [pair_taps[:, k, :].astype(F32) for k in (0, 1)], axis=1
    )
    rates = [
        jnp.concatenate([jnp.full((1, CHUNK), rate[d, h], F32) for h in range(HEADS)], axis=0)
        for d in (0, 1)
    ]
    v = raw[...]
    step = jnp.maximum(v, 0.0) + jnp.log1p(jnp.exp(-jnp.abs(v)))
    step_ref[...] = step
    lane = lax.broadcasted_iota(jnp.int32, (HEADS, CHUNK), 1)
    cums = []
    for k in range(CHUNKS):
        at = slice(k * CHUNK, (k + 1) * CHUNK)
        f = jump[:HEADS, at] - rates[0] * step[:HEADS, at]
        r = jump[HEADS:, at] - rates[1] * step[HEADS:, at]
        for shift in (1, 2, 4, 8, 16, 32, 64):
            f = f + jnp.where(lane >= shift, pltpu.roll(f, shift, 1), 0.0)
            r = r + jnp.where(lane < CHUNK - shift, pltpu.roll(r, CHUNK - shift, 1), 0.0)
        cums.append((f, r))
        cum_ref[:HEADS, k * CHUNK : (k + 1) * CHUNK] = f
        cum_ref[HEADS:, k * CHUNK : (k + 1) * CHUNK] = r
    totals = [(f[:, CHUNK - 1 :], r[:, :1]) for f, r in cums]
    zero = jnp.zeros((HEADS, 1), F32)
    ahead = zero
    for k in range(CHUNKS):
        run_ref[:HEADS, k * CHUNK : (k + 1) * CHUNK] = cums[k][0] + ahead
        ahead = ahead + totals[k][0]
    behind = zero
    for k in reversed(range(CHUNKS)):
        run_ref[HEADS:, k * CHUNK : (k + 1) * CHUNK] = cums[k][1] + behind
        behind = behind + totals[k][1]
    sp = spread[...]
    state_f[...] = jnp.zeros_like(state_f)
    state_b[...] = jnp.zeros_like(state_b)
    passed = zero
    for k in range(CHUNKS):
        if k == 0:
            source, base = first, EDGE - 2
        elif k == CHUNKS - 1:
            source, base = last, EDGE - 2
        else:
            source, base = rows, k * CHUNK - 2
        here = slice(k * CHUNK, (k + 1) * CHUNK)

        def active(tile):
            cols = slice(tile * STATE, (tile + 1) * STATE)
            acc = source[tile, base : base + CHUNK, :] * taps[0:1, cols]
            for t in range(1, 5):
                acc = acc + source[tile, base + t : base + t + CHUNK, :] * taps[t : t + 1, cols]
            return silu(acc)

        f, r = cums[k]
        tf, tr = totals[k]
        wf = jnp.exp(tf - f) * step[:HEADS, here]
        wr = jnp.exp(tr - r) * step[HEADS:, here]
        df = jnp.where(lane == 0, jnp.exp(tf), jnp.exp(passed))
        bm = active(INNER // STATE).astype(BF16)
        b_ref[here, :] = bm
        c_ref[here, :] = active(INNER // STATE + 1).astype(BF16)
        xf = jnp.concatenate([active(tile) for tile in range(INNER // STATE)], axis=1)
        x_ref[here, :] = xf.astype(BF16)
        wide = widen(jnp.concatenate([wf, wr, df], axis=1), sp)
        fresh_f = dot_tn(bm, (xf * wide[:CHUNK]).astype(BF16))
        fresh_b = dot_tn(bm, (xf * wide[CHUNK : 2 * CHUNK]).astype(BF16))
        enter_ref[k] = state_f[...].astype(BF16)
        back_ref[k] = fresh_b.astype(BF16)
        state_f[...] = state_f[...] * wide[2 * CHUNK : 2 * CHUNK + 1] + fresh_f
        state_b[...] = state_b[...] + fresh_b * wide[2 * CHUNK + 1 : 2 * CHUNK + 2]
        passed = passed + tr
    state_ref[:STATE, :] = state_f[...].astype(BF16)
    state_ref[STATE : 2 * STATE, :] = state_b[...].astype(BF16)
    parts = jnp.zeros((HEADS, CHUNK), F32)
    column = 0
    for total in (ahead, passed):
        rest = total
        for _ in range(3):
            piece = rest.astype(BF16).astype(F32)
            rest = rest - piece
            parts = jnp.where(lane == column, piece, parts)
            column += 1
    state_ref[2 * STATE :, :] = dot_tn(parts.astype(BF16), sp[:HEADS]).astype(BF16)[:16]


def logs_of(ref):
    tail = ref[2 * STATE :, :].astype(F32)
    return tail[0:1] + tail[1:2] + tail[2:3], tail[3:4] + tail[4:5] + tail[5:6]


def line_kernel(own, d1, d2, d3, m1, m2, m3, part_ref):
    place, level = lax.axis_index("y"), lax.axis_index("z")
    got = (own, d1, d2, d3)
    logs = [logs_of(r) for r in got]
    state = lambda r, back: r[STATE * back : STATE * (back + 1), :].astype(F32)
    totals = []
    for back in (0, 1):
        near = (lambda d: d) if back == 0 else (lambda d: LINE - d)
        count = place if back == 0 else LINE - 1 - place
        far_count = LINE - 1 - count
        prefix = jnp.zeros((STATE, INNER), F32)
        log_prefix = jnp.zeros((1, INNER), F32)
        for d in range(1, LINE):
            r = near(d)
            live = d <= count
            weight = jnp.where(live, jnp.exp(log_prefix), 0.0)
            prefix = prefix + weight * state(got[r], back)
            log_prefix = log_prefix + jnp.where(live, logs[r][back], 0.0)
        total = jnp.zeros((STATE, INNER), F32)
        suffix = jnp.zeros((1, INNER), F32)
        for e in reversed(range(1, LINE)):
            r = near(LINE - e)
            live = e <= far_count
            weight = jnp.where(live, jnp.exp(suffix), 0.0)
            total = total + weight * state(got[r], back)
            suffix = suffix + jnp.where(live, logs[r][back], 0.0)
        total = total + jnp.exp(suffix) * state(own, back)
        suffix = suffix + logs[0][back]
        total = total + jnp.exp(suffix) * prefix
        part_ref[STATE * back : STATE * (back + 1), :] = prefix
        part_ref[2 * STATE + back : 2 * STATE + back + 1, :] = log_prefix
        rest = suffix + log_prefix
        pieces = []
        for _ in range(3):
            piece = rest.astype(BF16).astype(F32)
            rest = rest - piece
            pieces.append(piece)
        pieces.append(jnp.zeros((13, INNER), F32))
        totals.append((total.astype(BF16), jnp.concatenate(pieces, axis=0).astype(BF16)))
    for d, ref in ((1, m1), (2, m2), (3, m3)):
        for back in (0, 1):

            @pl.when(level + d < LINE if back == 0 else level + d >= LINE)
            def _(ref=ref, back=back):
                ref[:STATE, :] = totals[back][0]
                ref[STATE:, :] = totals[back][1]


def heads_kernel(
    normed, low, high, w_gate, w_q, w_kv, q_row, k_row, h_near, h_far, gate, qs, ks, vs, near, far, sems
):
    copies = fetch([(h_near, near), (h_far.at[lax.axis_index(SP)], far)], sems)
    q_gain, k_gain = column(q_row[...]), column(k_row[...])
    for copy in copies:
        copy.wait()
    turns = column(far[...])
    far_cos = turns[:HALF, :]
    far_sin = turns[HALF:, :]
    scale = jnp.asarray(HEAD**-0.5, BF16)

    def turn(head, at, size):
        co = near[:HALF, at : at + size]
        so = near[HALF:, at : at + size]
        cos = far_cos * co - far_sin * so
        sin = far_sin * co + far_cos * so
        u, w = head[:HALF], head[HALF:]
        return jnp.concatenate([u * cos - w * sin, w * cos + u * sin], axis=0)

    def head_norm(head, scale):
        mean = jnp.mean(head * head, axis=0, keepdims=True)
        return head * lax.rsqrt(mean + NORM_EPS) * scale

    def keys_values(kv, at, size):
        k = head_norm(kv[:HEAD].astype(F32), k_gain)
        ks[:, at : at + size] = turn(k, at, size).astype(BF16)
        vs[:, at : at + size] = kv[HEAD:]

    for i in range(4):
        at = WINDOW + i * 256
        n = normed[i * 256 : (i + 1) * 256, :]
        keys_values(dot_nt(w_kv[...], n).astype(BF16), at, 256)
        gate[i * 256 : (i + 1) * 256, :] = dot(n, w_gate[...]).astype(BF16)
        q = dot(n, w_q[...]).astype(BF16).astype(F32).T
        for h in range(QHEADS):
            head = turn(head_norm(q[h * HEAD : (h + 1) * HEAD], q_gain), at, 256)
            qs[h * HEAD : (h + 1) * HEAD, i * 256 : (i + 1) * 256] = head.astype(BF16) * scale
    for ref, at in ((low, 0), (high, WINDOW + ROWS)):
        tiles = [ref[EDGE:, k * 128 : (k + 1) * 128] for k in range(WIDTH // 128)]
        keys_values(jnp.concatenate(tiles, axis=0), at, WINDOW)


def attend_kernel(sink, qs, ks, vs, attn_ref, even_mask, odd_mask, even, odd):
    reach = 3 * WINDOW
    pairs = ROWS // WINDOW // 2
    jj = lax.broadcasted_iota(jnp.int32, (reach, WINDOW), 0)
    ii = lax.broadcasted_iota(jnp.int32, (reach, WINDOW), 1)
    band = (jj >= ii) & (jj <= ii + 2 * WINDOW)
    first = lax.axis_index(SP) * ROWS - WINDOW

    def set_mask(mask, j):
        position = jj + (first + j * WINDOW)
        mask[...] = jnp.where(band & (position >= 0) & (position < SEQ), 0.0, NEG_FILL)

    def scores(j, out):
        here = pl.multiple_of(j * WINDOW, 128)
        qb = jnp.concatenate(
            [qs[h * HEAD : (h + 1) * HEAD, pl.ds(here, WINDOW)] for h in range(QHEADS)], axis=1
        )
        out[...] = dot_tn(ks[:, pl.ds(here, reach)], qb)

    def outputs(j, mask, saved):
        here = pl.multiple_of(j * WINDOW, 128)
        weights = []
        for h in range(QHEADS):
            s = saved[:, h * WINDOW : (h + 1) * WINDOW] + mask[...]
            top = jnp.maximum(jnp.max(s, axis=0, keepdims=True), sink[h])
            p = jnp.exp(s - top)
            scale = 1.0 / (jnp.sum(p, axis=0, keepdims=True) + jnp.exp(sink[h] - top))
            weights.append((p * scale).astype(BF16))
        o = dot(vs[:, pl.ds(here, reach)], jnp.concatenate(weights, axis=1))
        o = jnp.concatenate([o[:, h * WINDOW : (h + 1) * WINDOW] for h in range(QHEADS)], axis=0)
        attn_ref[pl.ds(here, WINDOW), :] = o.T.astype(BF16)

    set_mask(even_mask, 0)
    set_mask(odd_mask, 1)
    scores(0, even)

    def pair(i, _):
        @pl.when(i == 1)
        def _():
            set_mask(even_mask, 2)

        @pl.when(i == pairs - 1)
        def _():
            set_mask(odd_mask, 2 * pairs - 1)

        scores(2 * i + 1, odd)
        outputs(2 * i, even_mask, even)
        scores(jnp.minimum(2 * i + 2, 2 * pairs - 1), even)
        outputs(2 * i + 1, odd_mask, odd)
        return 0

    lax.fori_loop(0, pairs, pair, 0)


def mixer_kernel(x_ref, b_ref, c_ref, cum_ref, step_ref, enter_ref, back_ref, spread, y_ref, state):
    state[...] = jnp.zeros_like(state)
    tt = lax.broadcasted_iota(jnp.int32, (CHUNK, CHUNK), 0)
    ss = lax.broadcasted_iota(jnp.int32, (CHUNK, CHUNK), 1)
    below, same, left = tt > ss, tt == ss, ss < HEAD
    nothing = jnp.zeros((CHUNK, CHUNK), BF16)

    def chunk(i, _):
        k = CHUNKS - 1 - i
        at = pl.ds(pl.multiple_of(k * CHUNK, 128), CHUNK)
        c = c_ref[at, :]
        scores = dot_nt(c, b_ref[at, :])
        cum = cum_ref[:, at]
        step = step_ref[:, at]
        f, r = cum[:HEADS], cum[HEADS:]
        sf, sr = step[:HEADS], step[HEADS:]
        row_f = jnp.log(sf) - f
        row_r = jnp.log(sr) - r
        row_d = jnp.log(sf + sr)
        columns = cum.T

        def weights(h):
            lower = columns[:, h : h + 1] + row_f[h : h + 1]
            upper = columns[:, HEADS + h : HEADS + h + 1] + row_r[h : h + 1]
            power = jnp.where(below, lower, jnp.where(same, row_d[h : h + 1], upper))
            return (jnp.exp(power) * scores).astype(BF16)

        wide = widen(jnp.concatenate([jnp.exp(f), jnp.exp(r)], axis=1), spread[...])
        across = wide[:CHUNK] * dot(c, enter_ref[k])
        across = across + wide[CHUNK:] * dot(c, state[...].astype(BF16))
        for pair in range(HEADS // 2):
            cols = slice(pair * 2 * HEAD, (pair + 1) * 2 * HEAD)
            both = jnp.concatenate([weights(2 * pair), weights(2 * pair + 1)], axis=1)
            xp = x_ref[at, cols]
            stacked = jnp.concatenate(
                [jnp.where(left, xp, nothing), jnp.where(left, nothing, xp)], axis=0
            )
            y_ref[at, cols] = dot(both, stacked) + across[:, cols]
        state[...] = state[...] * wide[CHUNK : CHUNK + 1] + back_ref[k].astype(F32)
        return 0

    lax.fori_loop(0, CHUNKS, chunk, 0)


def finish_rows(core, y, c, run, gate, attn, gain, spread, from_low, from_high, out):
    scales = lane_row(gain)
    for i in range(LINE):
        at = pl.ds(pl.multiple_of(i * 256 + core * 128, 128), 128)
        cm = c[at, :]
        reach = jnp.exp(run[:, at])
        wide = widen(jnp.concatenate([reach[:HEADS], reach[HEADS:]], axis=1), spread[...])
        v = y[at, :] + wide[:128] * dot(cm, from_low[...]) + wide[128:] * dot(cm, from_high[...])
        v = v * silu(gate[at, :].astype(F32))
        mean = jnp.mean(v * v, axis=-1, keepdims=True)
        out[i, :, : QHEADS * HEAD] = attn[at, :]
        out[i, :, QHEADS * HEAD :] = (v * lax.rsqrt(mean + NORM_EPS) * scales).astype(BF16)


def theirs_kernel(
    part, d1, d2, d3, y, c, run, gate, attn, gain, spread, theirs, from_low, from_high
):
    got = (None, d1, d2, d3)
    level = lax.axis_index("z")
    for back, keep in ((0, from_low), (1, from_high)):
        count = level if back == 0 else LINE - 1 - level
        prefix = jnp.zeros((STATE, INNER), F32)
        log_prefix = jnp.zeros((1, INNER), F32)
        for d in range(1, LINE):
            r = got[d if back == 0 else LINE - d]
            live = d <= count
            weight = jnp.where(live, jnp.exp(log_prefix), 0.0)
            prefix = prefix + weight * r[:STATE, :].astype(F32)
            tail = r[STATE:, :].astype(F32)
            log = tail[0:1] + tail[1:2] + tail[2:3]
            log_prefix = log_prefix + jnp.where(live, log, 0.0)
        own = part[STATE * back : STATE * (back + 1), :]
        reach = jnp.exp(part[2 * STATE + back : 2 * STATE + back + 1, :])
        keep[...] = (own + reach * prefix).astype(BF16)
    core = 1 - lax.axis_index("c")
    finish_rows(core, y, c, run, gate, attn, gain, spread, from_low, from_high, theirs)


def mine_kernel(y, c, run, gate, attn, gain, spread, from_low, from_high, wa, ws, mine, first):
    finish_rows(lax.axis_index("c"), y, c, run, gate, attn, gain, spread, from_low, from_high, mine)
    first[...] = partial(mine[(lax.axis_index("x") + 2) % LINE], wa, ws)


def sum_kernel(own, direct_right, direct_left, last_right, last_left, out):
    upper = own[:HALVES] + direct_left[...].astype(F32) + last_right[...].astype(F32)
    lower = own[HALVES:] + direct_right[...].astype(F32) + last_left[...].astype(F32)
    out[:HALVES] = upper.astype(BF16)
    out[HALVES:] = lower.astype(BF16)


def partial(v, a, b):
    split = QHEADS * HEAD
    return (dot(v[:, :split], a[...]) + dot(v[:, split:], b[...])).astype(BF16).astype(F32)


def chunk_partial(order, mine, theirs, wa, ws, pa, ps):
    join = lambda ref: jnp.concatenate([ref[index] for index in order], axis=0)
    return partial(join(mine), wa, ws) + partial(join(theirs), pa, ps)


HALVES = 64


def opposite_kernel(first, theirs, pa, ps, right, left):
    value = first[...] + partial(theirs[(lax.axis_index("x") + 2) % LINE], pa, ps)
    right[...] = value[:HALVES].astype(BF16)
    left[...] = value[HALVES:].astype(BF16)


def beside_kernel(mine, theirs, wa, ws, pa, ps, right, left, keep_right, keep_left, own):
    x = lax.axis_index("x")
    order = [(x + 1) % LINE, (x + 3) % LINE, x]
    value = chunk_partial(order, mine, theirs, wa, ws, pa, ps)
    keep_right[...] = value[:HALVES]
    right[...] = value[HALVES : 2 * HALVES].astype(BF16)
    left[...] = value[2 * HALVES : 3 * HALVES].astype(BF16)
    keep_left[...] = value[3 * HALVES : 4 * HALVES]
    own[...] = value[4 * HALVES :]


HBM = pl.BlockSpec(memory_space=pltpu.HBM)


def whole(count):
    return [pl.BlockSpec(memory_space=pltpu.VMEM)] * count


SCALARS = pl.BlockSpec(memory_space=pltpu.SMEM)


def plain(kernel, name, inputs, outs, scalars=0, remote=0, scratch=(), size=8, flops=1e9):
    return pl.pallas_call(
        kernel,
        in_specs=[SCALARS] * scalars + whole(inputs) + [HBM] * remote,
        out_specs=whole(len(outs)),
        out_shape=outs,
        scratch_shapes=list(scratch),
        compiler_params=pltpu.CompilerParams(vmem_limit_bytes=size << 20),
        cost_estimate=cost(flops),
        name=name,
    )


def fixed(shape):
    return pl.BlockSpec(memory_space=pltpu.VMEM)


def params(size):
    return pltpu.CompilerParams(dimension_semantics=("arbitrary",), vmem_limit_bytes=size << 20)


def cost(flops):
    return pl.CostEstimate(flops=int(flops), transcendentals=0, bytes_accessed=8 << 20)


def shaped(shape, dtype):
    return jax.ShapeDtypeStruct(shape, dtype)


def local(
    tokens, norm_gain, query_weight, key_weight, value_weight, query_gain, key_gain, sink_logit,
    gate_weight, inner_weight, input_map, output_map, step_weight, conv_inner, conv_pair,
    decay_rate, decay_jump, inner_gain, attn_out_weight, ssm_out_weight,
):
    up = [(k, k + 1) for k in range(15)]
    down = [(k + 1, k) for k in range(15)]
    swap = [(0, 1), (1, 0)]
    pin = lambda v: pltpu.with_memory_space_constraint(v, pltpu.HBM)
    gain = norm_gain.reshape(WIDTH // 128, 128)
    halo = shaped((EDGE + 8, WIDTH), BF16)
    edge_low, edge_high = plain(
        edge_kernel, "edge", 0, [halo, halo], remote=4,
        scratch=[
            pltpu.VMEM((2 * WINDOW, WIDTH), BF16), pltpu.VMEM((2 * HEAD, WIDTH), BF16),
            pltpu.VMEM((WIDTH // 128, 128), BF16), pltpu.SemaphoreType.DMA((5,)),
        ],
        size=6, flops=1e10,
    )(*map(pin, (gain, tokens, key_weight.T, value_weight.T)))
    halo_low = lax.ppermute(edge_low, SP, up)
    halo_high = lax.ppermute(edge_high, SP, down)
    attn_partner = lax.ppermute(attn_out_weight, "c", swap)
    ssm_partner = lax.ppermute(ssm_out_weight, "c", swap)

    spread = jnp.asarray(head_spread(), BF16)
    step_rows = jnp.transpose(step_weight, (1, 2, 0)).reshape(2 * HEADS, WIDTH)
    jump = jnp.transpose(decay_jump, (1, 2, 0)).reshape(2 * HEADS, ROWS)
    normed, rows, raw, w_gate, w_q, w_kv = plain(
        front_kernel, "front", 5,
        [
            shaped((ROWS, WIDTH), BF16), shaped((CONV // STATE, ROWS, STATE), F32),
            shaped((2 * HEADS, ROWS), F32), shaped((WIDTH, INNER), BF16),
            shaped((WIDTH, QHEADS * HEAD), BF16), shaped((2 * HEAD, WIDTH), BF16),
        ],
        remote=5,
        scratch=[pltpu.VMEM((2 * HEADS, WIDTH), BF16), pltpu.SemaphoreType.DMA((9,))],
        size=8, flops=10e9,
    )(gain, inner_weight, input_map, output_map, tokens, *map(pin, (step_rows, gate_weight, query_weight,
      key_weight.T, value_weight.T)))

    x, b, c, cum, step, run, enter, back, state, spread = plain(
        state_kernel, "state", 8,
        [
            shaped((ROWS, INNER), BF16), shaped((ROWS, STATE), BF16),
            shaped((ROWS, STATE), BF16), shaped((2 * HEADS, ROWS), F32),
            shaped((2 * HEADS, ROWS), F32), shaped((2 * HEADS, ROWS), F32),
            shaped((CHUNKS, STATE, INNER), BF16), shaped((CHUNKS, STATE, INNER), BF16),
            shaped((PACK, INNER), BF16), shaped((2 * HEADS, INNER), BF16),
        ],
        scalars=1, remote=4,
        scratch=[pltpu.VMEM((CONV // STATE, CHUNK + 2 * EDGE, STATE), F32)] * 2
        + [pltpu.VMEM((STATE, INNER), F32)] * 2
        + [
            pltpu.VMEM((2 * HEADS, ROWS), F32), pltpu.VMEM((5, INNER), BF16),
            pltpu.VMEM((5, 2, STATE), BF16), pltpu.SemaphoreType.DMA((4,)),
        ],
        size=8, flops=6e9,
    )(decay_rate, rows, raw, halo_low, halo_high, gain, inner_weight, input_map, output_map, conv_inner, conv_pair,
      jump, spread)

    def along(values, axis):
        sent = {
            d: lax.ppermute(values[d - 1], axis, [(k, (k + d) % LINE) for k in range(LINE)])
            for d in (1, 3, 2)
        }
        return [sent[d] for d in (1, 2, 3)]

    got = along([state] * 3, "y")

    near, far = rope_tables()
    gate, qs, ks, vs = plain(
        heads_kernel, "heads", 8,
        [
            shaped((ROWS, INNER), BF16), shaped((QHEADS * HEAD, ROWS), BF16), shaped((HEAD, ROWS + 2 * WINDOW), BF16),
            shaped((HEAD, ROWS + 2 * WINDOW), BF16),
        ],
        remote=2,
        scratch=[
            pltpu.VMEM((HEAD, ROWS + 2 * WINDOW), F32), pltpu.VMEM((1, HEAD), F32),
            pltpu.SemaphoreType.DMA((2,)),
        ],
        size=6, flops=7e9,
    )(normed, halo_low, halo_high, w_gate, w_q, w_kv, query_gain[None, :], key_gain[None, :],
      jnp.asarray(near), jnp.asarray(far))

    *messages, part = plain(
        line_kernel, "line", 4,
        [shaped((STATE + 16, INNER), BF16)] * 3 + [shaped((PACK, INNER), F32)],
        size=4, flops=1e9,
    )(state, *got)

    far_got = along(messages, "z")

    attn = plain(
        attend_kernel, "attend", 3, [shaped((ROWS, QHEADS * HEAD), BF16)], scalars=1,
        scratch=[pltpu.VMEM((3 * WINDOW, WINDOW), F32)] * 2
        + [pltpu.VMEM((3 * WINDOW, QHEADS * WINDOW), F32)] * 2,
        size=8, flops=7e9,
    )(sink_logit, qs, ks, vs)[0]

    y = plain(
        mixer_kernel, "mixer", 8, [shaped((ROWS, INNER), F32)],
        scratch=[pltpu.VMEM((STATE, INNER), F32)], flops=10e9,
    )(x, b, c, cum, step, enter, back, spread)[0]

    depth = QHEADS * HEAD + INNER
    rest = (y, c, run, gate, attn, inner_gain.reshape(INNER // 128, 128), spread)
    incoming = shaped((STATE, INNER), BF16)
    theirs, from_low, from_high = plain(
        theirs_kernel, "theirs", 11, [shaped((4, 128, depth), BF16), incoming, incoming], flops=2e9
    )(part, *far_got, *rest)
    theirs = lax.ppermute(theirs, "c", swap)
    mine, first = plain(
        mine_kernel, "mine", 11, [shaped((4, 128, depth), BF16), shaped((128, WIDTH), F32)], flops=2e9
    )(*rest, from_low, from_high, attn_out_weight, ssm_out_weight)
    operands = (
        mine, theirs, attn_out_weight, ssm_out_weight, attn_partner, ssm_partner
    )
    sent = shaped((HALVES, WIDTH), BF16)
    kept = shaped((HALVES, WIDTH), F32)
    right = [(k, (k + 1) % LINE) for k in range(LINE)]
    left = [((k + 1) % LINE, k) for k in range(LINE)]
    shift_right = lambda value: lax.ppermute(value, "x", right)
    shift_left = lambda value: lax.ppermute(value, "x", left)
    relay_right, relay_left = plain(
        opposite_kernel, "opposite", 4, [sent, sent], flops=1e9
    )(first, theirs, attn_partner, ssm_partner)
    relay_right = shift_right(relay_right)
    relay_left = shift_left(relay_left)
    direct_right, direct_left, keep_right, keep_left, own = plain(
        beside_kernel, "beside", 6, [sent, sent, kept, kept, shaped((2 * HALVES, WIDTH), F32)],
        flops=3e9,
    )(*operands)
    direct_right = shift_right(direct_right)
    direct_left = shift_left(direct_left)
    last_right = shift_right((keep_right + relay_right.astype(F32)).astype(BF16))
    last_left = shift_left((keep_left + relay_left.astype(F32)).astype(BF16))
    return plain(
        sum_kernel, "sum", 5, [shaped((2 * HALVES, WIDTH), BF16)], size=4, flops=1e6
    )(own, direct_right, direct_left, last_right, last_left)[0]


def solution(mesh):
    split = Mesh(mesh.devices.reshape(4, 4, 4, 2), SP_TP)
    tp = ("x", "c")
    placed = (
        P(SP, None), P(), P(None, tp), P(None, tp), P(None, tp), P(), P(), P(tp),
        P(None, tp), P(None, tp), P(None, tp), P(None, tp), P(None, None, tp), P(None, tp),
        P(None, None, tp), P(None, tp), P(SP, None, tp), P(tp), P(tp, None), P(tp, None),
    )
    return jax.shard_map(
        local, mesh=split, in_specs=placed, out_specs=P(SP_TP, None), check_vma=False
    )
```

time: 90.2 us -> 81.1 us (0.90)
  Pallas kernels: 43.3 us -> 37.3 us
  waiting for transfers between devices: 14.7 us -> 12 us
  other arithmetic: 1.14 us -> 0.09 us
    pallas_call x6 -> x8, Pallas kernels: 26.5 us -> 23.6 us  [the longest x1 6.16 us: local(): plain(front_kernel, 'front', 5, [shaped((ROWS, WIDTH), BF16), shaped((CON...]
    ppermute x3, waiting for transfers between devices: 5.88 us -> 8.69 us  [local(): shift_right = lambda value: lax.ppermute(value, 'x', right)]
    pallas_call x1, Pallas kernels: 6.93 us -> 4.4 us  [local(): plain(attend_kernel, 'attend', 3, [shaped((ROWS, QHEADS * HEAD), BF16)],...]
    ppermute x3, waiting for transfers between devices: 4.41 us -> 2.02 us  [local(): shift_left = lambda value: lax.ppermute(value, 'x', left)]
    ppermute x1, waiting for transfers between devices: 1.91 us -> 0.36 us  [local(): theirs = lax.ppermute(theirs, 'c', swap)]
    ppermute x6, waiting for transfers between devices: 2.01 us -> 0.91 us  [along(): lax.ppermute(values[d - 1], axis, [(k, (k + d) % LINE) for k in range(LIN...]
  transfers between devices with their start and end apart: 17 -> 17, of which waited for: 8 -> 7; matrix products, arithmetic and copies ran while one was open for 0% -> 0% of each run, Pallas kernels for 46% -> 42%
where the time goes in v2:
time: 81.1 us; the launch traced here: 80.5 us
  Pallas kernels  37.3 us (46%)
  starting transfers between devices  30.6 us (38%)
  waiting for transfers between devices  12 us (15%)
    ppermute x6, starting transfers between devices, along(): lax.ppermute(values[d - 1], axis, [(k, (k + d) % LINE) for k in range(LIN...  13.1 us
    ppermute x3, waiting for transfers between devices, local(): shift_right = lambda value: lax.ppermute(value, 'x', right)  8.69 us
    ppermute x3, starting transfers between devices, local(): shift_left = lambda value: lax.ppermute(value, 'x', left)  8.29 us
    pallas_call x1, Pallas kernels, local(): plain(state_kernel, 'state', 8, [shaped((ROWS, INNER), BF16), shaped((ROW...  6.25 us
    pallas_call x1, Pallas kernels, local(): plain(front_kernel, 'front', 5, [shaped((ROWS, WIDTH), BF16), shaped((CON...  6.16 us
    pallas_call x1, Pallas kernels, local(): plain(mixer_kernel, 'mixer', 8, [shaped((ROWS, INNER), F32)], scratch=[pl...  5.87 us
    pallas_call x1, Pallas kernels, local(): plain(heads_kernel, 'heads', 8, [shaped((ROWS, INNER), BF16), shaped((QHE...  5.1 us
    pallas_call x1, Pallas kernels, local(): plain(attend_kernel, 'attend', 3, [shaped((ROWS, QHEADS * HEAD), BF16)],...  4.4 us
  transfers between devices with their start and end apart: 17, of which 7 were waited for; matrix products, arithmetic and copies ran while one was open for 0% of the time, Pallas kernels for 42%

profile of v2, /device:TPU:1, one launch (start us, length us, event | category | flops | bytes accessed | tf_op | source)
XLA Modules:
  0.0 80.5 jit_solution(2844623382731127949)
XLA Ops:
  0.0 2.3 %edge.1 = (bf16[24,2048]{1,0:T(8,128)(2,1)S(1)}, bf16[24,2048]{1,0:T(8,128)(2,1)S(1)}) custom-call(bf16[16,128]{1,0:T(8,128)(2,1)} %bitcast.15, bf16[1024,2048]{1,0:T(8,128)(2,1)} %tok.3, bf16[64,2048]{1,0:T(8,128)(2,1)} %bitcast.20, bf16[64,2048]{1,0:T(8,128)(2,1)} %bitcast.22), custom_call_target="tpu_custom_call" | custom-call | flops 10000000000 | bytes 8388608 | tf_op jit(solution)/shard_map/edge/pallas_call | solution.py:595
  2.3 4.3 %collective-permute-start = (bf16[24,2048]{1,0:T(8,128)(2,1)S(1)}, bf16[24,2048]{1,0:T(8,128)(2,1)S(1)}, u32[]{:S(2)}, u32[]{:S(2)}) collective-permute-start(bf16[24,2048]{1,0:T(8,128)(2,1)S(1)} %get-tuple-element.45), channel_id=1, source_target_pairs={{0,8},{8,16},{16,24},{24,32},{32,40},{40,48},{48,56},{56,64},{64,7... | collective-permute-start | bytes 294920 | tf_op jit(solution)/shard_map/ppermute | solution.py:603
  6.6 1.3 %collective-permute-start.1 = (bf16[24,2048]{1,0:T(8,128)(2,1)S(1)}, bf16[24,2048]{1,0:T(8,128)(2,1)S(1)}, u32[]{:S(2)}, u32[]{:S(2)}) collective-permute-start(bf16[24,2048]{1,0:T(8,128)(2,1)S(1)} %get-tuple-element.46), channel_id=1, source_target_pairs={{8,0},{16,8},{24,16},{32,24},{40,32},{48,40},{56,48},{64,56},{72,6... | collective-permute-start | bytes 294920 | tf_op jit(solution)/shard_map/ppermute | solution.py:604
  7.9 1.0 %collective-permute-start.10 = (bf16[512,2048]{1,0:T(8,128)(2,1)S(1)}, bf16[512,2048]{1,0:T(8,128)(2,1)S(1)}, u32[]{:S(2)}, u32[]{:S(2)}) collective-permute-start(bf16[512,2048]{1,0:T(8,128)(2,1)S(1)} %copy-done), channel_id=1, source_target_pairs={{0,1},{1,0},{2,3},{3,2},{4,5},{5,4},{6,7},{7,6},{8,9},{9,8},{10,11... | collective-permute-start | bytes 6291464 | tf_op jit(solution)/shard_map/ppermute | solution.py:606
  9.2 6.2 %front.1 = (bf16[1024,2048]{1,0:T(8,128)(2,1)S(1)}, f32[6,1024,128]{2,1,0:T(8,128)S(1)}, f32[16,1024]{1,0:T(8,128)S(1)}, bf16[2048,512]{1,0:T(8,128)(2,1)S(1)}, ...) custom-call(bf16[16,128]{1,0:T(8,128)(2,1)S(1)} %bitcast.16, bf16[2048,512]{1,0:T(8,128)(2,1)S(1)} %copy-done.4, ...), custom_call_target="tpu_custom_call" | custom-call | flops 10000000000 | bytes 8388608 | tf_op jit(solution)/shard_map/front/pallas_call | solution.py:611
  15.4 6.3 %state.1 = (bf16[1024,512]{1,0:T(8,128)(2,1)S(1)}, bf16[1024,128]{1,0:T(8,128)(2,1)S(1)}, bf16[1024,128]{1,0:T(8,128)(2,1)S(1)}, f32[16,1024]{1,0:T(8,128)S(1)},...) custom-call(f32[2,8]{1,0:T(2,128)S(1)} %copy-done.11, ...), custom_call_target="tpu_custom_call" | custom-call | flops 6000000000 | bytes 8388608 | tf_op jit(solution)/shard_map/state/pallas_call | solution.py:624
  21.7 2.4 %collective-permute-start.2 = (bf16[272,512]{1,0:T(8,128)(2,1)S(1)}, bf16[272,512]{1,0:T(8,128)(2,1)S(1)}, u32[]{:S(2)}, u32[]{:S(2)}) collective-permute-start(bf16[272,512]{1,0:T(8,128)(2,1)S(1)} %get-tuple-element.64.own), channel_id=1, source_target_pairs={{0,8},{8,16},{16,24},{24,0},{1,9},{9,17},{17,25},{25,1},{2,10},{10... | collective-permute-start | bytes 835592 | tf_op jit(solution)/shard_map/ppermute | solution.py:646
  24.1 2.6 %collective-permute-start.3 = (bf16[272,512]{1,0:T(8,128)(2,1)S(1)}, bf16[272,512]{1,0:T(8,128)(2,1)S(1)}, u32[]{:S(2)}, u32[]{:S(2)}) collective-permute-start(bf16[272,512]{1,0:T(8,128)(2,1)S(1)} %get-tuple-element.64.own), channel_id=1, source_target_pairs={{0,16},{8,24},{16,0},{24,8},{1,17},{9,25},{17,1},{25,9},{2,18},{10... | collective-permute-start | bytes 835592 | tf_op jit(solution)/shard_map/ppermute | solution.py:646
  26.7 1.1 %collective-permute-start.4 = (bf16[272,512]{1,0:T(8,128)(2,1)S(1)}, bf16[272,512]{1,0:T(8,128)(2,1)S(1)}, u32[]{:S(2)}, u32[]{:S(2)}) collective-permute-start(bf16[272,512]{1,0:T(8,128)(2,1)S(1)} %get-tuple-element.64.own), channel_id=1, source_target_pairs={{0,24},{8,0},{16,8},{24,16},{1,25},{9,1},{17,9},{25,17},{2,26},{10... | collective-permute-start | bytes 835592 | tf_op jit(solution)/shard_map/ppermute | solution.py:646
  27.8 5.9 %mixer.1.y = f32[1024,512]{1,0:T(8,128)S(1)} custom-call(bf16[1024,512]{1,0:T(8,128)(2,1)S(1)} %get-tuple-element.47.x_ref, bf16[1024,128]{1,0:T(8,128)(2,1)S(1)} %get-tuple-element.48.b_ref, bf16[1024,128]{1,0:T(8,128)(2,1)S(1)} %get-tuple-element.49.c_ref.c, f32[16,1024]{1,0:T(8,128)S(1)} %get-tuple-element.50.cum_ref, ...), custom_call_target="tpu_custom_call" | custom-call | flops 10000000000 | bytes 8388608 | tf_op jit(solution)/shard_map/mixer/pallas_call | solution.py:684
  33.7 5.1 %heads.1 = (bf16[1024,512]{1,0:T(8,128)(2,1)S(1)}, bf16[256,1024]{1,0:T(8,128)(2,1)S(1)}, bf16[64,1280]{1,0:T(8,128)(2,1)S(1)}, bf16[64,1280]{1,0:T(8,128)(2,1)S(1)}) custom-call(bf16[1024,2048]{1,0:T(8,128)(2,1)S(1)} %get-tuple-element.56.normed, bf16[24,2048]{1,0:T(8,128)(2,1)S(1)} %collective-permute-done.low, ...), custom_call_target="tpu_custom_call" | custom-call | flops 7000000000 | bytes 8388608 | tf_op jit(solution)/shard_map/heads/pallas_call | solution.py:654
  39.5 2.9 %collective-permute-start.5 = (bf16[144,512]{1,0:T(8,128)(2,1)S(1)}, bf16[144,512]{1,0:T(8,128)(2,1)S(1)}, u32[]{:S(2)}, u32[]{:S(2)}) collective-permute-start(bf16[144,512]{1,0:T(8,128)(2,1)S(1)} %get-tuple-element.66), channel_id=1, source_target_pairs={{0,32},{32,64},{64,96},{96,0},{1,33},{33,65},{65,97},{97,1},{2,34}... | collective-permute-start | bytes 442376 | tf_op jit(solution)/shard_map/ppermute | solution.py:646
  42.4 3.3 %collective-permute-start.6 = (bf16[144,512]{1,0:T(8,128)(2,1)S(1)}, bf16[144,512]{1,0:T(8,128)(2,1)S(1)}, u32[]{:S(2)}, u32[]{:S(2)}) collective-permute-start(bf16[144,512]{1,0:T(8,128)(2,1)S(1)} %get-tuple-element.67), channel_id=1, source_target_pairs={{0,64},{32,96},{64,0},{96,32},{1,65},{33,97},{65,1},{97,33},{2,66}... | collective-permute-start | bytes 442376 | tf_op jit(solution)/shard_map/ppermute | solution.py:646
  46.4 4.4 %attend.1.attn = bf16[1024,256]{1,0:T(8,128)(2,1)S(1)} custom-call(f32[4]{0:T(128)S(1)} %copy-done.14, bf16[256,1024]{1,0:T(8,128)(2,1)S(1)} %get-tuple-element.61.qs, bf16[64,1280]{1,0:T(8,128)(2,1)S(1)} %get-tuple-element.62.ks, bf16[64,1280]{1,0:T(8,128)(2,1)S(1)} %get-tuple-element.63.vs), custom_call_target="tpu_custom_call" | custom-call | flops 7000000000 | bytes 8388608 | tf_op jit(solution)/shard_map/attend/pallas_call | solution.py:677
  51.6 1.1 %theirs.1 = (bf16[4,128,768]{2,1,0:T(8,128)(2,1)S(1)}, bf16[128,512]{1,0:T(8,128)(2,1)S(1)}, bf16[128,512]{1,0:T(8,128)(2,1)S(1)}) custom-call(f32[272,512]{1,0:T(8,128)S(1)} %get-tuple-element.65.part, bf16[144,512]{1,0:T(8,128)(2,1)S(1)} %collective-permute-done.5.d1, bf16[144,512]{1,0:T(8,128)(2,1)S(1)} %collective-permute-done.6.d2, ...), custom_call_target="tpu_custom_call" | custom-call | flops 2000000000 | bytes 8388608 | tf_op jit(solution)/shard_map/theirs/pallas_call | solution.py:692
  52.6 2.2 %collective-permute-start.8 = (bf16[4,128,768]{2,1,0:T(8,128)(2,1)S(1)}, bf16[4,128,768]{2,1,0:T(8,128)(2,1)S(1)}, u32[]{:S(2)}, u32[]{:S(2)}) collective-permute-start(bf16[4,128,768]{2,1,0:T(8,128)(2,1)S(1)} %get-tuple-element.72), channel_id=1, source_target_pairs={{0,1},{1,0},{2,3},{3,2},{4,5},{5,4},{6,7},{7,6},{8,9},{9,8},{10,11... | collective-permute-start | bytes 2359304 | tf_op jit(solution)/shard_map/ppermute | solution.py:695
  54.8 1.5 %mine.1 = (bf16[4,128,768]{2,1,0:T(8,128)(2,1)S(1)}, f32[128,2048]{1,0:T(8,128)S(1)}) custom-call(f32[1024,512]{1,0:T(8,128)S(1)} %mixer.1.y, bf16[1024,128]{1,0:T(8,128)(2,1)S(1)} %get-tuple-element.49.c_ref.c, f32[16,1024]{1,0:T(8,128)S(1)} %get-tuple-element.55.run, bf16[1024,512]{1,0:T(8,128)(2,1)S(1)} %get-tuple-element.60.gate, ...), custom_call_target="tpu_custom_call" | custom-call | flops 2000000000 | bytes 8388608 | tf_op jit(solution)/shard_map/mine/pallas_call | solution.py:696
  57.4 2.5 %collective-permute-start.15 = (bf16[64,2048]{1,0:T(8,128)(2,1)S(1)}, bf16[64,2048]{1,0:T(8,128)(2,1)S(1)}, u32[]{:S(2)}, u32[]{:S(2)}) collective-permute-start(bf16[64,2048]{1,0:T(8,128)(2,1)S(1)} %get-tuple-element.80), channel_id=1, source_target_pairs={{2,0},{4,2},{6,4},{0,6},{3,1},{5,3},{7,5},{1,7},{10,8},{12,10},{14... | collective-permute-start | bytes 786440 | tf_op jit(solution)/shard_map/ppermute | solution.py:707
  59.9 2.7 %beside.1 = (bf16[64,2048]{1,0:T(8,128)(2,1)S(1)}, bf16[64,2048]{1,0:T(8,128)(2,1)S(1)}, f32[64,2048]{1,0:T(8,128)S(1)}, f32[64,2048]{1,0:T(8,128)S(1)}, f32[128,2048]{1,0:T(8,128)S(1)}) custom-call(bf16[4,128,768]{2,1,0:T(8,128)(2,1)S(1)} %get-tuple-element.71.mine, bf16[4,128,768]{2,1,0:T(8,128)(2,1)S(1)} %collective-permute-done.8.theirs, ...), custom_call_target="tpu_custom_call" | custom-call | flops 3000000000 | bytes 8388608 | tf_op jit(solution)/shard_map/beside/pallas_call | solution.py:713
  62.9 2.5 %collective-permute-start.12 = (bf16[64,2048]{1,0:T(8,128)(2,1)S(1)}, bf16[64,2048]{1,0:T(8,128)(2,1)S(1)}, u32[]{:S(2)}, u32[]{:S(2)}) collective-permute-start(bf16[64,2048]{1,0:T(8,128)(2,1)S(1)} %get-tuple-element.75), channel_id=1, source_target_pairs={{2,0},{4,2},{6,4},{0,6},{3,1},{5,3},{7,5},{1,7},{10,8},{12,10},{14... | collective-permute-start | bytes 786440 | tf_op jit(solution)/shard_map/ppermute | solution.py:707
  65.5 3.2 %collective-permute-start.16 = (bf16[64,2048]{1,0:T(8,128)(2,1)S(1)}, bf16[64,2048]{1,0:T(8,128)(2,1)S(1)}, u32[]{:S(2)}, u32[]{:S(2)}) collective-permute-start(bf16[64,2048]{1,0:T(8,128)(2,1)S(1)} %add_convert_fusion), channel_id=1, source_target_pairs={{2,0},{4,2},{6,4},{0,6},{3,1},{5,3},{7,5},{1,7},{10,8},{12,10},{14... | collective-permute-start | bytes 786440 | tf_op jit(solution)/shard_map/ppermute | solution.py:707
  68.8 5.1 %collective-permute-done.11.direct_right = bf16[64,2048]{1,0:T(8,128)(2,1)S(1)} collective-permute-done((bf16[64,2048]{1,0:T(8,128)(2,1)S(1)}, bf16[64,2048]{1,0:T(8,128)(2,1)S(1)}, u32[]{:S(2)}, u32[]{:S(2)}) %collective-permute-start.11) | collective-permute-done | bytes 262176 | tf_op jit(solution)/shard_map/ppermute | solution.py:706
  73.9 2.0 %collective-permute-done.16.last_left = bf16[64,2048]{1,0:T(8,128)(2,1)S(1)} collective-permute-done((bf16[64,2048]{1,0:T(8,128)(2,1)S(1)}, bf16[64,2048]{1,0:T(8,128)(2,1)S(1)}, u32[]{:S(2)}, u32[]{:S(2)}) %collective-permute-start.16) | collective-permute-done | bytes 262176 | tf_op jit(solution)/shard_map/ppermute | solution.py:707
  75.9 3.6 %collective-permute-done.14.last_right = bf16[64,2048]{1,0:T(8,128)(2,1)S(1)} collective-permute-done((bf16[64,2048]{1,0:T(8,128)(2,1)S(1)}, bf16[64,2048]{1,0:T(8,128)(2,1)S(1)}, u32[]{:S(2)}, u32[]{:S(2)}) %collective-permute-start.14) | collective-permute-done | bytes 262176 | tf_op jit(solution)/shard_map/ppermute | solution.py:706
  (60 shorter events, 4.6 us)
Async XLA Ops:
  0.0 7.9 %copy-start = (bf16[512,2048]{1,0:T(8,128)(2,1)S(1)}, bf16[512,2048]{1,0:T(8,128)(2,1)}, u32[]{:S(2)}) copy-start(bf16[512,2048]{1,0:T(8,128)(2,1)} %ws.3) | copy-start | bytes 6291460
  0.0 9.0 %copy-start.1 = (bf16[256,2048]{1,0:T(8,128)(2,1)S(1)}, bf16[256,2048]{1,0:T(8,128)(2,1)}, u32[]{:S(2)}) copy-start(bf16[256,2048]{1,0:T(8,128)(2,1)} %wa.3) | copy-start | bytes 3145732
  0.0 9.1 %copy-start.3 = (bf16[1024,2048]{1,0:T(8,128)(2,1)S(1)}, bf16[1024,2048]{1,0:T(8,128)(2,1)}, u32[]{:S(2)}) copy-start(bf16[1024,2048]{1,0:T(8,128)(2,1)} %tok.3) | copy-start | bytes 12582916
  0.0 9.1 %copy-start.4 = (bf16[2048,512]{1,0:T(8,128)(2,1)S(1)}, bf16[2048,512]{1,0:T(8,128)(2,1)}, u32[]{:S(2)}) copy-start(bf16[2048,512]{1,0:T(8,128)(2,1)} %w_inner.3) | copy-start | bytes 6291460
  0.0 9.1 %copy-start.5 = (bf16[2048,128]{1,0:T(8,128)(2,1)S(1)}, bf16[2048,128]{1,0:T(8,128)(2,1)}, u32[]{:S(2)}) copy-start(bf16[2048,128]{1,0:T(8,128)(2,1)} %w_in.3) | copy-start | bytes 1572868
  0.0 9.1 %copy-start.6 = (bf16[2048,128]{1,0:T(8,128)(2,1)S(1)}, bf16[2048,128]{1,0:T(8,128)(2,1)}, u32[]{:S(2)}) copy-start(bf16[2048,128]{1,0:T(8,128)(2,1)} %w_out.3) | copy-start | bytes 1572868
  0.0 9.1 %copy-start.9 = (bf16[2048]{0:T(1024)(128)(2,1)S(1)}, bf16[2048]{0:T(1024)(128)(2,1)}, u32[]{:S(2)}) copy-start(bf16[2048]{0:T(1024)(128)(2,1)} %param.24) | copy-start | bytes 12292
  2.3 13.0 %collective-permute-start = (bf16[24,2048]{1,0:T(8,128)(2,1)S(1)}, bf16[24,2048]{1,0:T(8,128)(2,1)S(1)}, u32[]{:S(2)}, u32[]{:S(2)}) collective-permute-start(bf16[24,2048]{1,0:T(8,128)(2,1)S(1)} %get-tuple-element.45), channel_id=1, source_target_pairs={{0,8},{8,16},{16,24},{24,32},{32,40},{40,48},{48,56},{56,64},{64,7... | collective-permute-start | bytes 294920 | tf_op jit(solution)/shard_map/ppermute | solution.py:603
  6.6 8.7 %collective-permute-start.1 = (bf16[24,2048]{1,0:T(8,128)(2,1)S(1)}, bf16[24,2048]{1,0:T(8,128)(2,1)S(1)}, u32[]{:S(2)}, u32[]{:S(2)}) collective-permute-start(bf16[24,2048]{1,0:T(8,128)(2,1)S(1)} %get-tuple-element.46), channel_id=1, source_target_pairs={{8,0},{16,8},{24,16},{32,24},{40,32},{48,40},{56,48},{64,56},{72,6... | collective-permute-start | bytes 294920 | tf_op jit(solution)/shard_map/ppermute | solution.py:604
  7.9 48.8 %collective-permute-start.10 = (bf16[512,2048]{1,0:T(8,128)(2,1)S(1)}, bf16[512,2048]{1,0:T(8,128)(2,1)S(1)}, u32[]{:S(2)}, u32[]{:S(2)}) collective-permute-start(bf16[512,2048]{1,0:T(8,128)(2,1)S(1)} %copy-done), channel_id=1, source_target_pairs={{0,1},{1,0},{2,3},{3,2},{4,5},{5,4},{6,7},{7,6},{8,9},{9,8},{10,11... | collective-permute-start | bytes 6291464 | tf_op jit(solution)/shard_map/ppermute | solution.py:606
  9.0 47.4 %collective-permute-start.9 = (bf16[256,2048]{1,0:T(8,128)(2,1)S(1)}, bf16[256,2048]{1,0:T(8,128)(2,1)S(1)}, u32[]{:S(2)}, u32[]{:S(2)}) collective-permute-start(bf16[256,2048]{1,0:T(8,128)(2,1)S(1)} %copy-done.1), channel_id=1, source_target_pairs={{0,1},{1,0},{2,3},{3,2},{4,5},{5,4},{6,7},{7,6},{8,9},{9,8},{10,11... | collective-permute-start | bytes 3145736 | tf_op jit(solution)/shard_map/ppermute | solution.py:605
  21.7 17.2 %collective-permute-start.2 = (bf16[272,512]{1,0:T(8,128)(2,1)S(1)}, bf16[272,512]{1,0:T(8,128)(2,1)S(1)}, u32[]{:S(2)}, u32[]{:S(2)}) collective-permute-start(bf16[272,512]{1,0:T(8,128)(2,1)S(1)} %get-tuple-element.64.own), channel_id=1, source_target_pairs={{0,8},{8,16},{16,24},{24,0},{1,9},{9,17},{17,25},{25,1},{2,10},{10... | collective-permute-start | bytes 835592 | tf_op jit(solution)/shard_map/ppermute | solution.py:646
  24.1 14.9 %collective-permute-start.3 = (bf16[272,512]{1,0:T(8,128)(2,1)S(1)}, bf16[272,512]{1,0:T(8,128)(2,1)S(1)}, u32[]{:S(2)}, u32[]{:S(2)}) collective-permute-start(bf16[272,512]{1,0:T(8,128)(2,1)S(1)} %get-tuple-element.64.own), channel_id=1, source_target_pairs={{0,16},{8,24},{16,0},{24,8},{1,17},{9,25},{17,1},{25,9},{2,18},{10... | collective-permute-start | bytes 835592 | tf_op jit(solution)/shard_map/ppermute | solution.py:646
  26.7 12.3 %collective-permute-start.4 = (bf16[272,512]{1,0:T(8,128)(2,1)S(1)}, bf16[272,512]{1,0:T(8,128)(2,1)S(1)}, u32[]{:S(2)}, u32[]{:S(2)}) collective-permute-start(bf16[272,512]{1,0:T(8,128)(2,1)S(1)} %get-tuple-element.64.own), channel_id=1, source_target_pairs={{0,24},{8,0},{16,8},{24,16},{1,25},{9,1},{17,9},{25,17},{2,26},{10... | collective-permute-start | bytes 835592 | tf_op jit(solution)/shard_map/ppermute | solution.py:646
  39.5 11.4 %collective-permute-start.5 = (bf16[144,512]{1,0:T(8,128)(2,1)S(1)}, bf16[144,512]{1,0:T(8,128)(2,1)S(1)}, u32[]{:S(2)}, u32[]{:S(2)}) collective-permute-start(bf16[144,512]{1,0:T(8,128)(2,1)S(1)} %get-tuple-element.66), channel_id=1, source_target_pairs={{0,32},{32,64},{64,96},{96,0},{1,33},{33,65},{65,97},{97,1},{2,34}... | collective-permute-start | bytes 442376 | tf_op jit(solution)/shard_map/ppermute | solution.py:646
  42.4 8.6 %collective-permute-start.6 = (bf16[144,512]{1,0:T(8,128)(2,1)S(1)}, bf16[144,512]{1,0:T(8,128)(2,1)S(1)}, u32[]{:S(2)}, u32[]{:S(2)}) collective-permute-start(bf16[144,512]{1,0:T(8,128)(2,1)S(1)} %get-tuple-element.67), channel_id=1, source_target_pairs={{0,64},{32,96},{64,0},{96,32},{1,65},{33,97},{65,1},{97,33},{2,66}... | collective-permute-start | bytes 442376 | tf_op jit(solution)/shard_map/ppermute | solution.py:646
  45.7 5.9 %collective-permute-start.7 = (bf16[144,512]{1,0:T(8,128)(2,1)S(1)}, bf16[144,512]{1,0:T(8,128)(2,1)S(1)}, u32[]{:S(2)}, u32[]{:S(2)}) collective-permute-start(bf16[144,512]{1,0:T(8,128)(2,1)S(1)} %get-tuple-element.68), channel_id=1, source_target_pairs={{0,96},{32,0},{64,32},{96,64},{1,97},{33,1},{65,33},{97,65},{2,98}... | collective-permute-start | bytes 442376 | tf_op jit(solution)/shard_map/ppermute | solution.py:646
  52.6 4.1 %collective-permute-start.8 = (bf16[4,128,768]{2,1,0:T(8,128)(2,1)S(1)}, bf16[4,128,768]{2,1,0:T(8,128)(2,1)S(1)}, u32[]{:S(2)}, u32[]{:S(2)}) collective-permute-start(bf16[4,128,768]{2,1,0:T(8,128)(2,1)S(1)} %get-tuple-element.72), channel_id=1, source_target_pairs={{0,1},{1,0},{2,3},{3,2},{4,5},{5,4},{6,7},{7,6},{8,9},{9,8},{10,11... | collective-permute-start | bytes 2359304 | tf_op jit(solution)/shard_map/ppermute | solution.py:695
  57.4 8.1 %collective-permute-start.15 = (bf16[64,2048]{1,0:T(8,128)(2,1)S(1)}, bf16[64,2048]{1,0:T(8,128)(2,1)S(1)}, u32[]{:S(2)}, u32[]{:S(2)}) collective-permute-start(bf16[64,2048]{1,0:T(8,128)(2,1)S(1)} %get-tuple-element.80), channel_id=1, source_target_pairs={{2,0},{4,2},{6,4},{0,6},{3,1},{5,3},{7,5},{1,7},{10,8},{12,10},{14... | collective-permute-start | bytes 786440 | tf_op jit(solution)/shard_map/ppermute | solution.py:707
  59.9 8.8 %collective-permute-start.13 = (bf16[64,2048]{1,0:T(8,128)(2,1)S(1)}, bf16[64,2048]{1,0:T(8,128)(2,1)S(1)}, u32[]{:S(2)}, u32[]{:S(2)}) collective-permute-start(bf16[64,2048]{1,0:T(8,128)(2,1)S(1)} %get-tuple-element.78), channel_id=1, source_target_pairs={{0,2},{2,4},{4,6},{6,0},{1,3},{3,5},{5,7},{7,1},{8,10},{10,12},{12... | collective-permute-start | bytes 786440 | tf_op jit(solution)/shard_map/ppermute | solution.py:706
  62.6 11.3 %collective-permute-start.11 = (bf16[64,2048]{1,0:T(8,128)(2,1)S(1)}, bf16[64,2048]{1,0:T(8,128)(2,1)S(1)}, u32[]{:S(2)}, u32[]{:S(2)}) collective-permute-start(bf16[64,2048]{1,0:T(8,128)(2,1)S(1)} %get-tuple-element.74), channel_id=1, source_target_pairs={{0,2},{2,4},{4,6},{6,0},{1,3},{3,5},{5,7},{7,1},{8,10},{10,12},{12... | collective-permute-start | bytes 786440 | tf_op jit(solution)/shard_map/ppermute | solution.py:706
  62.9 11.0 %collective-permute-start.12 = (bf16[64,2048]{1,0:T(8,128)(2,1)S(1)}, bf16[64,2048]{1,0:T(8,128)(2,1)S(1)}, u32[]{:S(2)}, u32[]{:S(2)}) collective-permute-start(bf16[64,2048]{1,0:T(8,128)(2,1)S(1)} %get-tuple-element.75), channel_id=1, source_target_pairs={{2,0},{4,2},{6,4},{0,6},{3,1},{5,3},{7,5},{1,7},{10,8},{12,10},{14... | collective-permute-start | bytes 786440 | tf_op jit(solution)/shard_map/ppermute | solution.py:707
  65.5 10.4 %collective-permute-start.16 = (bf16[64,2048]{1,0:T(8,128)(2,1)S(1)}, bf16[64,2048]{1,0:T(8,128)(2,1)S(1)}, u32[]{:S(2)}, u32[]{:S(2)}) collective-permute-start(bf16[64,2048]{1,0:T(8,128)(2,1)S(1)} %add_convert_fusion), channel_id=1, source_target_pairs={{2,0},{4,2},{6,4},{0,6},{3,1},{5,3},{7,5},{1,7},{10,8},{12,10},{14... | collective-permute-start | bytes 786440 | tf_op jit(solution)/shard_map/ppermute | solution.py:707
  68.8 10.8 %collective-permute-start.14 = (bf16[64,2048]{1,0:T(8,128)(2,1)S(1)}, bf16[64,2048]{1,0:T(8,128)(2,1)S(1)}, u32[]{:S(2)}, u32[]{:S(2)}) collective-permute-start(bf16[64,2048]{1,0:T(8,128)(2,1)S(1)} %add_convert_fusion.1), channel_id=1, source_target_pairs={{0,2},{2,4},{4,6},{6,0},{1,3},{3,5},{5,7},{7,1},{8,10},{10,12},{12... | collective-permute-start | bytes 786440 | tf_op jit(solution)/shard_map/ppermute | solution.py:706
  (11 other events, 67.6 us)

commit v3 on v2

--- a/solution.py
+++ b/solution.py
@@ -105,10 +105,12 @@
         ],
         sems,
     )
-    for copy in copies:
-        copy.wait()
-    g = lane_row(gain)
-    kv = dot_nt(w_kv[...], normalise(edge[...], g)).astype(BF16)
+    for k in (4, 0, 1):
+        copies[k].wait()
+    n = normalise(edge[...], lane_row(gain))
+    for k in (2, 3):
+        copies[k].wait()
+    kv = dot_nt(w_kv[...], n).astype(BF16)
     for ref, at, rows in ((low, 0, WINDOW - EDGE), (high, WINDOW, WINDOW)):
         ref[:EDGE, :] = edge[rows : rows + EDGE, :]
         for k in range(WIDTH // 128):
@@ -163,13 +165,10 @@
 
 
 def state_kernel(
-    rate, rows, raw, low, high, gain, w_inner, w_in, w_out, h_inner_taps, h_pair_taps, h_jump, h_spread,
-    x_ref, b_ref, c_ref, cum_ref, step_ref, run_ref, enter_ref, back_ref, state_ref, spread,
-    first, last, state_f, state_b, jump, inner_taps, pair_taps, sems,
+    rate, rows, raw, low, high, gain, w_inner, w_in, w_out, inner_taps, pair_taps, jump, spread,
+    x_ref, b_ref, c_ref, cum_ref, step_ref, run_ref, enter_ref, back_ref, state_ref,
+    first, last, state_f, state_b,
 ):
-    copies = fetch(
-        [(h_jump, jump), (h_spread, spread), (h_inner_taps, inner_taps), (h_pair_taps, pair_taps)], sems
-    )
     g = lane_row(gain)
     edge = normalise(jnp.concatenate([low[:EDGE, :], high[:EDGE, :]], axis=0), g)
     for k in range(CONV // STATE):
@@ -182,8 +181,6 @@
         first[k, EDGE:, :] = rows[k, : CHUNK + EDGE, :]
         last[k, : CHUNK + EDGE, :] = rows[k, ROWS - CHUNK - EDGE :, :]
         last[k, CHUNK + EDGE :, :] = value[EDGE:]
-    for copy in copies:
-        copy.wait()
     taps = jnp.concatenate(
         [inner_taps[...].astype(F32)] + [pair_taps[:, k, :].astype(F32) for k in (0, 1)], axis=1
     )
@@ -322,13 +319,10 @@
 
 
 def heads_kernel(
-    normed, low, high, w_gate, w_q, w_kv, q_row, k_row, h_near, h_far, gate, qs, ks, vs, near, far, sems
+    normed, low, high, w_gate, w_q, w_kv, q_row, k_row, near, far, gate, qs, ks, vs
 ):
-    copies = fetch([(h_near, near), (h_far.at[lax.axis_index(SP)], far)], sems)
     q_gain, k_gain = column(q_row[...]), column(k_row[...])
-    for copy in copies:
-        copy.wait()
-    turns = column(far[...])
+    turns = column(far[lax.axis_index(SP)])
     far_cos = turns[:HALF, :]
     far_sin = turns[HALF:, :]
     scale = jnp.asarray(HEAD**-0.5, BF16)
@@ -621,22 +615,18 @@
     )(gain, inner_weight, input_map, output_map, tokens, *map(pin, (step_rows, gate_weight, query_weight,
       key_weight.T, value_weight.T)))
 
-    x, b, c, cum, step, run, enter, back, state, spread = plain(
-        state_kernel, "state", 8,
+    x, b, c, cum, step, run, enter, back, state = plain(
+        state_kernel, "state", 12,
         [
             shaped((ROWS, INNER), BF16), shaped((ROWS, STATE), BF16),
             shaped((ROWS, STATE), BF16), shaped((2 * HEADS, ROWS), F32),
             shaped((2 * HEADS, ROWS), F32), shaped((2 * HEADS, ROWS), F32),
             shaped((CHUNKS, STATE, INNER), BF16), shaped((CHUNKS, STATE, INNER), BF16),
-            shaped((PACK, INNER), BF16), shaped((2 * HEADS, INNER), BF16),
+            shaped((PACK, INNER), BF16),
         ],
-        scalars=1, remote=4,
+        scalars=1,
         scratch=[pltpu.VMEM((CONV // STATE, CHUNK + 2 * EDGE, STATE), F32)] * 2
-        + [pltpu.VMEM((STATE, INNER), F32)] * 2
-        + [
-            pltpu.VMEM((2 * HEADS, ROWS), F32), pltpu.VMEM((5, INNER), BF16),
-            pltpu.VMEM((5, 2, STATE), BF16), pltpu.SemaphoreType.DMA((4,)),
-        ],
+        + [pltpu.VMEM((STATE, INNER), F32)] * 2,
         size=8, flops=6e9,
     )(decay_rate, rows, raw, halo_low, halo_high, gain, inner_weight, input_map, output_map, conv_inner, conv_pair,
       jump, spread)
@@ -652,15 +642,10 @@
 
     near, far = rope_tables()
     gate, qs, ks, vs = plain(
-        heads_kernel, "heads", 8,
+        heads_kernel, "heads", 10,
         [
             shaped((ROWS, INNER), BF16), shaped((QHEADS * HEAD, ROWS), BF16), shaped((HEAD, ROWS + 2 * WINDOW), BF16),
             shaped((HEAD, ROWS + 2 * WINDOW), BF16),
-        ],
-        remote=2,
-        scratch=[
-            pltpu.VMEM((HEAD, ROWS + 2 * WINDOW), F32), pltpu.VMEM((1, HEAD), F32),
-            pltpu.SemaphoreType.DMA((2,)),
         ],
         size=6, flops=7e9,
     )(normed, halo_low, halo_high, w_gate, w_q, w_kv, query_gain[None, :], key_gain[None, :],

time: 81.1 us -> 80.6 us (level)
  transfers between devices with their start and end apart: 17 -> 17, of which waited for: 7 -> 7; matrix products, arithmetic and copies ran while one was open for 0% -> 0% of each run, Pallas kernels for 42% -> 41%
where the time goes in v3:
time: 80.6 us; the launch traced here: 80 us
  Pallas kernels  36.6 us (45%)
  starting transfers between devices  30.7 us (38%)
  waiting for transfers between devices  12.2 us (15%)
    ppermute x6, starting transfers between devices, along(): lax.ppermute(values[d - 1], axis, [(k, (k + d) % LINE) for k in range(LIN...  13.1 us
    ppermute x3, waiting for transfers between devices, local(): shift_right = lambda value: lax.ppermute(value, 'x', right)  8.69 us
    ppermute x3, starting transfers between devices, local(): shift_left = lambda value: lax.ppermute(value, 'x', left)  8.31 us
    pallas_call x1, Pallas kernels, local(): plain(front_kernel, 'front', 5, [shaped((ROWS, WIDTH), BF16), shaped((CON...  6.15 us
    pallas_call x1, Pallas kernels, local(): plain(mixer_kernel, 'mixer', 8, [shaped((ROWS, INNER), F32)], scratch=[pl...  5.87 us
    pallas_call x1, Pallas kernels, local(): plain(state_kernel, 'state', 12, [shaped((ROWS, INNER), BF16), shaped((RO...  5.76 us
    pallas_call x1, Pallas kernels, local(): plain(heads_kernel, 'heads', 10, [shaped((ROWS, INNER), BF16), shaped((QH...  4.88 us
    pallas_call x1, Pallas kernels, local(): plain(attend_kernel, 'attend', 3, [shaped((ROWS, QHEADS * HEAD), BF16)],...  4.41 us
  transfers between devices with their start and end apart: 17, of which 7 were waited for; matrix products, arithmetic and copies ran while one was open for 0% of the time, Pallas kernels for 41%

profile of v3, /device:TPU:1, one launch (start us, length us, event | category | flops | bytes accessed | tf_op | source)
XLA Modules:
  0.0 80.0 jit_solution(8816541266377142160)
XLA Ops:
  0.0 2.3 %edge.1 = (bf16[24,2048]{1,0:T(8,128)(2,1)S(1)}, bf16[24,2048]{1,0:T(8,128)(2,1)S(1)}) custom-call(bf16[16,128]{1,0:T(8,128)(2,1)} %bitcast.15, bf16[1024,2048]{1,0:T(8,128)(2,1)} %tok.3, bf16[64,2048]{1,0:T(8,128)(2,1)} %bitcast.20, bf16[64,2048]{1,0:T(8,128)(2,1)} %bitcast.22), custom_call_target="tpu_custom_call" | custom-call | flops 10000000000 | bytes 8388608 | tf_op jit(solution)/shard_map/edge/pallas_call | solution.py:589
  2.3 4.3 %collective-permute-start = (bf16[24,2048]{1,0:T(8,128)(2,1)S(1)}, bf16[24,2048]{1,0:T(8,128)(2,1)S(1)}, u32[]{:S(2)}, u32[]{:S(2)}) collective-permute-start(bf16[24,2048]{1,0:T(8,128)(2,1)S(1)} %get-tuple-element.44), channel_id=1, source_target_pairs={{0,8},{8,16},{16,24},{24,32},{32,40},{40,48},{48,56},{56,64},{64,7... | collective-permute-start | bytes 294920 | tf_op jit(solution)/shard_map/ppermute | solution.py:597
  6.6 1.3 %collective-permute-start.1 = (bf16[24,2048]{1,0:T(8,128)(2,1)S(1)}, bf16[24,2048]{1,0:T(8,128)(2,1)S(1)}, u32[]{:S(2)}, u32[]{:S(2)}) collective-permute-start(bf16[24,2048]{1,0:T(8,128)(2,1)S(1)} %get-tuple-element.45), channel_id=1, source_target_pairs={{8,0},{16,8},{24,16},{32,24},{40,32},{48,40},{56,48},{64,56},{72,6... | collective-permute-start | bytes 294920 | tf_op jit(solution)/shard_map/ppermute | solution.py:598
  7.9 1.0 %collective-permute-start.10 = (bf16[512,2048]{1,0:T(8,128)(2,1)S(1)}, bf16[512,2048]{1,0:T(8,128)(2,1)S(1)}, u32[]{:S(2)}, u32[]{:S(2)}) collective-permute-start(bf16[512,2048]{1,0:T(8,128)(2,1)S(1)} %copy-done), channel_id=1, source_target_pairs={{0,1},{1,0},{2,3},{3,2},{4,5},{5,4},{6,7},{7,6},{8,9},{9,8},{10,11... | collective-permute-start | bytes 6291464 | tf_op jit(solution)/shard_map/ppermute | solution.py:600
  9.2 6.2 %front.1 = (bf16[1024,2048]{1,0:T(8,128)(2,1)S(1)}, f32[6,1024,128]{2,1,0:T(8,128)S(1)}, f32[16,1024]{1,0:T(8,128)S(1)}, bf16[2048,512]{1,0:T(8,128)(2,1)S(1)}, ...) custom-call(bf16[16,128]{1,0:T(8,128)(2,1)S(1)} %bitcast.16, bf16[2048,512]{1,0:T(8,128)(2,1)S(1)} %copy-done.5, ...), custom_call_target="tpu_custom_call" | custom-call | flops 10000000000 | bytes 8388608 | tf_op jit(solution)/shard_map/front/pallas_call | solution.py:605
  15.4 5.8 %state.1 = (bf16[1024,512]{1,0:T(8,128)(2,1)S(1)}, bf16[1024,128]{1,0:T(8,128)(2,1)S(1)}, bf16[1024,128]{1,0:T(8,128)(2,1)S(1)}, f32[16,1024]{1,0:T(8,128)S(1)},...) custom-call(f32[2,8]{1,0:T(2,128)S(1)} %copy-done.12, ...), custom_call_target="tpu_custom_call" | custom-call | flops 6000000000 | bytes 8388608 | tf_op jit(solution)/shard_map/state/pallas_call | solution.py:618
  21.2 2.4 %collective-permute-start.2 = (bf16[272,512]{1,0:T(8,128)(2,1)S(1)}, bf16[272,512]{1,0:T(8,128)(2,1)S(1)}, u32[]{:S(2)}, u32[]{:S(2)}) collective-permute-start(bf16[272,512]{1,0:T(8,128)(2,1)S(1)} %get-tuple-element.62.own), channel_id=1, source_target_pairs={{0,8},{8,16},{16,24},{24,0},{1,9},{9,17},{17,25},{25,1},{2,10},{10... | collective-permute-start | bytes 835592 | tf_op jit(solution)/shard_map/ppermute | solution.py:636
  23.6 2.6 %collective-permute-start.3 = (bf16[272,512]{1,0:T(8,128)(2,1)S(1)}, bf16[272,512]{1,0:T(8,128)(2,1)S(1)}, u32[]{:S(2)}, u32[]{:S(2)}) collective-permute-start(bf16[272,512]{1,0:T(8,128)(2,1)S(1)} %get-tuple-element.62.own), channel_id=1, source_target_pairs={{0,16},{8,24},{16,0},{24,8},{1,17},{9,25},{17,1},{25,9},{2,18},{10... | collective-permute-start | bytes 835592 | tf_op jit(solution)/shard_map/ppermute | solution.py:636
  26.2 1.1 %collective-permute-start.4 = (bf16[272,512]{1,0:T(8,128)(2,1)S(1)}, bf16[272,512]{1,0:T(8,128)(2,1)S(1)}, u32[]{:S(2)}, u32[]{:S(2)}) collective-permute-start(bf16[272,512]{1,0:T(8,128)(2,1)S(1)} %get-tuple-element.62.own), channel_id=1, source_target_pairs={{0,24},{8,0},{16,8},{24,16},{1,25},{9,1},{17,9},{25,17},{2,26},{10... | collective-permute-start | bytes 835592 | tf_op jit(solution)/shard_map/ppermute | solution.py:636
  27.3 5.9 %mixer.1.y = f32[1024,512]{1,0:T(8,128)S(1)} custom-call(bf16[1024,512]{1,0:T(8,128)(2,1)S(1)} %get-tuple-element.46.x_ref, bf16[1024,128]{1,0:T(8,128)(2,1)S(1)} %get-tuple-element.47.b_ref, bf16[1024,128]{1,0:T(8,128)(2,1)S(1)} %get-tuple-element.48.c_ref.c, f32[16,1024]{1,0:T(8,128)S(1)} %get-tuple-element.49.cum_ref, ...), custom_call_target="tpu_custom_call" | custom-call | flops 10000000000 | bytes 8388608 | tf_op jit(solution)/shard_map/mixer/pallas_call | solution.py:669
  33.2 4.9 %heads.1 = (bf16[1024,512]{1,0:T(8,128)(2,1)S(1)}, bf16[256,1024]{1,0:T(8,128)(2,1)S(1)}, bf16[64,1280]{1,0:T(8,128)(2,1)S(1)}, bf16[64,1280]{1,0:T(8,128)(2,1)S(1)}) custom-call(bf16[1024,2048]{1,0:T(8,128)(2,1)S(1)} %get-tuple-element.54.normed, bf16[24,2048]{1,0:T(8,128)(2,1)S(1)} %collective-permute-done.low, ...), custom_call_target="tpu_custom_call" | custom-call | flops 7000000000 | bytes 8388608 | tf_op jit(solution)/shard_map/heads/pallas_call | solution.py:644
  38.9 3.0 %collective-permute-start.5 = (bf16[144,512]{1,0:T(8,128)(2,1)S(1)}, bf16[144,512]{1,0:T(8,128)(2,1)S(1)}, u32[]{:S(2)}, u32[]{:S(2)}) collective-permute-start(bf16[144,512]{1,0:T(8,128)(2,1)S(1)} %get-tuple-element.64), channel_id=1, source_target_pairs={{0,32},{32,64},{64,96},{96,0},{1,33},{33,65},{65,97},{97,1},{2,34}... | collective-permute-start | bytes 442376 | tf_op jit(solution)/shard_map/ppermute | solution.py:636
  41.9 3.3 %collective-permute-start.6 = (bf16[144,512]{1,0:T(8,128)(2,1)S(1)}, bf16[144,512]{1,0:T(8,128)(2,1)S(1)}, u32[]{:S(2)}, u32[]{:S(2)}) collective-permute-start(bf16[144,512]{1,0:T(8,128)(2,1)S(1)} %get-tuple-element.65), channel_id=1, source_target_pairs={{0,64},{32,96},{64,0},{96,32},{1,65},{33,97},{65,1},{97,33},{2,66}... | collective-permute-start | bytes 442376 | tf_op jit(solution)/shard_map/ppermute | solution.py:636
  45.9 4.4 %attend.1.attn = bf16[1024,256]{1,0:T(8,128)(2,1)S(1)} custom-call(f32[4]{0:T(128)S(1)} %copy-done.15, bf16[256,1024]{1,0:T(8,128)(2,1)S(1)} %get-tuple-element.59.qs, bf16[64,1280]{1,0:T(8,128)(2,1)S(1)} %get-tuple-element.60.ks, bf16[64,1280]{1,0:T(8,128)(2,1)S(1)} %get-tuple-element.61.vs), custom_call_target="tpu_custom_call" | custom-call | flops 7000000000 | bytes 8388608 | tf_op jit(solution)/shard_map/attend/pallas_call | solution.py:662
  51.1 1.1 %theirs.1 = (bf16[4,128,768]{2,1,0:T(8,128)(2,1)S(1)}, bf16[128,512]{1,0:T(8,128)(2,1)S(1)}, bf16[128,512]{1,0:T(8,128)(2,1)S(1)}) custom-call(f32[272,512]{1,0:T(8,128)S(1)} %get-tuple-element.63.part, bf16[144,512]{1,0:T(8,128)(2,1)S(1)} %collective-permute-done.5.d1, bf16[144,512]{1,0:T(8,128)(2,1)S(1)} %collective-permute-done.6.d2, ...), custom_call_target="tpu_custom_call" | custom-call | flops 2000000000 | bytes 8388608 | tf_op jit(solution)/shard_map/theirs/pallas_call | solution.py:677
  52.1 2.2 %collective-permute-start.8 = (bf16[4,128,768]{2,1,0:T(8,128)(2,1)S(1)}, bf16[4,128,768]{2,1,0:T(8,128)(2,1)S(1)}, u32[]{:S(2)}, u32[]{:S(2)}) collective-permute-start(bf16[4,128,768]{2,1,0:T(8,128)(2,1)S(1)} %get-tuple-element.70), channel_id=1, source_target_pairs={{0,1},{1,0},{2,3},{3,2},{4,5},{5,4},{6,7},{7,6},{8,9},{9,8},{10,11... | collective-permute-start | bytes 2359304 | tf_op jit(solution)/shard_map/ppermute | solution.py:680
  54.3 1.5 %mine.1 = (bf16[4,128,768]{2,1,0:T(8,128)(2,1)S(1)}, f32[128,2048]{1,0:T(8,128)S(1)}) custom-call(f32[1024,512]{1,0:T(8,128)S(1)} %mixer.1.y, bf16[1024,128]{1,0:T(8,128)(2,1)S(1)} %get-tuple-element.48.c_ref.c, f32[16,1024]{1,0:T(8,128)S(1)} %get-tuple-element.53.run, bf16[1024,512]{1,0:T(8,128)(2,1)S(1)} %get-tuple-element.58.gate, ...), custom_call_target="tpu_custom_call" | custom-call | flops 2000000000 | bytes 8388608 | tf_op jit(solution)/shard_map/mine/pallas_call | solution.py:681
  56.9 2.5 %collective-permute-start.15 = (bf16[64,2048]{1,0:T(8,128)(2,1)S(1)}, bf16[64,2048]{1,0:T(8,128)(2,1)S(1)}, u32[]{:S(2)}, u32[]{:S(2)}) collective-permute-start(bf16[64,2048]{1,0:T(8,128)(2,1)S(1)} %get-tuple-element.78), channel_id=1, source_target_pairs={{2,0},{4,2},{6,4},{0,6},{3,1},{5,3},{7,5},{1,7},{10,8},{12,10},{14... | collective-permute-start | bytes 786440 | tf_op jit(solution)/shard_map/ppermute | solution.py:692
  59.4 2.7 %beside.1 = (bf16[64,2048]{1,0:T(8,128)(2,1)S(1)}, bf16[64,2048]{1,0:T(8,128)(2,1)S(1)}, f32[64,2048]{1,0:T(8,128)S(1)}, f32[64,2048]{1,0:T(8,128)S(1)}, f32[128,2048]{1,0:T(8,128)S(1)}) custom-call(bf16[4,128,768]{2,1,0:T(8,128)(2,1)S(1)} %get-tuple-element.69.mine, bf16[4,128,768]{2,1,0:T(8,128)(2,1)S(1)} %collective-permute-done.8.theirs, ...), custom_call_target="tpu_custom_call" | custom-call | flops 3000000000 | bytes 8388608 | tf_op jit(solution)/shard_map/beside/pallas_call | solution.py:698
  62.4 2.5 %collective-permute-start.12 = (bf16[64,2048]{1,0:T(8,128)(2,1)S(1)}, bf16[64,2048]{1,0:T(8,128)(2,1)S(1)}, u32[]{:S(2)}, u32[]{:S(2)}) collective-permute-start(bf16[64,2048]{1,0:T(8,128)(2,1)S(1)} %get-tuple-element.73), channel_id=1, source_target_pairs={{2,0},{4,2},{6,4},{0,6},{3,1},{5,3},{7,5},{1,7},{10,8},{12,10},{14... | collective-permute-start | bytes 786440 | tf_op jit(solution)/shard_map/ppermute | solution.py:692
  65.0 3.2 %collective-permute-start.16 = (bf16[64,2048]{1,0:T(8,128)(2,1)S(1)}, bf16[64,2048]{1,0:T(8,128)(2,1)S(1)}, u32[]{:S(2)}, u32[]{:S(2)}) collective-permute-start(bf16[64,2048]{1,0:T(8,128)(2,1)S(1)} %add_convert_fusion), channel_id=1, source_target_pairs={{2,0},{4,2},{6,4},{0,6},{3,1},{5,3},{7,5},{1,7},{10,8},{12,10},{14... | collective-permute-start | bytes 786440 | tf_op jit(solution)/shard_map/ppermute | solution.py:692
  68.4 5.1 %collective-permute-done.11.direct_right = bf16[64,2048]{1,0:T(8,128)(2,1)S(1)} collective-permute-done((bf16[64,2048]{1,0:T(8,128)(2,1)S(1)}, bf16[64,2048]{1,0:T(8,128)(2,1)S(1)}, u32[]{:S(2)}, u32[]{:S(2)}) %collective-permute-start.11) | collective-permute-done | bytes 262176 | tf_op jit(solution)/shard_map/ppermute | solution.py:691
  73.5 2.0 %collective-permute-done.16.last_left = bf16[64,2048]{1,0:T(8,128)(2,1)S(1)} collective-permute-done((bf16[64,2048]{1,0:T(8,128)(2,1)S(1)}, bf16[64,2048]{1,0:T(8,128)(2,1)S(1)}, u32[]{:S(2)}, u32[]{:S(2)}) %collective-permute-start.16) | collective-permute-done | bytes 262176 | tf_op jit(solution)/shard_map/ppermute | solution.py:692
  75.5 3.6 %collective-permute-done.14.last_right = bf16[64,2048]{1,0:T(8,128)(2,1)S(1)} collective-permute-done((bf16[64,2048]{1,0:T(8,128)(2,1)S(1)}, bf16[64,2048]{1,0:T(8,128)(2,1)S(1)}, u32[]{:S(2)}, u32[]{:S(2)}) %collective-permute-start.14) | collective-permute-done | bytes 262176 | tf_op jit(solution)/shard_map/ppermute | solution.py:691
  (60 shorter events, 4.9 us)
Async XLA Ops:
  0.0 7.9 %copy-start = (bf16[512,2048]{1,0:T(8,128)(2,1)S(1)}, bf16[512,2048]{1,0:T(8,128)(2,1)}, u32[]{:S(2)}) copy-start(bf16[512,2048]{1,0:T(8,128)(2,1)} %ws.3) | copy-start | bytes 6291460
  0.0 9.0 %copy-start.1 = (bf16[256,2048]{1,0:T(8,128)(2,1)S(1)}, bf16[256,2048]{1,0:T(8,128)(2,1)}, u32[]{:S(2)}) copy-start(bf16[256,2048]{1,0:T(8,128)(2,1)} %wa.3) | copy-start | bytes 3145732
  0.0 9.1 %copy-start.4 = (bf16[1024,2048]{1,0:T(8,128)(2,1)S(1)}, bf16[1024,2048]{1,0:T(8,128)(2,1)}, u32[]{:S(2)}) copy-start(bf16[1024,2048]{1,0:T(8,128)(2,1)} %tok.3) | copy-start | bytes 12582916
  0.0 9.1 %copy-start.5 = (bf16[2048,512]{1,0:T(8,128)(2,1)S(1)}, bf16[2048,512]{1,0:T(8,128)(2,1)}, u32[]{:S(2)}) copy-start(bf16[2048,512]{1,0:T(8,128)(2,1)} %w_inner.3) | copy-start | bytes 6291460
  0.0 9.1 %copy-start.6 = (bf16[2048,128]{1,0:T(8,128)(2,1)S(1)}, bf16[2048,128]{1,0:T(8,128)(2,1)}, u32[]{:S(2)}) copy-start(bf16[2048,128]{1,0:T(8,128)(2,1)} %w_in.3) | copy-start | bytes 1572868
  0.0 9.0 %copy-start.7 = (bf16[2048,128]{1,0:T(8,128)(2,1)S(1)}, bf16[2048,128]{1,0:T(8,128)(2,1)}, u32[]{:S(2)}) copy-start(bf16[2048,128]{1,0:T(8,128)(2,1)} %w_out.3) | copy-start | bytes 1572868
  0.0 9.0 %copy-start.10 = (bf16[2048]{0:T(1024)(128)(2,1)S(1)}, bf16[2048]{0:T(1024)(128)(2,1)}, u32[]{:S(2)}) copy-start(bf16[2048]{0:T(1024)(128)(2,1)} %param.24) | copy-start | bytes 12292
  2.3 13.0 %collective-permute-start = (bf16[24,2048]{1,0:T(8,128)(2,1)S(1)}, bf16[24,2048]{1,0:T(8,128)(2,1)S(1)}, u32[]{:S(2)}, u32[]{:S(2)}) collective-permute-start(bf16[24,2048]{1,0:T(8,128)(2,1)S(1)} %get-tuple-element.44), channel_id=1, source_target_pairs={{0,8},{8,16},{16,24},{24,32},{32,40},{40,48},{48,56},{56,64},{64,7... | collective-permute-start | bytes 294920 | tf_op jit(solution)/shard_map/ppermute | solution.py:597
  6.6 8.7 %collective-permute-start.1 = (bf16[24,2048]{1,0:T(8,128)(2,1)S(1)}, bf16[24,2048]{1,0:T(8,128)(2,1)S(1)}, u32[]{:S(2)}, u32[]{:S(2)}) collective-permute-start(bf16[24,2048]{1,0:T(8,128)(2,1)S(1)} %get-tuple-element.45), channel_id=1, source_target_pairs={{8,0},{16,8},{24,16},{32,24},{40,32},{48,40},{56,48},{64,56},{72,6... | collective-permute-start | bytes 294920 | tf_op jit(solution)/shard_map/ppermute | solution.py:598
  7.9 48.3 %collective-permute-start.10 = (bf16[512,2048]{1,0:T(8,128)(2,1)S(1)}, bf16[512,2048]{1,0:T(8,128)(2,1)S(1)}, u32[]{:S(2)}, u32[]{:S(2)}) collective-permute-start(bf16[512,2048]{1,0:T(8,128)(2,1)S(1)} %copy-done), channel_id=1, source_target_pairs={{0,1},{1,0},{2,3},{3,2},{4,5},{5,4},{6,7},{7,6},{8,9},{9,8},{10,11... | collective-permute-start | bytes 6291464 | tf_op jit(solution)/shard_map/ppermute | solution.py:600
  9.0 46.9 %collective-permute-start.9 = (bf16[256,2048]{1,0:T(8,128)(2,1)S(1)}, bf16[256,2048]{1,0:T(8,128)(2,1)S(1)}, u32[]{:S(2)}, u32[]{:S(2)}) collective-permute-start(bf16[256,2048]{1,0:T(8,128)(2,1)S(1)} %copy-done.1), channel_id=1, source_target_pairs={{0,1},{1,0},{2,3},{3,2},{4,5},{5,4},{6,7},{7,6},{8,9},{9,8},{10,11... | collective-permute-start | bytes 3145736 | tf_op jit(solution)/shard_map/ppermute | solution.py:599
  21.2 16.9 %collective-permute-start.2 = (bf16[272,512]{1,0:T(8,128)(2,1)S(1)}, bf16[272,512]{1,0:T(8,128)(2,1)S(1)}, u32[]{:S(2)}, u32[]{:S(2)}) collective-permute-start(bf16[272,512]{1,0:T(8,128)(2,1)S(1)} %get-tuple-element.62.own), channel_id=1, source_target_pairs={{0,8},{8,16},{16,24},{24,0},{1,9},{9,17},{17,25},{25,1},{2,10},{10... | collective-permute-start | bytes 835592 | tf_op jit(solution)/shard_map/ppermute | solution.py:636
  23.6 14.9 %collective-permute-start.3 = (bf16[272,512]{1,0:T(8,128)(2,1)S(1)}, bf16[272,512]{1,0:T(8,128)(2,1)S(1)}, u32[]{:S(2)}, u32[]{:S(2)}) collective-permute-start(bf16[272,512]{1,0:T(8,128)(2,1)S(1)} %get-tuple-element.62.own), channel_id=1, source_target_pairs={{0,16},{8,24},{16,0},{24,8},{1,17},{9,25},{17,1},{25,9},{2,18},{10... | collective-permute-start | bytes 835592 | tf_op jit(solution)/shard_map/ppermute | solution.py:636
  26.2 12.3 %collective-permute-start.4 = (bf16[272,512]{1,0:T(8,128)(2,1)S(1)}, bf16[272,512]{1,0:T(8,128)(2,1)S(1)}, u32[]{:S(2)}, u32[]{:S(2)}) collective-permute-start(bf16[272,512]{1,0:T(8,128)(2,1)S(1)} %get-tuple-element.62.own), channel_id=1, source_target_pairs={{0,24},{8,0},{16,8},{24,16},{1,25},{9,1},{17,9},{25,17},{2,26},{10... | collective-permute-start | bytes 835592 | tf_op jit(solution)/shard_map/ppermute | solution.py:636
  38.9 11.4 %collective-permute-start.5 = (bf16[144,512]{1,0:T(8,128)(2,1)S(1)}, bf16[144,512]{1,0:T(8,128)(2,1)S(1)}, u32[]{:S(2)}, u32[]{:S(2)}) collective-permute-start(bf16[144,512]{1,0:T(8,128)(2,1)S(1)} %get-tuple-element.64), channel_id=1, source_target_pairs={{0,32},{32,64},{64,96},{96,0},{1,33},{33,65},{65,97},{97,1},{2,34}... | collective-permute-start | bytes 442376 | tf_op jit(solution)/shard_map/ppermute | solution.py:636
  41.9 8.6 %collective-permute-start.6 = (bf16[144,512]{1,0:T(8,128)(2,1)S(1)}, bf16[144,512]{1,0:T(8,128)(2,1)S(1)}, u32[]{:S(2)}, u32[]{:S(2)}) collective-permute-start(bf16[144,512]{1,0:T(8,128)(2,1)S(1)} %get-tuple-element.65), channel_id=1, source_target_pairs={{0,64},{32,96},{64,0},{96,32},{1,65},{33,97},{65,1},{97,33},{2,66}... | collective-permute-start | bytes 442376 | tf_op jit(solution)/shard_map/ppermute | solution.py:636
  45.2 5.9 %collective-permute-start.7 = (bf16[144,512]{1,0:T(8,128)(2,1)S(1)}, bf16[144,512]{1,0:T(8,128)(2,1)S(1)}, u32[]{:S(2)}, u32[]{:S(2)}) collective-permute-start(bf16[144,512]{1,0:T(8,128)(2,1)S(1)} %get-tuple-element.66), channel_id=1, source_target_pairs={{0,96},{32,0},{64,32},{96,64},{1,97},{33,1},{65,33},{97,65},{2,98}... | collective-permute-start | bytes 442376 | tf_op jit(solution)/shard_map/ppermute | solution.py:636
  52.1 4.1 %collective-permute-start.8 = (bf16[4,128,768]{2,1,0:T(8,128)(2,1)S(1)}, bf16[4,128,768]{2,1,0:T(8,128)(2,1)S(1)}, u32[]{:S(2)}, u32[]{:S(2)}) collective-permute-start(bf16[4,128,768]{2,1,0:T(8,128)(2,1)S(1)} %get-tuple-element.70), channel_id=1, source_target_pairs={{0,1},{1,0},{2,3},{3,2},{4,5},{5,4},{6,7},{7,6},{8,9},{9,8},{10,11... | collective-permute-start | bytes 2359304 | tf_op jit(solution)/shard_map/ppermute | solution.py:680
  56.9 8.1 %collective-permute-start.15 = (bf16[64,2048]{1,0:T(8,128)(2,1)S(1)}, bf16[64,2048]{1,0:T(8,128)(2,1)S(1)}, u32[]{:S(2)}, u32[]{:S(2)}) collective-permute-start(bf16[64,2048]{1,0:T(8,128)(2,1)S(1)} %get-tuple-element.78), channel_id=1, source_target_pairs={{2,0},{4,2},{6,4},{0,6},{3,1},{5,3},{7,5},{1,7},{10,8},{12,10},{14... | collective-permute-start | bytes 786440 | tf_op jit(solution)/shard_map/ppermute | solution.py:692
  59.4 8.8 %collective-permute-start.13 = (bf16[64,2048]{1,0:T(8,128)(2,1)S(1)}, bf16[64,2048]{1,0:T(8,128)(2,1)S(1)}, u32[]{:S(2)}, u32[]{:S(2)}) collective-permute-start(bf16[64,2048]{1,0:T(8,128)(2,1)S(1)} %get-tuple-element.76), channel_id=1, source_target_pairs={{0,2},{2,4},{4,6},{6,0},{1,3},{3,5},{5,7},{7,1},{8,10},{10,12},{12... | collective-permute-start | bytes 786440 | tf_op jit(solution)/shard_map/ppermute | solution.py:691
  62.1 11.3 %collective-permute-start.11 = (bf16[64,2048]{1,0:T(8,128)(2,1)S(1)}, bf16[64,2048]{1,0:T(8,128)(2,1)S(1)}, u32[]{:S(2)}, u32[]{:S(2)}) collective-permute-start(bf16[64,2048]{1,0:T(8,128)(2,1)S(1)} %get-tuple-element.72), channel_id=1, source_target_pairs={{0,2},{2,4},{4,6},{6,0},{1,3},{3,5},{5,7},{7,1},{8,10},{10,12},{12... | collective-permute-start | bytes 786440 | tf_op jit(solution)/shard_map/ppermute | solution.py:691
  62.4 11.0 %collective-permute-start.12 = (bf16[64,2048]{1,0:T(8,128)(2,1)S(1)}, bf16[64,2048]{1,0:T(8,128)(2,1)S(1)}, u32[]{:S(2)}, u32[]{:S(2)}) collective-permute-start(bf16[64,2048]{1,0:T(8,128)(2,1)S(1)} %get-tuple-element.73), channel_id=1, source_target_pairs={{2,0},{4,2},{6,4},{0,6},{3,1},{5,3},{7,5},{1,7},{10,8},{12,10},{14... | collective-permute-start | bytes 786440 | tf_op jit(solution)/shard_map/ppermute | solution.py:692
  65.0 10.5 %collective-permute-start.16 = (bf16[64,2048]{1,0:T(8,128)(2,1)S(1)}, bf16[64,2048]{1,0:T(8,128)(2,1)S(1)}, u32[]{:S(2)}, u32[]{:S(2)}) collective-permute-start(bf16[64,2048]{1,0:T(8,128)(2,1)S(1)} %add_convert_fusion), channel_id=1, source_target_pairs={{2,0},{4,2},{6,4},{0,6},{3,1},{5,3},{7,5},{1,7},{10,8},{12,10},{14... | collective-permute-start | bytes 786440 | tf_op jit(solution)/shard_map/ppermute | solution.py:692
  68.3 10.8 %collective-permute-start.14 = (bf16[64,2048]{1,0:T(8,128)(2,1)S(1)}, bf16[64,2048]{1,0:T(8,128)(2,1)S(1)}, u32[]{:S(2)}, u32[]{:S(2)}) collective-permute-start(bf16[64,2048]{1,0:T(8,128)(2,1)S(1)} %add_convert_fusion.1), channel_id=1, source_target_pairs={{0,2},{2,4},{4,6},{6,0},{1,3},{3,5},{5,7},{7,1},{8,10},{10,12},{12... | collective-permute-start | bytes 786440 | tf_op jit(solution)/shard_map/ppermute | solution.py:691
  (11 other events, 67.8 us)

commit v4 on v3

--- a/solution.py
+++ b/solution.py
@@ -596,8 +596,6 @@
     )(*map(pin, (gain, tokens, key_weight.T, value_weight.T)))
     halo_low = lax.ppermute(edge_low, SP, up)
     halo_high = lax.ppermute(edge_high, SP, down)
-    attn_partner = lax.ppermute(attn_out_weight, "c", swap)
-    ssm_partner = lax.ppermute(ssm_out_weight, "c", swap)
 
     spread = jnp.asarray(head_spread(), BF16)
     step_rows = jnp.transpose(step_weight, (1, 2, 0)).reshape(2 * HEADS, WIDTH)
@@ -670,6 +668,10 @@
         mixer_kernel, "mixer", 8, [shaped((ROWS, INNER), F32)],
         scratch=[pltpu.VMEM((STATE, INNER), F32)], flops=10e9,
     )(x, b, c, cum, step, enter, back, spread)[0]
+
+    attn_own, ssm_own, y = lax.optimization_barrier((attn_out_weight, ssm_out_weight, y))
+    attn_partner = lax.ppermute(attn_own, "c", swap)
+    ssm_partner = lax.ppermute(ssm_own, "c", swap)
 
     depth = QHEADS * HEAD + INNER
     rest = (y, c, run, gate, attn, inner_gain.reshape(INNER // 128, 128), spread)

time: 80.6 us -> 77.6 us (0.963)
  starting transfers between devices: 30.7 us -> 28 us
    ppermute x6, starting transfers between devices: 13.1 us -> 10.4 us  [along(): lax.ppermute(values[d - 1], axis, [(k, (k + d) % LINE) for k in range(LIN...]
    ppermute x6, waiting for transfers between devices: 1.12 us -> 3.29 us  [along(): lax.ppermute(values[d - 1], axis, [(k, (k + d) % LINE) for k in range(LIN...]
    ppermute x3, waiting for transfers between devices: 2.01 us -> 0.15 us  [local(): shift_left = lambda value: lax.ppermute(value, 'x', left)]
    ppermute x3, starting transfers between devices: 8.31 us -> 6.96 us  [local(): shift_left = lambda value: lax.ppermute(value, 'x', left)]
    ppermute x2, starting transfers between devices: 1.14 us -> 2.41 us  [the longest x1 2.13 us: local(): attn_partner = lax.ppermute(attn_own, 'c', swap)]
    ppermute x3, starting transfers between devices: 0.38 us -> 1.43 us  [local(): shift_right = lambda value: lax.ppermute(value, 'x', right)]
  transfers between devices with their start and end apart: 17 -> 17, of which waited for: 7 -> 8; matrix products, arithmetic and copies ran while one was open for 0% -> 0% of each run, Pallas kernels for 41% -> 35%
where the time goes in v4:
time: 77.6 us; the launch traced here: 77.1 us
  Pallas kernels  36.3 us (47%)
  starting transfers between devices  28 us (36%)
  waiting for transfers between devices  12.2 us (16%)
    ppermute x6, starting transfers between devices, along(): lax.ppermute(values[d - 1], axis, [(k, (k + d) % LINE) for k in range(LIN...  10.4 us
    ppermute x3, waiting for transfers between devices, local(): shift_right = lambda value: lax.ppermute(value, 'x', right)  8.35 us
    ppermute x3, starting transfers between devices, local(): shift_left = lambda value: lax.ppermute(value, 'x', left)  6.96 us
    pallas_call x1, Pallas kernels, local(): plain(front_kernel, 'front', 5, [shaped((ROWS, WIDTH), BF16), shaped((CON...  6.02 us
    pallas_call x1, Pallas kernels, local(): plain(mixer_kernel, 'mixer', 8, [shaped((ROWS, INNER), F32)], scratch=[pl...  5.8 us
    pallas_call x1, Pallas kernels, local(): plain(state_kernel, 'state', 12, [shaped((ROWS, INNER), BF16), shaped((RO...  5.77 us
    pallas_call x1, Pallas kernels, local(): plain(heads_kernel, 'heads', 10, [shaped((ROWS, INNER), BF16), shaped((QH...  4.85 us
    pallas_call x1, Pallas kernels, local(): plain(attend_kernel, 'attend', 3, [shaped((ROWS, QHEADS * HEAD), BF16)],...  4.4 us
  transfers between devices with their start and end apart: 17, of which 8 were waited for; matrix products, arithmetic and copies ran while one was open for 0% of the time, Pallas kernels for 35%

profile of v4, /device:TPU:1, one launch (start us, length us, event | category | flops | bytes accessed | tf_op | source)
XLA Modules:
  0.0 77.1 jit_solution(16799178852845682409)
XLA Ops:
  0.0 2.3 %edge.1 = (bf16[24,2048]{1,0:T(8,128)(2,1)S(1)}, bf16[24,2048]{1,0:T(8,128)(2,1)S(1)}) custom-call(bf16[16,128]{1,0:T(8,128)(2,1)} %bitcast.15, bf16[1024,2048]{1,0:T(8,128)(2,1)} %tok.3, bf16[64,2048]{1,0:T(8,128)(2,1)} %bitcast.20, bf16[64,2048]{1,0:T(8,128)(2,1)} %bitcast.22), custom_call_target="tpu_custom_call" | custom-call | flops 10000000000 | bytes 8388608 | tf_op jit(solution)/shard_map/edge/pallas_call | solution.py:589
  2.3 4.2 %collective-permute-start = (bf16[24,2048]{1,0:T(8,128)(2,1)S(1)}, bf16[24,2048]{1,0:T(8,128)(2,1)S(1)}, u32[]{:S(2)}, u32[]{:S(2)}) collective-permute-start(bf16[24,2048]{1,0:T(8,128)(2,1)S(1)} %get-tuple-element.47), channel_id=1, source_target_pairs={{0,8},{8,16},{16,24},{24,32},{32,40},{40,48},{48,56},{56,64},{64,7... | collective-permute-start | bytes 294920 | tf_op jit(solution)/shard_map/ppermute | solution.py:597
  6.5 1.3 %collective-permute-start.1 = (bf16[24,2048]{1,0:T(8,128)(2,1)S(1)}, bf16[24,2048]{1,0:T(8,128)(2,1)S(1)}, u32[]{:S(2)}, u32[]{:S(2)}) collective-permute-start(bf16[24,2048]{1,0:T(8,128)(2,1)S(1)} %get-tuple-element.48), channel_id=1, source_target_pairs={{8,0},{16,8},{24,16},{32,24},{40,32},{48,40},{56,48},{64,56},{72,6... | collective-permute-start | bytes 294920 | tf_op jit(solution)/shard_map/ppermute | solution.py:598
  7.9 6.0 %front.1 = (bf16[1024,2048]{1,0:T(8,128)(2,1)S(1)}, f32[6,1024,128]{2,1,0:T(8,128)S(1)}, f32[16,1024]{1,0:T(8,128)S(1)}, bf16[2048,512]{1,0:T(8,128)(2,1)S(1)}, ...) custom-call(bf16[16,128]{1,0:T(8,128)(2,1)S(1)} %bitcast.16, bf16[2048,512]{1,0:T(8,128)(2,1)S(1)} %copy-done.5, ...), custom_call_target="tpu_custom_call" | custom-call | flops 10000000000 | bytes 8388608 | tf_op jit(solution)/shard_map/front/pallas_call | solution.py:603
  14.0 5.8 %state.1 = (bf16[1024,512]{1,0:T(8,128)(2,1)S(1)}, bf16[1024,128]{1,0:T(8,128)(2,1)S(1)}, bf16[1024,128]{1,0:T(8,128)(2,1)S(1)}, f32[16,1024]{1,0:T(8,128)S(1)},...) custom-call(f32[2,8]{1,0:T(2,128)S(1)} %copy-done.12, ...), custom_call_target="tpu_custom_call" | custom-call | flops 6000000000 | bytes 8388608 | tf_op jit(solution)/shard_map/state/pallas_call | solution.py:616
  19.7 3.6 %collective-permute-start.4 = (bf16[272,512]{1,0:T(8,128)(2,1)S(1)}, bf16[272,512]{1,0:T(8,128)(2,1)S(1)}, u32[]{:S(2)}, u32[]{:S(2)}) collective-permute-start(bf16[272,512]{1,0:T(8,128)(2,1)S(1)} %get-tuple-element.66.own), channel_id=1, source_target_pairs={{0,24},{8,0},{16,8},{24,16},{1,25},{9,1},{17,9},{25,17},{2,26},{10... | collective-permute-start | bytes 835592 | tf_op jit(solution)/shard_map/ppermute | solution.py:634
  24.4 5.8 %mixer.1.y = f32[1024,512]{1,0:T(8,128)S(1)} custom-call(bf16[1024,512]{1,0:T(8,128)(2,1)S(1)} %get-tuple-element.49.x_ref, bf16[1024,128]{1,0:T(8,128)(2,1)S(1)} %get-tuple-element.50.b_ref, bf16[1024,128]{1,0:T(8,128)(2,1)S(1)} %get-tuple-element.51.c_ref.c, f32[16,1024]{1,0:T(8,128)S(1)} %get-tuple-element.52.cum_ref, ...), custom_call_target="tpu_custom_call" | custom-call | flops 10000000000 | bytes 8388608 | tf_op jit(solution)/shard_map/mixer/pallas_call | solution.py:667
  30.2 2.1 %collective-permute-start.9 = (bf16[256,2048]{1,0:T(8,128)(2,1)S(1)}, bf16[256,2048]{1,0:T(8,128)(2,1)S(1)}, u32[]{:S(2)}, u32[]{:S(2)}) collective-permute-start(bf16[256,2048]{1,0:T(8,128)(2,1)S(1)} %copy-done.1), channel_id=1, source_target_pairs={{0,1},{1,0},{2,3},{3,2},{4,5},{5,4},{6,7},{7,6},{8,9},{9,8},{10,11... | collective-permute-start | bytes 3145736 | tf_op jit(solution)/shard_map/ppermute | solution.py:673
  32.7 4.8 %heads.1 = (bf16[1024,512]{1,0:T(8,128)(2,1)S(1)}, bf16[256,1024]{1,0:T(8,128)(2,1)S(1)}, bf16[64,1280]{1,0:T(8,128)(2,1)S(1)}, bf16[64,1280]{1,0:T(8,128)(2,1)S(1)}) custom-call(bf16[1024,2048]{1,0:T(8,128)(2,1)S(1)} %get-tuple-element.58.normed, bf16[24,2048]{1,0:T(8,128)(2,1)S(1)} %collective-permute-done.low, ...), custom_call_target="tpu_custom_call" | custom-call | flops 7000000000 | bytes 8388608 | tf_op jit(solution)/shard_map/heads/pallas_call | solution.py:642
  37.5 1.8 %collective-permute-done.2.d1 = bf16[272,512]{1,0:T(8,128)(2,1)S(1)} collective-permute-done((bf16[272,512]{1,0:T(8,128)(2,1)S(1)}, bf16[272,512]{1,0:T(8,128)(2,1)S(1)}, u32[]{:S(2)}, u32[]{:S(2)}) %collective-permute-start.2) | collective-permute-done | bytes 278560 | tf_op jit(solution)/shard_map/ppermute | solution.py:634
  39.8 1.7 %collective-permute-start.5 = (bf16[144,512]{1,0:T(8,128)(2,1)S(1)}, bf16[144,512]{1,0:T(8,128)(2,1)S(1)}, u32[]{:S(2)}, u32[]{:S(2)}) collective-permute-start(bf16[144,512]{1,0:T(8,128)(2,1)S(1)} %get-tuple-element.68), channel_id=1, source_target_pairs={{0,32},{32,64},{64,96},{96,0},{1,33},{33,65},{65,97},{97,1},{2,34}... | collective-permute-start | bytes 442376 | tf_op jit(solution)/shard_map/ppermute | solution.py:634
  41.5 3.3 %collective-permute-start.6 = (bf16[144,512]{1,0:T(8,128)(2,1)S(1)}, bf16[144,512]{1,0:T(8,128)(2,1)S(1)}, u32[]{:S(2)}, u32[]{:S(2)}) collective-permute-start(bf16[144,512]{1,0:T(8,128)(2,1)S(1)} %get-tuple-element.69), channel_id=1, source_target_pairs={{0,64},{32,96},{64,0},{96,32},{1,65},{33,97},{65,1},{97,33},{2,66}... | collective-permute-start | bytes 442376 | tf_op jit(solution)/shard_map/ppermute | solution.py:634
  45.6 4.4 %attend.1.attn = bf16[1024,256]{1,0:T(8,128)(2,1)S(1)} custom-call(f32[4]{0:T(128)S(1)} %copy-done.15, bf16[256,1024]{1,0:T(8,128)(2,1)S(1)} %get-tuple-element.63.qs, bf16[64,1280]{1,0:T(8,128)(2,1)S(1)} %get-tuple-element.64.ks, bf16[64,1280]{1,0:T(8,128)(2,1)S(1)} %get-tuple-element.65.vs), custom_call_target="tpu_custom_call" | custom-call | flops 7000000000 | bytes 8388608 | tf_op jit(solution)/shard_map/attend/pallas_call | solution.py:660
  50.0 1.4 %collective-permute-done.6.d2 = bf16[144,512]{1,0:T(8,128)(2,1)S(1)} collective-permute-done((bf16[144,512]{1,0:T(8,128)(2,1)S(1)}, bf16[144,512]{1,0:T(8,128)(2,1)S(1)}, u32[]{:S(2)}, u32[]{:S(2)}) %collective-permute-start.6) | collective-permute-done | bytes 147488 | tf_op jit(solution)/shard_map/ppermute | solution.py:634
  51.4 1.0 %theirs.1 = (bf16[4,128,768]{2,1,0:T(8,128)(2,1)S(1)}, bf16[128,512]{1,0:T(8,128)(2,1)S(1)}, bf16[128,512]{1,0:T(8,128)(2,1)S(1)}) custom-call(f32[272,512]{1,0:T(8,128)S(1)} %get-tuple-element.67.part, bf16[144,512]{1,0:T(8,128)(2,1)S(1)} %collective-permute-done.5.d1, bf16[144,512]{1,0:T(8,128)(2,1)S(1)} %collective-permute-done.6.d2, ...), custom_call_target="tpu_custom_call" | custom-call | flops 2000000000 | bytes 8388608 | tf_op jit(solution)/shard_map/theirs/pallas_call | solution.py:679
  52.5 1.4 %collective-permute-start.8 = (bf16[4,128,768]{2,1,0:T(8,128)(2,1)S(1)}, bf16[4,128,768]{2,1,0:T(8,128)(2,1)S(1)}, u32[]{:S(2)}, u32[]{:S(2)}) collective-permute-start(bf16[4,128,768]{2,1,0:T(8,128)(2,1)S(1)} %get-tuple-element.74), channel_id=1, source_target_pairs={{0,1},{1,0},{2,3},{3,2},{4,5},{5,4},{6,7},{7,6},{8,9},{9,8},{10,11... | collective-permute-start | bytes 2359304 | tf_op jit(solution)/shard_map/ppermute | solution.py:682
  53.9 1.5 %mine.1 = (bf16[4,128,768]{2,1,0:T(8,128)(2,1)S(1)}, f32[128,2048]{1,0:T(8,128)S(1)}) custom-call(f32[1024,512]{1,0:T(8,128)S(1)} %mixer.1.y, bf16[1024,128]{1,0:T(8,128)(2,1)S(1)} %get-tuple-element.51.c_ref.c, f32[16,1024]{1,0:T(8,128)S(1)} %get-tuple-element.57.run, bf16[1024,512]{1,0:T(8,128)(2,1)S(1)} %get-tuple-element.62.gate, ...), custom_call_target="tpu_custom_call" | custom-call | flops 2000000000 | bytes 8388608 | tf_op jit(solution)/shard_map/mine/pallas_call | solution.py:683
  56.4 1.3 %collective-permute-start.13 = (bf16[64,2048]{1,0:T(8,128)(2,1)S(1)}, bf16[64,2048]{1,0:T(8,128)(2,1)S(1)}, u32[]{:S(2)}, u32[]{:S(2)}) collective-permute-start(bf16[64,2048]{1,0:T(8,128)(2,1)S(1)} %get-tuple-element.82), channel_id=1, source_target_pairs={{0,2},{2,4},{4,6},{6,0},{1,3},{3,5},{5,7},{7,1},{8,10},{10,12},{12... | collective-permute-start | bytes 786440 | tf_op jit(solution)/shard_map/ppermute | solution.py:693
  57.7 1.6 %collective-permute-start.15 = (bf16[64,2048]{1,0:T(8,128)(2,1)S(1)}, bf16[64,2048]{1,0:T(8,128)(2,1)S(1)}, u32[]{:S(2)}, u32[]{:S(2)}) collective-permute-start(bf16[64,2048]{1,0:T(8,128)(2,1)S(1)} %get-tuple-element.84), channel_id=1, source_target_pairs={{2,0},{4,2},{6,4},{0,6},{3,1},{5,3},{7,5},{1,7},{10,8},{12,10},{14... | collective-permute-start | bytes 786440 | tf_op jit(solution)/shard_map/ppermute | solution.py:694
  59.3 2.7 %beside.1 = (bf16[64,2048]{1,0:T(8,128)(2,1)S(1)}, bf16[64,2048]{1,0:T(8,128)(2,1)S(1)}, f32[64,2048]{1,0:T(8,128)S(1)}, f32[64,2048]{1,0:T(8,128)S(1)}, f32[128,2048]{1,0:T(8,128)S(1)}) custom-call(bf16[4,128,768]{2,1,0:T(8,128)(2,1)S(1)} %get-tuple-element.73.mine, bf16[4,128,768]{2,1,0:T(8,128)(2,1)S(1)} %collective-permute-done.8.theirs, ...), custom_call_target="tpu_custom_call" | custom-call | flops 3000000000 | bytes 8388608 | tf_op jit(solution)/shard_map/beside/pallas_call | solution.py:700
  62.0 2.7 %collective-permute-start.12 = (bf16[64,2048]{1,0:T(8,128)(2,1)S(1)}, bf16[64,2048]{1,0:T(8,128)(2,1)S(1)}, u32[]{:S(2)}, u32[]{:S(2)}) collective-permute-start(bf16[64,2048]{1,0:T(8,128)(2,1)S(1)} %get-tuple-element.79), channel_id=1, source_target_pairs={{2,0},{4,2},{6,4},{0,6},{3,1},{5,3},{7,5},{1,7},{10,8},{12,10},{14... | collective-permute-start | bytes 786440 | tf_op jit(solution)/shard_map/ppermute | solution.py:694
  65.4 2.7 %collective-permute-start.16 = (bf16[64,2048]{1,0:T(8,128)(2,1)S(1)}, bf16[64,2048]{1,0:T(8,128)(2,1)S(1)}, u32[]{:S(2)}, u32[]{:S(2)}) collective-permute-start(bf16[64,2048]{1,0:T(8,128)(2,1)S(1)} %add_convert_fusion), channel_id=1, source_target_pairs={{2,0},{4,2},{6,4},{0,6},{3,1},{5,3},{7,5},{1,7},{10,8},{12,10},{14... | collective-permute-start | bytes 786440 | tf_op jit(solution)/shard_map/ppermute | solution.py:694
  68.1 2.3 %collective-permute-done.11.direct_right = bf16[64,2048]{1,0:T(8,128)(2,1)S(1)} collective-permute-done((bf16[64,2048]{1,0:T(8,128)(2,1)S(1)}, bf16[64,2048]{1,0:T(8,128)(2,1)S(1)}, u32[]{:S(2)}, u32[]{:S(2)}) %collective-permute-start.11) | collective-permute-done | bytes 262176 | tf_op jit(solution)/shard_map/ppermute | solution.py:693
  70.5 5.5 %collective-permute-done.14.last_right = bf16[64,2048]{1,0:T(8,128)(2,1)S(1)} collective-permute-done((bf16[64,2048]{1,0:T(8,128)(2,1)S(1)}, bf16[64,2048]{1,0:T(8,128)(2,1)S(1)}, u32[]{:S(2)}, u32[]{:S(2)}) %collective-permute-start.14) | collective-permute-done | bytes 262176 | tf_op jit(solution)/shard_map/ppermute | solution.py:693
  (60 shorter events, 5.4 us)
Async XLA Ops:
  0.0 7.8 %copy-start.7 = (bf16[2048,128]{1,0:T(8,128)(2,1)S(1)}, bf16[2048,128]{1,0:T(8,128)(2,1)}, u32[]{:S(2)}) copy-start(bf16[2048,128]{1,0:T(8,128)(2,1)} %w_out.3) | copy-start | bytes 1572868
  2.3 11.6 %collective-permute-start = (bf16[24,2048]{1,0:T(8,128)(2,1)S(1)}, bf16[24,2048]{1,0:T(8,128)(2,1)S(1)}, u32[]{:S(2)}, u32[]{:S(2)}) collective-permute-start(bf16[24,2048]{1,0:T(8,128)(2,1)S(1)} %get-tuple-element.47), channel_id=1, source_target_pairs={{0,8},{8,16},{16,24},{24,32},{32,40},{40,48},{48,56},{56,64},{64,7... | collective-permute-start | bytes 294920 | tf_op jit(solution)/shard_map/ppermute | solution.py:597
  6.5 7.5 %collective-permute-start.1 = (bf16[24,2048]{1,0:T(8,128)(2,1)S(1)}, bf16[24,2048]{1,0:T(8,128)(2,1)S(1)}, u32[]{:S(2)}, u32[]{:S(2)}) collective-permute-start(bf16[24,2048]{1,0:T(8,128)(2,1)S(1)} %get-tuple-element.48), channel_id=1, source_target_pairs={{8,0},{16,8},{24,16},{32,24},{40,32},{48,40},{56,48},{64,56},{72,6... | collective-permute-start | bytes 294920 | tf_op jit(solution)/shard_map/ppermute | solution.py:598
  19.7 17.8 %collective-permute-start.4 = (bf16[272,512]{1,0:T(8,128)(2,1)S(1)}, bf16[272,512]{1,0:T(8,128)(2,1)S(1)}, u32[]{:S(2)}, u32[]{:S(2)}) collective-permute-start(bf16[272,512]{1,0:T(8,128)(2,1)S(1)} %get-tuple-element.66.own), channel_id=1, source_target_pairs={{0,24},{8,0},{16,8},{24,16},{1,25},{9,1},{17,9},{25,17},{2,26},{10... | collective-permute-start | bytes 835592 | tf_op jit(solution)/shard_map/ppermute | solution.py:634
  23.3 14.2 %collective-permute-start.3 = (bf16[272,512]{1,0:T(8,128)(2,1)S(1)}, bf16[272,512]{1,0:T(8,128)(2,1)S(1)}, u32[]{:S(2)}, u32[]{:S(2)}) collective-permute-start(bf16[272,512]{1,0:T(8,128)(2,1)S(1)} %get-tuple-element.66.own), channel_id=1, source_target_pairs={{0,16},{8,24},{16,0},{24,8},{1,17},{9,25},{17,1},{25,9},{2,18},{10... | collective-permute-start | bytes 835592 | tf_op jit(solution)/shard_map/ppermute | solution.py:634
  23.7 15.7 %collective-permute-start.2 = (bf16[272,512]{1,0:T(8,128)(2,1)S(1)}, bf16[272,512]{1,0:T(8,128)(2,1)S(1)}, u32[]{:S(2)}, u32[]{:S(2)}) collective-permute-start(bf16[272,512]{1,0:T(8,128)(2,1)S(1)} %get-tuple-element.66.own), channel_id=1, source_target_pairs={{0,8},{8,16},{16,24},{24,0},{1,9},{9,17},{17,25},{25,1},{2,10},{10... | collective-permute-start | bytes 835592 | tf_op jit(solution)/shard_map/ppermute | solution.py:634
  24.4 8.0 %copy-start = (bf16[512,2048]{1,0:T(8,128)(2,1)S(1)}, bf16[512,2048]{1,0:T(8,128)(2,1)}, u32[]{:S(2)}) copy-start(bf16[512,2048]{1,0:T(8,128)(2,1)} %ws.3) | copy-start | bytes 6291460
  24.4 8.3 %copy-start.13 = (f32[64]{0:T(128)S(1)}, f32[64]{0:T(128)}, u32[]{:S(2)}) copy-start(f32[64]{0:T(128)} %param.28) | copy-start | bytes 772
  24.4 8.3 %copy-start.14 = (f32[64]{0:T(128)S(1)}, f32[64]{0:T(128)}, u32[]{:S(2)}) copy-start(f32[64]{0:T(128)} %param.29) | copy-start | bytes 772
  24.4 8.3 %copy-start.16 = (f32[64,1280]{1,0:T(8,128)S(1)}, f32[64,1280]{1,0:T(8,128)}, u32[]{:S(2)}) copy-start(f32[64,1280]{1,0:T(8,128)} %constant.7.clone.near) | copy-start | bytes 983044
  24.4 8.3 %copy-start.17 = (f32[16,1,64]{2,1,0:T(1,128)S(1)}, f32[16,1,64]{2,1,0:T(1,128)}, u32[]{:S(2)}) copy-start(f32[16,1,64]{2,1,0:T(1,128)} %constant.8.clone.far) | copy-start | bytes 12292
  30.2 25.2 %collective-permute-start.9 = (bf16[256,2048]{1,0:T(8,128)(2,1)S(1)}, bf16[256,2048]{1,0:T(8,128)(2,1)S(1)}, u32[]{:S(2)}, u32[]{:S(2)}) collective-permute-start(bf16[256,2048]{1,0:T(8,128)(2,1)S(1)} %copy-done.1), channel_id=1, source_target_pairs={{0,1},{1,0},{2,3},{3,2},{4,5},{5,4},{6,7},{7,6},{8,9},{9,8},{10,11... | collective-permute-start | bytes 3145736 | tf_op jit(solution)/shard_map/ppermute | solution.py:673
  32.4 23.4 %collective-permute-start.10 = (bf16[512,2048]{1,0:T(8,128)(2,1)S(1)}, bf16[512,2048]{1,0:T(8,128)(2,1)S(1)}, u32[]{:S(2)}, u32[]{:S(2)}) collective-permute-start(bf16[512,2048]{1,0:T(8,128)(2,1)S(1)} %copy-done), channel_id=1, source_target_pairs={{0,1},{1,0},{2,3},{3,2},{4,5},{5,4},{6,7},{7,6},{8,9},{9,8},{10,11... | collective-permute-start | bytes 6291464 | tf_op jit(solution)/shard_map/ppermute | solution.py:674
  37.5 8.0 %copy-start.15 = (f32[4]{0:T(128)S(1)}, f32[4]{0:T(128)}, u32[]{:S(2)}) copy-start(f32[4]{0:T(128)} %sink.1) | copy-start | bytes 52
  39.8 10.2 %collective-permute-start.5 = (bf16[144,512]{1,0:T(8,128)(2,1)S(1)}, bf16[144,512]{1,0:T(8,128)(2,1)S(1)}, u32[]{:S(2)}, u32[]{:S(2)}) collective-permute-start(bf16[144,512]{1,0:T(8,128)(2,1)S(1)} %get-tuple-element.68), channel_id=1, source_target_pairs={{0,32},{32,64},{64,96},{96,0},{1,33},{33,65},{65,97},{97,1},{2,34}... | collective-permute-start | bytes 442376 | tf_op jit(solution)/shard_map/ppermute | solution.py:634
  41.5 9.9 %collective-permute-start.6 = (bf16[144,512]{1,0:T(8,128)(2,1)S(1)}, bf16[144,512]{1,0:T(8,128)(2,1)S(1)}, u32[]{:S(2)}, u32[]{:S(2)}) collective-permute-start(bf16[144,512]{1,0:T(8,128)(2,1)S(1)} %get-tuple-element.69), channel_id=1, source_target_pairs={{0,64},{32,96},{64,0},{96,32},{1,65},{33,97},{65,1},{97,33},{2,66}... | collective-permute-start | bytes 442376 | tf_op jit(solution)/shard_map/ppermute | solution.py:634
  44.8 6.6 %collective-permute-start.7 = (bf16[144,512]{1,0:T(8,128)(2,1)S(1)}, bf16[144,512]{1,0:T(8,128)(2,1)S(1)}, u32[]{:S(2)}, u32[]{:S(2)}) collective-permute-start(bf16[144,512]{1,0:T(8,128)(2,1)S(1)} %get-tuple-element.70), channel_id=1, source_target_pairs={{0,96},{32,0},{64,32},{96,64},{1,97},{33,1},{65,33},{97,65},{2,98}... | collective-permute-start | bytes 442376 | tf_op jit(solution)/shard_map/ppermute | solution.py:634
  52.5 3.3 %collective-permute-start.8 = (bf16[4,128,768]{2,1,0:T(8,128)(2,1)S(1)}, bf16[4,128,768]{2,1,0:T(8,128)(2,1)S(1)}, u32[]{:S(2)}, u32[]{:S(2)}) collective-permute-start(bf16[4,128,768]{2,1,0:T(8,128)(2,1)S(1)} %get-tuple-element.74), channel_id=1, source_target_pairs={{0,1},{1,0},{2,3},{3,2},{4,5},{5,4},{6,7},{7,6},{8,9},{9,8},{10,11... | collective-permute-start | bytes 2359304 | tf_op jit(solution)/shard_map/ppermute | solution.py:682
  56.4 8.8 %collective-permute-start.13 = (bf16[64,2048]{1,0:T(8,128)(2,1)S(1)}, bf16[64,2048]{1,0:T(8,128)(2,1)S(1)}, u32[]{:S(2)}, u32[]{:S(2)}) collective-permute-start(bf16[64,2048]{1,0:T(8,128)(2,1)S(1)} %get-tuple-element.82), channel_id=1, source_target_pairs={{0,2},{2,4},{4,6},{6,0},{1,3},{3,5},{5,7},{7,1},{8,10},{10,12},{12... | collective-permute-start | bytes 786440 | tf_op jit(solution)/shard_map/ppermute | solution.py:693
  57.7 7.6 %collective-permute-start.15 = (bf16[64,2048]{1,0:T(8,128)(2,1)S(1)}, bf16[64,2048]{1,0:T(8,128)(2,1)S(1)}, u32[]{:S(2)}, u32[]{:S(2)}) collective-permute-start(bf16[64,2048]{1,0:T(8,128)(2,1)S(1)} %get-tuple-element.84), channel_id=1, source_target_pairs={{2,0},{4,2},{6,4},{0,6},{3,1},{5,3},{7,5},{1,7},{10,8},{12,10},{14... | collective-permute-start | bytes 786440 | tf_op jit(solution)/shard_map/ppermute | solution.py:694
  61.9 8.5 %collective-permute-start.11 = (bf16[64,2048]{1,0:T(8,128)(2,1)S(1)}, bf16[64,2048]{1,0:T(8,128)(2,1)S(1)}, u32[]{:S(2)}, u32[]{:S(2)}) collective-permute-start(bf16[64,2048]{1,0:T(8,128)(2,1)S(1)} %get-tuple-element.78), channel_id=1, source_target_pairs={{0,2},{2,4},{4,6},{6,0},{1,3},{3,5},{5,7},{7,1},{8,10},{10,12},{12... | collective-permute-start | bytes 786440 | tf_op jit(solution)/shard_map/ppermute | solution.py:693
  62.0 8.5 %collective-permute-start.12 = (bf16[64,2048]{1,0:T(8,128)(2,1)S(1)}, bf16[64,2048]{1,0:T(8,128)(2,1)S(1)}, u32[]{:S(2)}, u32[]{:S(2)}) collective-permute-start(bf16[64,2048]{1,0:T(8,128)(2,1)S(1)} %get-tuple-element.79), channel_id=1, source_target_pairs={{2,0},{4,2},{6,4},{0,6},{3,1},{5,3},{7,5},{1,7},{10,8},{12,10},{14... | collective-permute-start | bytes 786440 | tf_op jit(solution)/shard_map/ppermute | solution.py:694
  65.2 10.8 %collective-permute-start.14 = (bf16[64,2048]{1,0:T(8,128)(2,1)S(1)}, bf16[64,2048]{1,0:T(8,128)(2,1)S(1)}, u32[]{:S(2)}, u32[]{:S(2)}) collective-permute-start(bf16[64,2048]{1,0:T(8,128)(2,1)S(1)} %add_convert_fusion.1), channel_id=1, source_target_pairs={{0,2},{2,4},{4,6},{6,0},{1,3},{3,5},{5,7},{7,1},{8,10},{10,12},{12... | collective-permute-start | bytes 786440 | tf_op jit(solution)/shard_map/ppermute | solution.py:693
  65.4 10.7 %collective-permute-start.16 = (bf16[64,2048]{1,0:T(8,128)(2,1)S(1)}, bf16[64,2048]{1,0:T(8,128)(2,1)S(1)}, u32[]{:S(2)}, u32[]{:S(2)}) collective-permute-start(bf16[64,2048]{1,0:T(8,128)(2,1)S(1)} %add_convert_fusion), channel_id=1, source_target_pairs={{2,0},{4,2},{6,4},{0,6},{3,1},{5,3},{7,5},{1,7},{10,8},{12,10},{14... | collective-permute-start | bytes 786440 | tf_op jit(solution)/shard_map/ppermute | solution.py:694
  (11 other events, 73.4 us)

commit v5 on v4

--- a/solution.py
+++ b/solution.py
@@ -270,7 +270,7 @@
     return tail[0:1] + tail[1:2] + tail[2:3], tail[3:4] + tail[4:5] + tail[5:6]
 
 
-def line_kernel(own, d1, d2, d3, m1, m2, m3, part_ref):
+def line_kernel(own, d3, d2, d1, m1, m2, m3, part_ref):
     place, level = lax.axis_index("y"), lax.axis_index("z")
     got = (own, d1, d2, d3)
     logs = [logs_of(r) for r in got]
@@ -653,7 +653,7 @@
         line_kernel, "line", 4,
         [shaped((STATE + 16, INNER), BF16)] * 3 + [shaped((PACK, INNER), F32)],
         size=4, flops=1e9,
-    )(state, *got)
+    )(state, *got[::-1])
 
     far_got = along(messages, "z")
 

time: 77.6 us -> 77 us (level)
  waiting for transfers between devices: 12.2 us -> 10.1 us
  starting transfers between devices: 28 us -> 29.6 us
    ppermute x6, waiting for transfers between devices: 3.29 us -> 1.17 us  [along(): lax.ppermute(values[d - 1], axis, [(k, (k + d) % LINE) for k in range(LIN...]
    ppermute x6, starting transfers between devices: 10.4 us -> 11.6 us  [along(): lax.ppermute(values[d - 1], axis, [(k, (k + d) % LINE) for k in range(LIN...]
  transfers between devices with their start and end apart: 17 -> 17, of which waited for: 8 -> 7; matrix products, arithmetic and copies ran while one was open for 0% -> 0% of each run, Pallas kernels for 35% -> 35%
where the time goes in v5:
time: 77 us; the launch traced here: 76.5 us
  Pallas kernels  36.2 us (47%)
  starting transfers between devices  29.6 us (38%)
  waiting for transfers between devices  10.1 us (13%)
    ppermute x6, starting transfers between devices, along(): lax.ppermute(values[d - 1], axis, [(k, (k + d) % LINE) for k in range(LIN...  11.6 us
    ppermute x3, waiting for transfers between devices, local(): shift_right = lambda value: lax.ppermute(value, 'x', right)  8.34 us
    ppermute x3, starting transfers between devices, local(): shift_left = lambda value: lax.ppermute(value, 'x', left)  6.95 us
    pallas_call x1, Pallas kernels, local(): plain(front_kernel, 'front', 5, [shaped((ROWS, WIDTH), BF16), shaped((CON...  6.02 us
    pallas_call x1, Pallas kernels, local(): plain(mixer_kernel, 'mixer', 8, [shaped((ROWS, INNER), F32)], scratch=[pl...  5.79 us
    pallas_call x1, Pallas kernels, local(): plain(state_kernel, 'state', 12, [shaped((ROWS, INNER), BF16), shaped((RO...  5.77 us
    pallas_call x1, Pallas kernels, local(): plain(heads_kernel, 'heads', 10, [shaped((ROWS, INNER), BF16), shaped((QH...  4.85 us
    pallas_call x1, Pallas kernels, local(): plain(attend_kernel, 'attend', 3, [shaped((ROWS, QHEADS * HEAD), BF16)],...  4.4 us
  transfers between devices with their start and end apart: 17, of which 7 were waited for; matrix products, arithmetic and copies ran while one was open for 0% of the time, Pallas kernels for 35%

profile of v5, /device:TPU:1, one launch (start us, length us, event | category | flops | bytes accessed | tf_op | source)
XLA Modules:
  0.0 76.5 jit_solution(7528517015045777646)
XLA Ops:
  0.0 2.3 %edge.1 = (bf16[24,2048]{1,0:T(8,128)(2,1)S(1)}, bf16[24,2048]{1,0:T(8,128)(2,1)S(1)}) custom-call(bf16[16,128]{1,0:T(8,128)(2,1)} %bitcast.15, bf16[1024,2048]{1,0:T(8,128)(2,1)} %tok.3, bf16[64,2048]{1,0:T(8,128)(2,1)} %bitcast.20, bf16[64,2048]{1,0:T(8,128)(2,1)} %bitcast.22), custom_call_target="tpu_custom_call" | custom-call | flops 10000000000 | bytes 8388608 | tf_op jit(solution)/shard_map/edge/pallas_call | solution.py:589
  2.3 4.2 %collective-permute-start = (bf16[24,2048]{1,0:T(8,128)(2,1)S(1)}, bf16[24,2048]{1,0:T(8,128)(2,1)S(1)}, u32[]{:S(2)}, u32[]{:S(2)}) collective-permute-start(bf16[24,2048]{1,0:T(8,128)(2,1)S(1)} %get-tuple-element.47), channel_id=1, source_target_pairs={{0,8},{8,16},{16,24},{24,32},{32,40},{40,48},{48,56},{56,64},{64,7... | collective-permute-start | bytes 294920 | tf_op jit(solution)/shard_map/ppermute | solution.py:597
  6.5 1.3 %collective-permute-start.1 = (bf16[24,2048]{1,0:T(8,128)(2,1)S(1)}, bf16[24,2048]{1,0:T(8,128)(2,1)S(1)}, u32[]{:S(2)}, u32[]{:S(2)}) collective-permute-start(bf16[24,2048]{1,0:T(8,128)(2,1)S(1)} %get-tuple-element.48), channel_id=1, source_target_pairs={{8,0},{16,8},{24,16},{32,24},{40,32},{48,40},{56,48},{64,56},{72,6... | collective-permute-start | bytes 294920 | tf_op jit(solution)/shard_map/ppermute | solution.py:598
  7.9 6.0 %front.1 = (bf16[1024,2048]{1,0:T(8,128)(2,1)S(1)}, f32[6,1024,128]{2,1,0:T(8,128)S(1)}, f32[16,1024]{1,0:T(8,128)S(1)}, bf16[2048,512]{1,0:T(8,128)(2,1)S(1)}, ...) custom-call(bf16[16,128]{1,0:T(8,128)(2,1)S(1)} %bitcast.16, bf16[2048,512]{1,0:T(8,128)(2,1)S(1)} %copy-done.5, ...), custom_call_target="tpu_custom_call" | custom-call | flops 10000000000 | bytes 8388608 | tf_op jit(solution)/shard_map/front/pallas_call | solution.py:603
  14.0 5.8 %state.1 = (bf16[1024,512]{1,0:T(8,128)(2,1)S(1)}, bf16[1024,128]{1,0:T(8,128)(2,1)S(1)}, bf16[1024,128]{1,0:T(8,128)(2,1)S(1)}, f32[16,1024]{1,0:T(8,128)S(1)},...) custom-call(f32[2,8]{1,0:T(2,128)S(1)} %copy-done.12, ...), custom_call_target="tpu_custom_call" | custom-call | flops 6000000000 | bytes 8388608 | tf_op jit(solution)/shard_map/state/pallas_call | solution.py:616
  19.7 2.1 %collective-permute-start.4 = (bf16[272,512]{1,0:T(8,128)(2,1)S(1)}, bf16[272,512]{1,0:T(8,128)(2,1)S(1)}, u32[]{:S(2)}, u32[]{:S(2)}) collective-permute-start(bf16[272,512]{1,0:T(8,128)(2,1)S(1)} %get-tuple-element.66.own), channel_id=1, source_target_pairs={{0,8},{8,16},{16,24},{24,0},{1,9},{9,17},{17,25},{25,1},{2,10},{10... | collective-permute-start | bytes 835592 | tf_op jit(solution)/shard_map/ppermute | solution.py:634
  21.9 2.6 %collective-permute-start.3 = (bf16[272,512]{1,0:T(8,128)(2,1)S(1)}, bf16[272,512]{1,0:T(8,128)(2,1)S(1)}, u32[]{:S(2)}, u32[]{:S(2)}) collective-permute-start(bf16[272,512]{1,0:T(8,128)(2,1)S(1)} %get-tuple-element.66.own), channel_id=1, source_target_pairs={{0,16},{8,24},{16,0},{24,8},{1,17},{9,25},{17,1},{25,9},{2,18},{10... | collective-permute-start | bytes 835592 | tf_op jit(solution)/shard_map/ppermute | solution.py:634
  24.5 1.1 %collective-permute-start.2 = (bf16[272,512]{1,0:T(8,128)(2,1)S(1)}, bf16[272,512]{1,0:T(8,128)(2,1)S(1)}, u32[]{:S(2)}, u32[]{:S(2)}) collective-permute-start(bf16[272,512]{1,0:T(8,128)(2,1)S(1)} %get-tuple-element.66.own), channel_id=1, source_target_pairs={{0,24},{8,0},{16,8},{24,16},{1,25},{9,1},{17,9},{25,17},{2,26},{10... | collective-permute-start | bytes 835592 | tf_op jit(solution)/shard_map/ppermute | solution.py:634
  25.6 5.8 %mixer.1.y = f32[1024,512]{1,0:T(8,128)S(1)} custom-call(bf16[1024,512]{1,0:T(8,128)(2,1)S(1)} %get-tuple-element.49.x_ref, bf16[1024,128]{1,0:T(8,128)(2,1)S(1)} %get-tuple-element.50.b_ref, bf16[1024,128]{1,0:T(8,128)(2,1)S(1)} %get-tuple-element.51.c_ref.c, f32[16,1024]{1,0:T(8,128)S(1)} %get-tuple-element.52.cum_ref, ...), custom_call_target="tpu_custom_call" | custom-call | flops 10000000000 | bytes 8388608 | tf_op jit(solution)/shard_map/mixer/pallas_call | solution.py:667
  31.4 2.2 %collective-permute-start.9 = (bf16[256,2048]{1,0:T(8,128)(2,1)S(1)}, bf16[256,2048]{1,0:T(8,128)(2,1)S(1)}, u32[]{:S(2)}, u32[]{:S(2)}) collective-permute-start(bf16[256,2048]{1,0:T(8,128)(2,1)S(1)} %copy-done.1), channel_id=1, source_target_pairs={{0,1},{1,0},{2,3},{3,2},{4,5},{5,4},{6,7},{7,6},{8,9},{9,8},{10,11... | collective-permute-start | bytes 3145736 | tf_op jit(solution)/shard_map/ppermute | solution.py:673
  33.9 4.8 %heads.1 = (bf16[1024,512]{1,0:T(8,128)(2,1)S(1)}, bf16[256,1024]{1,0:T(8,128)(2,1)S(1)}, bf16[64,1280]{1,0:T(8,128)(2,1)S(1)}, bf16[64,1280]{1,0:T(8,128)(2,1)S(1)}) custom-call(bf16[1024,2048]{1,0:T(8,128)(2,1)S(1)} %get-tuple-element.58.normed, bf16[24,2048]{1,0:T(8,128)(2,1)S(1)} %collective-permute-done.low, ...), custom_call_target="tpu_custom_call" | custom-call | flops 7000000000 | bytes 8388608 | tf_op jit(solution)/shard_map/heads/pallas_call | solution.py:642
  39.2 1.7 %collective-permute-start.5 = (bf16[144,512]{1,0:T(8,128)(2,1)S(1)}, bf16[144,512]{1,0:T(8,128)(2,1)S(1)}, u32[]{:S(2)}, u32[]{:S(2)}) collective-permute-start(bf16[144,512]{1,0:T(8,128)(2,1)S(1)} %get-tuple-element.68), channel_id=1, source_target_pairs={{0,32},{32,64},{64,96},{96,0},{1,33},{33,65},{65,97},{97,1},{2,34}... | collective-permute-start | bytes 442376 | tf_op jit(solution)/shard_map/ppermute | solution.py:634
  40.9 3.3 %collective-permute-start.6 = (bf16[144,512]{1,0:T(8,128)(2,1)S(1)}, bf16[144,512]{1,0:T(8,128)(2,1)S(1)}, u32[]{:S(2)}, u32[]{:S(2)}) collective-permute-start(bf16[144,512]{1,0:T(8,128)(2,1)S(1)} %get-tuple-element.69), channel_id=1, source_target_pairs={{0,64},{32,96},{64,0},{96,32},{1,65},{33,97},{65,1},{97,33},{2,66}... | collective-permute-start | bytes 442376 | tf_op jit(solution)/shard_map/ppermute | solution.py:634
  45.0 4.4 %attend.1.attn = bf16[1024,256]{1,0:T(8,128)(2,1)S(1)} custom-call(f32[4]{0:T(128)S(1)} %copy-done.15, bf16[256,1024]{1,0:T(8,128)(2,1)S(1)} %get-tuple-element.63.qs, bf16[64,1280]{1,0:T(8,128)(2,1)S(1)} %get-tuple-element.64.ks, bf16[64,1280]{1,0:T(8,128)(2,1)S(1)} %get-tuple-element.65.vs), custom_call_target="tpu_custom_call" | custom-call | flops 7000000000 | bytes 8388608 | tf_op jit(solution)/shard_map/attend/pallas_call | solution.py:660
  49.4 1.2 %collective-permute-done.6.d2 = bf16[144,512]{1,0:T(8,128)(2,1)S(1)} collective-permute-done((bf16[144,512]{1,0:T(8,128)(2,1)S(1)}, bf16[144,512]{1,0:T(8,128)(2,1)S(1)}, u32[]{:S(2)}, u32[]{:S(2)}) %collective-permute-start.6) | collective-permute-done | bytes 147488 | tf_op jit(solution)/shard_map/ppermute | solution.py:634
  51.6 1.7 %collective-permute-start.8 = (bf16[4,128,768]{2,1,0:T(8,128)(2,1)S(1)}, bf16[4,128,768]{2,1,0:T(8,128)(2,1)S(1)}, u32[]{:S(2)}, u32[]{:S(2)}) collective-permute-start(bf16[4,128,768]{2,1,0:T(8,128)(2,1)S(1)} %get-tuple-element.74), channel_id=1, source_target_pairs={{0,1},{1,0},{2,3},{3,2},{4,5},{5,4},{6,7},{7,6},{8,9},{9,8},{10,11... | collective-permute-start | bytes 2359304 | tf_op jit(solution)/shard_map/ppermute | solution.py:682
  53.3 1.5 %mine.1 = (bf16[4,128,768]{2,1,0:T(8,128)(2,1)S(1)}, f32[128,2048]{1,0:T(8,128)S(1)}) custom-call(f32[1024,512]{1,0:T(8,128)S(1)} %mixer.1.y, bf16[1024,128]{1,0:T(8,128)(2,1)S(1)} %get-tuple-element.51.c_ref.c, f32[16,1024]{1,0:T(8,128)S(1)} %get-tuple-element.57.run, bf16[1024,512]{1,0:T(8,128)(2,1)S(1)} %get-tuple-element.62.gate, ...), custom_call_target="tpu_custom_call" | custom-call | flops 2000000000 | bytes 8388608 | tf_op jit(solution)/shard_map/mine/pallas_call | solution.py:683
  55.8 1.3 %collective-permute-start.13 = (bf16[64,2048]{1,0:T(8,128)(2,1)S(1)}, bf16[64,2048]{1,0:T(8,128)(2,1)S(1)}, u32[]{:S(2)}, u32[]{:S(2)}) collective-permute-start(bf16[64,2048]{1,0:T(8,128)(2,1)S(1)} %get-tuple-element.82), channel_id=1, source_target_pairs={{0,2},{2,4},{4,6},{6,0},{1,3},{3,5},{5,7},{7,1},{8,10},{10,12},{12... | collective-permute-start | bytes 786440 | tf_op jit(solution)/shard_map/ppermute | solution.py:693
  57.1 1.6 %collective-permute-start.15 = (bf16[64,2048]{1,0:T(8,128)(2,1)S(1)}, bf16[64,2048]{1,0:T(8,128)(2,1)S(1)}, u32[]{:S(2)}, u32[]{:S(2)}) collective-permute-start(bf16[64,2048]{1,0:T(8,128)(2,1)S(1)} %get-tuple-element.84), channel_id=1, source_target_pairs={{2,0},{4,2},{6,4},{0,6},{3,1},{5,3},{7,5},{1,7},{10,8},{12,10},{14... | collective-permute-start | bytes 786440 | tf_op jit(solution)/shard_map/ppermute | solution.py:694
  58.7 2.7 %beside.1 = (bf16[64,2048]{1,0:T(8,128)(2,1)S(1)}, bf16[64,2048]{1,0:T(8,128)(2,1)S(1)}, f32[64,2048]{1,0:T(8,128)S(1)}, f32[64,2048]{1,0:T(8,128)S(1)}, f32[128,2048]{1,0:T(8,128)S(1)}) custom-call(bf16[4,128,768]{2,1,0:T(8,128)(2,1)S(1)} %get-tuple-element.73.mine, bf16[4,128,768]{2,1,0:T(8,128)(2,1)S(1)} %collective-permute-done.8.theirs, ...), custom_call_target="tpu_custom_call" | custom-call | flops 3000000000 | bytes 8388608 | tf_op jit(solution)/shard_map/beside/pallas_call | solution.py:700
  61.4 2.7 %collective-permute-start.12 = (bf16[64,2048]{1,0:T(8,128)(2,1)S(1)}, bf16[64,2048]{1,0:T(8,128)(2,1)S(1)}, u32[]{:S(2)}, u32[]{:S(2)}) collective-permute-start(bf16[64,2048]{1,0:T(8,128)(2,1)S(1)} %get-tuple-element.79), channel_id=1, source_target_pairs={{2,0},{4,2},{6,4},{0,6},{3,1},{5,3},{7,5},{1,7},{10,8},{12,10},{14... | collective-permute-start | bytes 786440 | tf_op jit(solution)/shard_map/ppermute | solution.py:694
  64.8 2.7 %collective-permute-start.16 = (bf16[64,2048]{1,0:T(8,128)(2,1)S(1)}, bf16[64,2048]{1,0:T(8,128)(2,1)S(1)}, u32[]{:S(2)}, u32[]{:S(2)}) collective-permute-start(bf16[64,2048]{1,0:T(8,128)(2,1)S(1)} %add_convert_fusion), channel_id=1, source_target_pairs={{2,0},{4,2},{6,4},{0,6},{3,1},{5,3},{7,5},{1,7},{10,8},{12,10},{14... | collective-permute-start | bytes 786440 | tf_op jit(solution)/shard_map/ppermute | solution.py:694
  67.5 2.3 %collective-permute-done.11.direct_right = bf16[64,2048]{1,0:T(8,128)(2,1)S(1)} collective-permute-done((bf16[64,2048]{1,0:T(8,128)(2,1)S(1)}, bf16[64,2048]{1,0:T(8,128)(2,1)S(1)}, u32[]{:S(2)}, u32[]{:S(2)}) %collective-permute-start.11) | collective-permute-done | bytes 262176 | tf_op jit(solution)/shard_map/ppermute | solution.py:693
  69.9 5.5 %collective-permute-done.14.last_right = bf16[64,2048]{1,0:T(8,128)(2,1)S(1)} collective-permute-done((bf16[64,2048]{1,0:T(8,128)(2,1)S(1)}, bf16[64,2048]{1,0:T(8,128)(2,1)S(1)}, u32[]{:S(2)}, u32[]{:S(2)}) %collective-permute-start.14) | collective-permute-done | bytes 262176 | tf_op jit(solution)/shard_map/ppermute | solution.py:693
  (60 shorter events, 5.5 us)
Async XLA Ops:
  0.0 7.8 %copy-start.7 = (bf16[2048,128]{1,0:T(8,128)(2,1)S(1)}, bf16[2048,128]{1,0:T(8,128)(2,1)}, u32[]{:S(2)}) copy-start(bf16[2048,128]{1,0:T(8,128)(2,1)} %w_out.3) | copy-start | bytes 1572868
  0.0 7.8 %copy-start.10 = (bf16[2048]{0:T(1024)(128)(2,1)S(1)}, bf16[2048]{0:T(1024)(128)(2,1)}, u32[]{:S(2)}) copy-start(bf16[2048]{0:T(1024)(128)(2,1)} %param.24) | copy-start | bytes 12292
  2.3 11.6 %collective-permute-start = (bf16[24,2048]{1,0:T(8,128)(2,1)S(1)}, bf16[24,2048]{1,0:T(8,128)(2,1)S(1)}, u32[]{:S(2)}, u32[]{:S(2)}) collective-permute-start(bf16[24,2048]{1,0:T(8,128)(2,1)S(1)} %get-tuple-element.47), channel_id=1, source_target_pairs={{0,8},{8,16},{16,24},{24,32},{32,40},{40,48},{48,56},{56,64},{64,7... | collective-permute-start | bytes 294920 | tf_op jit(solution)/shard_map/ppermute | solution.py:597
  6.5 7.5 %collective-permute-start.1 = (bf16[24,2048]{1,0:T(8,128)(2,1)S(1)}, bf16[24,2048]{1,0:T(8,128)(2,1)S(1)}, u32[]{:S(2)}, u32[]{:S(2)}) collective-permute-start(bf16[24,2048]{1,0:T(8,128)(2,1)S(1)} %get-tuple-element.48), channel_id=1, source_target_pairs={{8,0},{16,8},{24,16},{32,24},{40,32},{48,40},{56,48},{64,56},{72,6... | collective-permute-start | bytes 294920 | tf_op jit(solution)/shard_map/ppermute | solution.py:598
  19.7 19.0 %collective-permute-start.4 = (bf16[272,512]{1,0:T(8,128)(2,1)S(1)}, bf16[272,512]{1,0:T(8,128)(2,1)S(1)}, u32[]{:S(2)}, u32[]{:S(2)}) collective-permute-start(bf16[272,512]{1,0:T(8,128)(2,1)S(1)} %get-tuple-element.66.own), channel_id=1, source_target_pairs={{0,8},{8,16},{16,24},{24,0},{1,9},{9,17},{17,25},{25,1},{2,10},{10... | collective-permute-start | bytes 835592 | tf_op jit(solution)/shard_map/ppermute | solution.py:634
  21.9 16.9 %collective-permute-start.3 = (bf16[272,512]{1,0:T(8,128)(2,1)S(1)}, bf16[272,512]{1,0:T(8,128)(2,1)S(1)}, u32[]{:S(2)}, u32[]{:S(2)}) collective-permute-start(bf16[272,512]{1,0:T(8,128)(2,1)S(1)} %get-tuple-element.66.own), channel_id=1, source_target_pairs={{0,16},{8,24},{16,0},{24,8},{1,17},{9,25},{17,1},{25,9},{2,18},{10... | collective-permute-start | bytes 835592 | tf_op jit(solution)/shard_map/ppermute | solution.py:634
  24.5 14.3 %collective-permute-start.2 = (bf16[272,512]{1,0:T(8,128)(2,1)S(1)}, bf16[272,512]{1,0:T(8,128)(2,1)S(1)}, u32[]{:S(2)}, u32[]{:S(2)}) collective-permute-start(bf16[272,512]{1,0:T(8,128)(2,1)S(1)} %get-tuple-element.66.own), channel_id=1, source_target_pairs={{0,24},{8,0},{16,8},{24,16},{1,25},{9,1},{17,9},{25,17},{2,26},{10... | collective-permute-start | bytes 835592 | tf_op jit(solution)/shard_map/ppermute | solution.py:634
  25.6 8.0 %copy-start = (bf16[512,2048]{1,0:T(8,128)(2,1)S(1)}, bf16[512,2048]{1,0:T(8,128)(2,1)}, u32[]{:S(2)}) copy-start(bf16[512,2048]{1,0:T(8,128)(2,1)} %ws.3) | copy-start | bytes 6291460
  25.6 8.3 %copy-start.13 = (f32[64]{0:T(128)S(1)}, f32[64]{0:T(128)}, u32[]{:S(2)}) copy-start(f32[64]{0:T(128)} %param.28) | copy-start | bytes 772
  25.6 8.3 %copy-start.14 = (f32[64]{0:T(128)S(1)}, f32[64]{0:T(128)}, u32[]{:S(2)}) copy-start(f32[64]{0:T(128)} %param.29) | copy-start | bytes 772
  25.6 8.3 %copy-start.16 = (f32[64,1280]{1,0:T(8,128)S(1)}, f32[64,1280]{1,0:T(8,128)}, u32[]{:S(2)}) copy-start(f32[64,1280]{1,0:T(8,128)} %constant.7.clone.near) | copy-start | bytes 983044
  25.6 8.3 %copy-start.17 = (f32[16,1,64]{2,1,0:T(1,128)S(1)}, f32[16,1,64]{2,1,0:T(1,128)}, u32[]{:S(2)}) copy-start(f32[16,1,64]{2,1,0:T(1,128)} %constant.8.clone.far) | copy-start | bytes 12292
  31.4 23.4 %collective-permute-start.9 = (bf16[256,2048]{1,0:T(8,128)(2,1)S(1)}, bf16[256,2048]{1,0:T(8,128)(2,1)S(1)}, u32[]{:S(2)}, u32[]{:S(2)}) collective-permute-start(bf16[256,2048]{1,0:T(8,128)(2,1)S(1)} %copy-done.1), channel_id=1, source_target_pairs={{0,1},{1,0},{2,3},{3,2},{4,5},{5,4},{6,7},{7,6},{8,9},{9,8},{10,11... | collective-permute-start | bytes 3145736 | tf_op jit(solution)/shard_map/ppermute | solution.py:673
  33.6 21.6 %collective-permute-start.10 = (bf16[512,2048]{1,0:T(8,128)(2,1)S(1)}, bf16[512,2048]{1,0:T(8,128)(2,1)S(1)}, u32[]{:S(2)}, u32[]{:S(2)}) collective-permute-start(bf16[512,2048]{1,0:T(8,128)(2,1)S(1)} %copy-done), channel_id=1, source_target_pairs={{0,1},{1,0},{2,3},{3,2},{4,5},{5,4},{6,7},{7,6},{8,9},{9,8},{10,11... | collective-permute-start | bytes 6291464 | tf_op jit(solution)/shard_map/ppermute | solution.py:674
  39.2 10.2 %collective-permute-start.5 = (bf16[144,512]{1,0:T(8,128)(2,1)S(1)}, bf16[144,512]{1,0:T(8,128)(2,1)S(1)}, u32[]{:S(2)}, u32[]{:S(2)}) collective-permute-start(bf16[144,512]{1,0:T(8,128)(2,1)S(1)} %get-tuple-element.68), channel_id=1, source_target_pairs={{0,32},{32,64},{64,96},{96,0},{1,33},{33,65},{65,97},{97,1},{2,34}... | collective-permute-start | bytes 442376 | tf_op jit(solution)/shard_map/ppermute | solution.py:634
  40.9 9.6 %collective-permute-start.6 = (bf16[144,512]{1,0:T(8,128)(2,1)S(1)}, bf16[144,512]{1,0:T(8,128)(2,1)S(1)}, u32[]{:S(2)}, u32[]{:S(2)}) collective-permute-start(bf16[144,512]{1,0:T(8,128)(2,1)S(1)} %get-tuple-element.69), channel_id=1, source_target_pairs={{0,64},{32,96},{64,0},{96,32},{1,65},{33,97},{65,1},{97,33},{2,66}... | collective-permute-start | bytes 442376 | tf_op jit(solution)/shard_map/ppermute | solution.py:634
  44.2 6.3 %collective-permute-start.7 = (bf16[144,512]{1,0:T(8,128)(2,1)S(1)}, bf16[144,512]{1,0:T(8,128)(2,1)S(1)}, u32[]{:S(2)}, u32[]{:S(2)}) collective-permute-start(bf16[144,512]{1,0:T(8,128)(2,1)S(1)} %get-tuple-element.70), channel_id=1, source_target_pairs={{0,96},{32,0},{64,32},{96,64},{1,97},{33,1},{65,33},{97,65},{2,98}... | collective-permute-start | bytes 442376 | tf_op jit(solution)/shard_map/ppermute | solution.py:634
  51.6 3.6 %collective-permute-start.8 = (bf16[4,128,768]{2,1,0:T(8,128)(2,1)S(1)}, bf16[4,128,768]{2,1,0:T(8,128)(2,1)S(1)}, u32[]{:S(2)}, u32[]{:S(2)}) collective-permute-start(bf16[4,128,768]{2,1,0:T(8,128)(2,1)S(1)} %get-tuple-element.74), channel_id=1, source_target_pairs={{0,1},{1,0},{2,3},{3,2},{4,5},{5,4},{6,7},{7,6},{8,9},{9,8},{10,11... | collective-permute-start | bytes 2359304 | tf_op jit(solution)/shard_map/ppermute | solution.py:682
  55.8 8.8 %collective-permute-start.13 = (bf16[64,2048]{1,0:T(8,128)(2,1)S(1)}, bf16[64,2048]{1,0:T(8,128)(2,1)S(1)}, u32[]{:S(2)}, u32[]{:S(2)}) collective-permute-start(bf16[64,2048]{1,0:T(8,128)(2,1)S(1)} %get-tuple-element.82), channel_id=1, source_target_pairs={{0,2},{2,4},{4,6},{6,0},{1,3},{3,5},{5,7},{7,1},{8,10},{10,12},{12... | collective-permute-start | bytes 786440 | tf_op jit(solution)/shard_map/ppermute | solution.py:693
  57.1 7.6 %collective-permute-start.15 = (bf16[64,2048]{1,0:T(8,128)(2,1)S(1)}, bf16[64,2048]{1,0:T(8,128)(2,1)S(1)}, u32[]{:S(2)}, u32[]{:S(2)}) collective-permute-start(bf16[64,2048]{1,0:T(8,128)(2,1)S(1)} %get-tuple-element.84), channel_id=1, source_target_pairs={{2,0},{4,2},{6,4},{0,6},{3,1},{5,3},{7,5},{1,7},{10,8},{12,10},{14... | collective-permute-start | bytes 786440 | tf_op jit(solution)/shard_map/ppermute | solution.py:694
  61.3 8.5 %collective-permute-start.11 = (bf16[64,2048]{1,0:T(8,128)(2,1)S(1)}, bf16[64,2048]{1,0:T(8,128)(2,1)S(1)}, u32[]{:S(2)}, u32[]{:S(2)}) collective-permute-start(bf16[64,2048]{1,0:T(8,128)(2,1)S(1)} %get-tuple-element.78), channel_id=1, source_target_pairs={{0,2},{2,4},{4,6},{6,0},{1,3},{3,5},{5,7},{7,1},{8,10},{10,12},{12... | collective-permute-start | bytes 786440 | tf_op jit(solution)/shard_map/ppermute | solution.py:693
  61.4 8.5 %collective-permute-start.12 = (bf16[64,2048]{1,0:T(8,128)(2,1)S(1)}, bf16[64,2048]{1,0:T(8,128)(2,1)S(1)}, u32[]{:S(2)}, u32[]{:S(2)}) collective-permute-start(bf16[64,2048]{1,0:T(8,128)(2,1)S(1)} %get-tuple-element.79), channel_id=1, source_target_pairs={{2,0},{4,2},{6,4},{0,6},{3,1},{5,3},{7,5},{1,7},{10,8},{12,10},{14... | collective-permute-start | bytes 786440 | tf_op jit(solution)/shard_map/ppermute | solution.py:694
  64.7 10.8 %collective-permute-start.14 = (bf16[64,2048]{1,0:T(8,128)(2,1)S(1)}, bf16[64,2048]{1,0:T(8,128)(2,1)S(1)}, u32[]{:S(2)}, u32[]{:S(2)}) collective-permute-start(bf16[64,2048]{1,0:T(8,128)(2,1)S(1)} %add_convert_fusion.1), channel_id=1, source_target_pairs={{0,2},{2,4},{4,6},{6,0},{1,3},{3,5},{5,7},{7,1},{8,10},{10,12},{12... | collective-permute-start | bytes 786440 | tf_op jit(solution)/shard_map/ppermute | solution.py:693
  64.8 10.7 %collective-permute-start.16 = (bf16[64,2048]{1,0:T(8,128)(2,1)S(1)}, bf16[64,2048]{1,0:T(8,128)(2,1)S(1)}, u32[]{:S(2)}, u32[]{:S(2)}) collective-permute-start(bf16[64,2048]{1,0:T(8,128)(2,1)S(1)} %add_convert_fusion), channel_id=1, source_target_pairs={{2,0},{4,2},{6,4},{0,6},{3,1},{5,3},{7,5},{1,7},{10,8},{12,10},{14... | collective-permute-start | bytes 786440 | tf_op jit(solution)/shard_map/ppermute | solution.py:694
  (11 other events, 71.5 us)
